TPU v7x, 512 devices: a whole 4x8x8 slice. The times are simulated.
512 devices in a mesh: ep: 128 (over z, y, core), tp: 4 (over x).
Axes of the slice: x: 4, y: 8, z: 8, core: 2. Of those that a mesh axis runs over, the one named last changes fastest.
Arguments:
- residual_in: bfloat16 [256, 2048], P('ep'), may hold values from -6 to 6
- gla_state: float32 [256, 4, 256, 512], P('ep', 'tp'), may hold values from -6 to 6
- norm_gain: bfloat16 [2048], replicated, may hold values from 0.099609375 to 1.8984375
- w_query: bfloat16 [2048, 1024], P('ep', 'tp'), may hold values from -0.125 to 0.125
- w_key: bfloat16 [2048, 1024], P('ep', 'tp'), may hold values from -0.125 to 0.125
- w_value: bfloat16 [2048, 2048], P('ep', 'tp'), may hold values from -0.125 to 0.125
- w_decay: bfloat16 [2048, 1024], P('ep', 'tp'), may hold values from -0.5 to 0.5
- decay_bias: float32 [1024], P('tp'), may hold values from -40 to 8
- head_gain: bfloat16 [512], replicated, may hold values from 0.099609375 to 1.8984375
- w_output: bfloat16 [2048, 2048], P('tp', 'ep'), may hold values from -0.125 to 0.125
- ffn_gain: bfloat16 [2048], replicated, may hold values from 0.099609375 to 1.8984375
- router_group: bfloat16 [2048, 4], replicated, may hold values from -0.125 to 0.125
- router_expert: bfloat16 [128, 2048], replicated, may hold values from -0.125 to 0.125
- expert_ids: int32 [256, 2], replicated, may hold values from 0 to 127, all different within a row; in each aligned block of 256 rows (0 to 255, 256 to 511, ...) at most 16 rows name the same one
- w_gate: bfloat16 [128, 2048, 512], P('ep', None, 'tp'), may hold values from -0.125 to 0.125
- w_up: bfloat16 [128, 2048, 512], P('ep', None, 'tp'), may hold values from -0.125 to 0.125
- w_down: bfloat16 [128, 512, 2048], P('ep', 'tp'), may hold values from -0.75 to 0.75
Outputs:
- layer_out: bfloat16 [256, 2048], P('ep')
- new_state: float32 [256, 4, 256, 512], P('ep', 'tp')
Inputs may be any that keep to these rules, and one draw needn't show every extreme that they name: `expert_ids`: each row names 2 different experts; no expert is named by more than 16 rows of the whole batch, a bound that some block reaches.
All inputs are finite; a program needn't handle non-finite values.
Results may differ from a plain program's by a relative error of at most 0.023.
Values may be sent and summed in bfloat16 or wider, within the bound.
No kernel may reach another device: no remote copies, remote signals or barrier semaphores. Data moves between devices by JAX's collectives and lax.ppermute only.
A program may use at most 64 MiB of HBM per device.

v0:
```python
import jax
import jax.numpy as jnp
from jax import lax
from jax.sharding import Mesh
from jax.sharding import PartitionSpec as P

CAP = 16
EP = ("ep_0", "ep_1", "ep_2")


EPSILON = 1e-06
GATE_SCALE = 16.0


def in_blocks(shard, dim, length):
    shape = shard.shape
    blocks = shard.reshape(*shape[:dim], length, shape[dim] // length, *shape[dim + 1 :])
    return jnp.moveaxis(blocks, dim, 0)


def summed_on_arrival(shard, axis, dim):
    blocks = in_blocks(shard, dim, lax.axis_size(axis))
    arrived = lax.all_to_all(blocks, axis, split_axis=0, concat_axis=0, tiled=True)
    return arrived.sum(axis=0)


def sum_by_axis(shard, axes, dim):
    far, near = axes
    own = summed_on_arrival(in_blocks(shard, dim, lax.axis_size(far)), near, dim + 1)
    return jnp.sum(lax.all_to_all(own, far, 0, 0, tiled=True), axis=0)


def from_everyone(shard, axis):
    copies = jnp.broadcast_to(shard, (lax.axis_size(axis), *shard.shape))
    return lax.all_to_all(copies, axis, split_axis=0, concat_axis=0, tiled=True)


def in_order(blocks, dim):
    shape = list(blocks.shape[1:])
    shape[dim] *= blocks.shape[0]
    return jnp.moveaxis(blocks, 0, dim).reshape(shape)


def whole_of(shard, axes, dim):
    far, near = axes
    blocks = from_everyone(from_everyone(shard, far), near)
    return in_order(blocks.swapaxes(0, 1).reshape(-1, *shard.shape), dim)


def taken_together(shard, axis):
    everything = from_everyone(shard, axis)
    return jnp.sum(everything.astype(jnp.float32), axis=0)


def sent_and_summed(shard, axis, dim):
    length = lax.axis_size(axis)
    blocks = lax.all_to_all(in_blocks(shard, dim, length), axis, 0, 0, tiled=True)
    return jnp.sum(blocks.astype(jnp.float32), axis=0)


def collect(shard, axis, dim):
    return in_order(from_everyone(shard, axis), dim)


def rms_scale(values, gain_vec):
    floats = values.astype(jnp.float32)
    return (
        floats
        * lax.rsqrt(jnp.mean(floats * floats, axis=-1, keepdims=True) + EPSILON)
        * gain_vec.astype(jnp.float32)
    )


def finish_part(hidden_res, moe_part, tp_index):
    part_cols = moe_part.shape[1]
    own_cols = lax.dynamic_slice_in_dim(hidden_res, tp_index * part_cols, part_cols, 1)
    return (own_cols.astype(jnp.float32) + moe_part).astype(jnp.bfloat16)


def on_device(
    residual_in,
    gla_state,
    norm_gain,
    w_query,
    w_key,
    w_value,
    w_decay,
    decay_bias,
    head_gain,
    w_output,
    ffn_gain,
    router_group,
    router_expert,
    expert_ids,
    w_gate,
    w_up,
    w_down,
):
    seq_rows = residual_in.shape[0]
    key_width = w_query.shape[1]
    value_width = w_value.shape[1]
    normed = rms_scale(residual_in, norm_gain).astype(jnp.bfloat16)
    columns = lax.all_to_all(normed, EP, split_axis=1, concat_axis=0, tiled=True)
    projected = sum_by_axis(
        jnp.concatenate(
            [
                jnp.dot(columns, w_query, preferred_element_type=jnp.float32),
                jnp.dot(columns, w_key, preferred_element_type=jnp.float32),
                jnp.dot(columns, w_value, preferred_element_type=jnp.float32),
                jnp.dot(columns, w_decay, preferred_element_type=jnp.float32),
            ],
            axis=1,
        ),
        (("ep_0", "ep_1"), "ep_2"),
        0,
    )
    query_rows = projected[:, :key_width].astype(jnp.bfloat16)
    key_rows = projected[:, key_width : 2 * key_width].astype(jnp.bfloat16)
    value_rows = projected[:, 2 * key_width : 2 * key_width + value_width].astype(jnp.bfloat16)
    decay_pre = projected[:, 2 * key_width + value_width :]
    log_decay = jax.nn.log_sigmoid(decay_pre + decay_bias) / GATE_SCALE
    query_float = lax.optimization_barrier(query_rows).astype(jnp.float32) * key_width ** (-0.5)
    key_float = lax.optimization_barrier(key_rows).astype(jnp.float32)
    value_float = lax.optimization_barrier(value_rows).astype(jnp.float32)
    old_state = gla_state[:, 0]
    new_state = (
        jnp.exp(log_decay)[:, :, None] * old_state + key_float[:, :, None] * value_float[:, None, :]
    )
    read_out = jnp.einsum("tk,tkv->tv", query_float, new_state, precision=lax.Precision.HIGHEST)
    gated_heads = rms_scale(read_out, head_gain).astype(jnp.bfloat16)
    partial_out = jnp.dot(
        whole_of(gated_heads, (("ep_0", "ep_1"), "ep_2"), 0),
        w_output,
        preferred_element_type=jnp.float32,
    ).astype(jnp.bfloat16)
    returned = lax.all_to_all(partial_out, EP, split_axis=0, concat_axis=1, tiled=True)
    attention = taken_together(returned.astype(jnp.float32).astype(jnp.bfloat16), "tp").astype(
        jnp.float32
    )
    hidden_res = (residual_in.astype(jnp.float32) + attention).astype(jnp.bfloat16)
    moe_in = rms_scale(hidden_res, ffn_gain).astype(jnp.bfloat16)
    expert = lax.axis_index(EP)
    is_named = jnp.any(expert_ids == expert, axis=1)
    slot_of = jnp.cumsum(is_named.astype(jnp.int32)) - 1
    slot_index = jnp.arange(CAP, dtype=jnp.int32)
    select_int = (is_named[None, :] & (slot_of[None, :] == slot_index[:, None])).astype(jnp.int32)
    select_bf = select_int.astype(jnp.bfloat16)
    slot_rows = jnp.dot(
        select_bf,
        whole_of(moe_in, (("ep_0", "ep_1"), "ep_2"), 0),
        preferred_element_type=jnp.float32,
    ).astype(jnp.bfloat16)
    slot_ids = jnp.sum(select_int[:, :, None] * expert_ids[None, :, :], axis=1)
    rival_ids = jnp.where(slot_ids[:, 0] == expert, slot_ids[:, 1], slot_ids[:, 0])
    group_logits = jnp.dot(slot_rows, router_group, preferred_element_type=jnp.float32)
    per_group = router_expert.shape[0] // router_group.shape[1]
    own_group = jnp.arange(router_group.shape[1], dtype=jnp.int32) == expert // per_group
    group_logit = jnp.sum(
        jnp.where(own_group[None, :], group_logits, jnp.zeros_like(group_logits)), axis=1
    )
    group_share = 1.0 / jnp.sum(jnp.exp(group_logits - group_logit[:, None]), axis=1)
    chosen = jnp.dot(slot_rows, router_expert[expert], preferred_element_type=jnp.float32)
    rival_logit = jnp.einsum(
        "cd,cd->c", slot_rows, router_expert[rival_ids], preferred_element_type=jnp.float32
    )
    slot_weight = group_share * jax.nn.sigmoid(chosen - rival_logit)
    gate_out = jnp.dot(slot_rows, w_gate[0], preferred_element_type=jnp.float32)
    up_out = jnp.dot(slot_rows, w_up[0], preferred_element_type=jnp.float32)
    hidden = (jax.nn.silu(gate_out) * up_out).astype(jnp.bfloat16)
    output = jnp.dot(hidden, w_down[0], preferred_element_type=jnp.float32)
    select_float = select_int.astype(jnp.float32)
    width_piece = sent_and_summed(output.astype(jnp.bfloat16), "tp", 1)
    weighted_piece = width_piece * slot_weight[:, None]
    piece_cols = weighted_piece.shape[1]
    outgoing = jnp.dot(select_float.T, weighted_piece, precision=lax.Precision.HIGHEST)
    owners = outgoing.shape[0] // seq_rows
    outgoing = outgoing.reshape(owners, seq_rows, piece_cols)
    arrived = lax.all_to_all(
        outgoing.astype(jnp.bfloat16), EP, split_axis=0, concat_axis=0, tiled=True
    ).astype(outgoing.dtype)
    moe_piece = jnp.sum(arrived, axis=0)
    layer_piece = finish_part(hidden_res, moe_piece, lax.axis_index("tp"))
    layer_out = collect(layer_piece, "tp", 1)
    return (layer_out, new_state[:, None])


def solution(mesh):
    torus = Mesh(mesh.devices.reshape(8, 8, 2, mesh.shape["tp"]), ("ep_0", "ep_1", "ep_2", "tp"))
    in_specs = (
        P(EP, None),
        P(EP, "tp", None, None),
        P(),
        P(EP, "tp"),
        P(EP, "tp"),
        P(EP, "tp"),
        P(EP, "tp"),
        P("tp"),
        P(),
        P("tp", EP),
        P(),
        P(),
        P(),
        P(),
        P(EP, None, "tp"),
        P(EP, None, "tp"),
        P(EP, "tp", None),
    )
    out_specs = (P(EP, None), P(EP, "tp", None, None))
    return jax.shard_map(
        on_device, mesh=torus, in_specs=in_specs, out_specs=out_specs, check_vma=False
    )
```

profile of v0, /device:TPU:1, one launch (start us, length us, event | category | flops | bytes accessed | tf_op | source)
XLA Modules:
  0.0 201.6 jit_solution(11595900406696143059)
XLA Ops:
  1.4 0.8 fusion.24
  2.2 0.8 fusion.26
  3.2 29.7 %all_to_all.88 = bf16[2,128,16]{2,0,1:T(2,128)(2,1)S(1)} all-to-all(bf16[2,128,16]{2,0,1:T(2,128)(2,1)S(1)} %copy.63), channel_id=1, replica_groups=mesh['ep_0'=8,'ep_1'=8,'ep_2'=2,'tp'=4] {'ep_0','ep_1','ep_2'}, dimensions={1} | all-to-all | bytes 16384 | tf_op jit(solution)/shard_map/all_to_all | solution.py:103
  32.9 0.9 fusion.62
  33.8 0.8 fusion.60
  36.0 5.0 %all_to_all.89 = f32[2,64,2,1280]{3,2,1,0:T(2,128)S(1)} all-to-all(f32[2,64,2,1280]{3,2,1,0:T(2,128)S(1)} %bitcast.85), channel_id=1, replica_groups=mesh['ep_0'=8,'ep_1'=8,'ep_2'=2,'tp'=4] {'ep_2'}, dimensions={0} | all-to-all | bytes 2621440 | tf_op jit(solution)/shard_map/all_to_all | solution.py:23
  41.0 2.0 %reduce_sum.100 = f32[64,2,1280]{2,1,0:T(2,128)} reduce(f32[2,64,2,1280]{3,2,1,0:T(2,128)S(1)} %all_to_all.89, f32[]{:T(128)} %constant.26.clone.1), dimensions={0}, to_apply=%region_1.0 | reduce | flops 163840 | bytes 1966084 | tf_op jit(solution)/shard_map/reduce_sum | solution.py:24
  43.0 4.8 %all-to-all-start.2 = ((f32[64,2,1280]{2,1,0:T(2,128)}), f32[64,2,1280]{2,1,0:T(2,128)S(1)}, u32[]{:S(2)}, u32[]{:S(2)}) async-start(f32[64,2,1280]{2,1,0:T(2,128)} %reduce_sum.100), calls=%async_computation.2 | async-start | bytes 1310720 | tf_op jit(solution)/shard_map/all_to_all | solution.py:30
  47.8 20.1 %all-to-all-done.2 = f32[64,2,1280]{2,1,0:T(2,128)S(1)} async-done(((f32[64,2,1280]{2,1,0:T(2,128)}), f32[64,2,1280]{2,1,0:T(2,128)S(1)}, u32[]{:S(2)}, u32[]{:S(2)}) %all-to-all-start.2) | async-done | bytes 655392 | tf_op jit(solution)/shard_map/all_to_all | solution.py:30
  70.0 7.0 %all-to-all-start.3 = ((bf16[64,2,512]{2,1,0:T(2,128)(2,1)}), bf16[64,2,512]{2,1,0:T(2,128)(2,1)S(1)}, u32[]{:S(2)}, u32[]{:S(2)}) async-start(bf16[64,2,512]{2,1,0:T(2,128)(2,1)} %broadcast_in_dim.19), calls=%async_computation.3 | async-start | bytes 262144 | tf_op jit(solution)/shard_map/all_to_all | solution.py:35
  77.0 11.5 %all-to-all-done.3 = bf16[64,2,512]{2,1,0:T(2,128)(2,1)S(1)} async-done(((bf16[64,2,512]{2,1,0:T(2,128)(2,1)}), bf16[64,2,512]{2,1,0:T(2,128)(2,1)S(1)}, u32[]{:S(2)}, u32[]{:S(2)}) %all-to-all-start.3) | async-done | bytes 131104 | tf_op jit(solution)/shard_map/all_to_all | solution.py:35
  88.7 6.5 %all_to_all.90 = bf16[2,64,2,512]{3,2,1,0:T(2,128)(2,1)S(1)} all-to-all(bf16[2,64,2,512]{3,2,1,0:T(2,128)(2,1)S(1)} %broadcast_in_dim.20), channel_id=1, replica_groups=mesh['ep_0'=8,'ep_1'=8,'ep_2'=2,'tp'=4] {'ep_2'}, dimensions={0} | all-to-all | bytes 524288 | tf_op jit(solution)/shard_map/all_to_all | solution.py:35
  96.4 5.5 %all-to-all-start.5 = ((bf16[128,2,16]{2,1,0:T(2,128)(2,1)}), bf16[128,2,16]{2,1,0:T(2,128)(2,1)S(1)}, u32[]{:S(2)}, u32[]{:S(2)}) async-start(bf16[128,2,16]{2,1,0:T(2,128)(2,1)} %bitcast.8), calls=%async_computation.5 | async-start | bytes 131072 | tf_op jit(solution)/shard_map/all_to_all | solution.py:136
  101.9 11.5 %all-to-all-done.5 = bf16[128,2,16]{2,1,0:T(2,128)(2,1)S(1)} async-done(((bf16[128,2,16]{2,1,0:T(2,128)(2,1)}), bf16[128,2,16]{2,1,0:T(2,128)(2,1)S(1)}, u32[]{:S(2)}, u32[]{:S(2)}) %all-to-all-start.5) | async-done | bytes 8224 | tf_op jit(solution)/shard_map/all_to_all | solution.py:136
  114.2 4.0 %all-to-all-start.6 = ((bf16[4,2,2048]{2,1,0:T(2,128)(2,1)}), bf16[4,2,2048]{2,1,0:T(2,128)(2,1)S(1)}, u32[]{:S(2)}, u32[]{:S(2)}) async-start(bf16[4,2,2048]{2,1,0:T(2,128)(2,1)} %broadcast_in_dim.21), calls=%async_computation.6 | async-start | bytes 65536 | tf_op jit(solution)/shard_map/all_to_all | solution.py:35
  118.6 3.9 %all-to-all-done.6 = bf16[4,2,2048]{2,1,0:T(2,128)(2,1)S(1)} async-done(((bf16[4,2,2048]{2,1,0:T(2,128)(2,1)}), bf16[4,2,2048]{2,1,0:T(2,128)(2,1)S(1)}, u32[]{:S(2)}, u32[]{:S(2)}) %all-to-all-start.6) | async-done | bytes 32800 | tf_op jit(solution)/shard_map/all_to_all | solution.py:35
  122.8 1.1 broadcast_in_dim.22
  123.9 4.8 %all-to-all-start.7 = ((bf16[64,2,2048]{2,1,0:T(2,128)(2,1)}), bf16[64,2,2048]{2,1,0:T(2,128)(2,1)S(1)}, u32[]{:S(2)}, u32[]{:S(2)}) async-start(bf16[64,2,2048]{2,1,0:T(2,128)(2,1)} %broadcast_in_dim.22), calls=%async_computation.7 | async-start | bytes 1048576 | tf_op jit(solution)/shard_map/all_to_all | solution.py:35
  129.7 14.8 %all-to-all-done.7 = bf16[64,2,2048]{2,1,0:T(2,128)(2,1)S(1)} async-done(((bf16[64,2,2048]{2,1,0:T(2,128)(2,1)}), bf16[64,2,2048]{2,1,0:T(2,128)(2,1)S(1)}, u32[]{:S(2)}, u32[]{:S(2)}) %all-to-all-start.7) | async-done | bytes 524320 | tf_op jit(solution)/shard_map/all_to_all | solution.py:35
  145.0 9.1 %all_to_all.91 = bf16[2,64,2,2048]{3,2,1,0:T(2,128)(2,1)S(1)} all-to-all(bf16[2,64,2,2048]{3,2,1,0:T(2,128)(2,1)S(1)} %broadcast_in_dim.23), channel_id=1, replica_groups=mesh['ep_0'=8,'ep_1'=8,'ep_2'=2,'tp'=4] {'ep_2'}, dimensions={0} | all-to-all | bytes 2097152 | tf_op jit(solution)/shard_map/all_to_all | solution.py:35
  154.1 2.2 %copy.73 = bf16[64,2,2,2048]{3,2,1,0:T(2,128)(2,1)} copy(bf16[64,2,2,2048]{3,2,0,1:T(2,128)(2,1)S(1)} %bitcast.86) | data formatting | bytes 2097152 | tf_op jit(solution)/shard_map/transpose | solution.py:47
  156.3 1.5 reshape_reshape.11
  158.2 1.2 fusion.14
  159.4 1.4 convolution_convert_fusion
  161.5 3.3 %all-to-all-start.9 = ((bf16[4,16,512]{2,1,0:T(8,128)(2,1)}), bf16[4,16,512]{2,1,0:T(8,128)(2,1)S(1)}, u32[]{:S(2)}, u32[]{:S(2)}) async-start(bf16[4,16,512]{2,1,0:T(8,128)(2,1)} %bitcast.84), calls=%async_computation.9 | async-start | bytes 131072 | tf_op jit(solution)/shard_map/all_to_all | solution.py:57
  165.1 4.1 %all-to-all-done.9 = bf16[4,16,512]{2,1,0:T(8,128)(2,1)S(1)} async-done(((bf16[4,16,512]{2,1,0:T(8,128)(2,1)}), bf16[4,16,512]{2,1,0:T(8,128)(2,1)S(1)}, u32[]{:S(2)}, u32[]{:S(2)}) %all-to-all-start.9) | async-done | bytes 65568 | tf_op jit(solution)/shard_map/all_to_all | solution.py:57
  169.9 0.8 convert_element_type.120
  170.7 6.8 %all-to-all-start.10 = ((bf16[128,2,512]{2,1,0:T(2,128)(2,1)}), bf16[128,2,512]{2,1,0:T(2,128)(2,1)S(1)}, u32[]{:S(2)}, u32[]{:S(2)}) async-start(bf16[128,2,512]{2,1,0:T(2,128)(2,1)} %convert_element_type.120), calls=%async_computation.10 | async-start | bytes 524288 | tf_op jit(solution)/shard_map/all_to_all | solution.py:178
  177.5 15.2 %all-to-all-done.10 = bf16[128,2,512]{2,1,0:T(2,128)(2,1)S(1)} async-done(((bf16[128,2,512]{2,1,0:T(2,128)(2,1)}), bf16[128,2,512]{2,1,0:T(2,128)(2,1)S(1)}, u32[]{:S(2)}, u32[]{:S(2)}) %all-to-all-start.10) | async-done | bytes 262176 | tf_op jit(solution)/shard_map/all_to_all | solution.py:178
  193.6 3.2 %all-to-all-start.11 = ((bf16[4,2,512]{2,1,0:T(2,128)(2,1)}), bf16[4,2,512]{2,1,0:T(2,128)(2,1)S(1)}, u32[]{:S(2)}, u32[]{:S(2)}) async-start(bf16[4,2,512]{2,1,0:T(2,128)(2,1)} %broadcast_in_dim.29), calls=%async_computation.11 | async-start | bytes 16384 | tf_op jit(solution)/shard_map/all_to_all | solution.py:35
  196.9 1.2 multiply_add_fusion
  198.0 3.0 %all-to-all-done.11 = bf16[4,2,512]{2,1,0:T(2,128)(2,1)S(1)} async-done(((bf16[4,2,512]{2,1,0:T(2,128)(2,1)}), bf16[4,2,512]{2,1,0:T(2,128)(2,1)S(1)}, u32[]{:S(2)}, u32[]{:S(2)}) %all-to-all-start.11) | async-done | bytes 8224 | tf_op jit(solution)/shard_map/all_to_all | solution.py:35
  (85 shorter events, 12.0 us)
Async XLA Ops:
  0.6 128.4 %copy-start = (bf16[128,2048]{1,0:T(8,128)(2,1)S(1)}, bf16[128,2048]{1,0:T(8,128)(2,1)}, u32[]{:S(2)}) copy-start(bf16[128,2048]{1,0:T(8,128)(2,1)} %param.29) | copy-start | bytes 1572868
  0.6 34.0 %copy-start.6 = (bf16[16,256]{1,0:T(8,128)(2,1)S(1)}, bf16[16,256]{1,0:T(8,128)(2,1)}, u32[]{:S(2)}) copy-start(bf16[16,256]{1,0:T(8,128)(2,1)} %param.21) | copy-start | bytes 24580
  0.7 34.2 %copy-start.7 = (bf16[16,256]{1,0:T(8,128)(2,1)S(1)}, bf16[16,256]{1,0:T(8,128)(2,1)}, u32[]{:S(2)}) copy-start(bf16[16,256]{1,0:T(8,128)(2,1)} %param.23) | copy-start | bytes 24580
  41.0 6.8 %copy-start.9 = (bf16[512]{0:T(512)(128)(2,1)S(1)}, bf16[512]{0:T(512)(128)(2,1)}, u32[]{:S(2)}) copy-start(bf16[512]{0:T(512)(128)(2,1)} %param.25) | copy-start | bytes 3076
  43.0 25.2 %copy-start.10 = (f32[256]{0:T(256)S(1)}, f32[256]{0:T(256)}, u32[]{:S(2)}) copy-start(f32[256]{0:T(256)} %param.24) | copy-start | bytes 3076
  43.0 25.2 %copy-start.1 = (f32[2,1,256,512]{3,2,1,0:T(8,128)S(1)}, f32[2,1,256,512]{3,2,1,0:T(8,128)}, u32[]{:S(2)}) copy-start(f32[2,1,256,512]{3,2,1,0:T(8,128)} %param.18) | copy-start | bytes 3145732
  43.0 24.9 %all-to-all-start.2 = ((f32[64,2,1280]{2,1,0:T(2,128)}), f32[64,2,1280]{2,1,0:T(2,128)S(1)}, u32[]{:S(2)}, u32[]{:S(2)}) async-start(f32[64,2,1280]{2,1,0:T(2,128)} %reduce_sum.100), calls=%async_computation.2 | async-start | bytes 1310720 | tf_op jit(solution)/shard_map/all_to_all | solution.py:30
  69.1 26.4 %copy-start.4 = (bf16[512,16]{0,1:T(8,128)(2,1)S(1)}, bf16[512,16]{0,1:T(8,128)(2,1)}, u32[]{:S(2)}) copy-start(bf16[512,16]{0,1:T(8,128)(2,1)} %param.26) | copy-start | bytes 49156
  70.0 31.9 %copy-start.5 = (s32[256,2]{0,1:T(2,128)S(1)}, s32[256,2]{0,1:T(2,128)}, u32[]{:S(2)}) copy-start(s32[256,2]{0,1:T(2,128)} %param.30) | copy-start | bytes 6148
  70.0 18.5 %all-to-all-start.3 = ((bf16[64,2,512]{2,1,0:T(2,128)(2,1)}), bf16[64,2,512]{2,1,0:T(2,128)(2,1)S(1)}, u32[]{:S(2)}, u32[]{:S(2)}) async-start(bf16[64,2,512]{2,1,0:T(2,128)(2,1)} %broadcast_in_dim.19), calls=%async_computation.3 | async-start | bytes 262144 | tf_op jit(solution)/shard_map/all_to_all | solution.py:35
  77.0 41.2 %copy-start.8 = (bf16[2048]{0:T(1024)(128)(2,1)S(1)}, bf16[2048]{0:T(1024)(128)(2,1)}, u32[]{:S(2)}) copy-start(bf16[2048]{0:T(1024)(128)(2,1)} %param.27) | copy-start | bytes 12292
  88.7 33.9 %copy-start.3 = (bf16[2,2048]{1,0:T(2,128)(2,1)S(1)}, bf16[2,2048]{1,0:T(2,128)(2,1)}, u32[]{:S(2)}) copy-start(bf16[2,2048]{1,0:T(2,128)(2,1)} %param.17) | copy-start | bytes 24580
  96.4 17.0 %all-to-all-start.5 = ((bf16[128,2,16]{2,1,0:T(2,128)(2,1)}), bf16[128,2,16]{2,1,0:T(2,128)(2,1)S(1)}, u32[]{:S(2)}, u32[]{:S(2)}) async-start(bf16[128,2,16]{2,1,0:T(2,128)(2,1)} %bitcast.8), calls=%async_computation.5 | async-start | bytes 131072 | tf_op jit(solution)/shard_map/all_to_all | solution.py:136
  114.2 8.3 %all-to-all-start.6 = ((bf16[4,2,2048]{2,1,0:T(2,128)(2,1)}), bf16[4,2,2048]{2,1,0:T(2,128)(2,1)S(1)}, u32[]{:S(2)}, u32[]{:S(2)}) async-start(bf16[4,2,2048]{2,1,0:T(2,128)(2,1)} %broadcast_in_dim.21), calls=%async_computation.6 | async-start | bytes 65536 | tf_op jit(solution)/shard_map/all_to_all | solution.py:35
  123.9 20.6 %all-to-all-start.7 = ((bf16[64,2,2048]{2,1,0:T(2,128)(2,1)}), bf16[64,2,2048]{2,1,0:T(2,128)(2,1)S(1)}, u32[]{:S(2)}, u32[]{:S(2)}) async-start(bf16[64,2,2048]{2,1,0:T(2,128)(2,1)} %broadcast_in_dim.22), calls=%async_computation.7 | async-start | bytes 1048576 | tf_op jit(solution)/shard_map/all_to_all | solution.py:35
  157.8 1.6 copy-start.2
  158.2 6.6 %copy-start.11 = (bf16[2048,4]{0,1:T(4,128)(2,1)S(1)}, bf16[2048,4]{0,1:T(4,128)(2,1)}, u32[]{:S(2)}) copy-start(bf16[2048,4]{0,1:T(4,128)(2,1)} %param.28) | copy-start | bytes 49156
  161.5 7.7 %all-to-all-start.9 = ((bf16[4,16,512]{2,1,0:T(8,128)(2,1)}), bf16[4,16,512]{2,1,0:T(8,128)(2,1)S(1)}, u32[]{:S(2)}, u32[]{:S(2)}) async-start(bf16[4,16,512]{2,1,0:T(8,128)(2,1)} %bitcast.84), calls=%async_computation.9 | async-start | bytes 131072 | tf_op jit(solution)/shard_map/all_to_all | solution.py:57
  170.7 22.0 %all-to-all-start.10 = ((bf16[128,2,512]{2,1,0:T(2,128)(2,1)}), bf16[128,2,512]{2,1,0:T(2,128)(2,1)S(1)}, u32[]{:S(2)}, u32[]{:S(2)}) async-start(bf16[128,2,512]{2,1,0:T(2,128)(2,1)} %convert_element_type.120), calls=%async_computation.10 | async-start | bytes 524288 | tf_op jit(solution)/shard_map/all_to_all | solution.py:178
  193.6 7.4 %all-to-all-start.11 = ((bf16[4,2,512]{2,1,0:T(2,128)(2,1)}), bf16[4,2,512]{2,1,0:T(2,128)(2,1)S(1)}, u32[]{:S(2)}, u32[]{:S(2)}) async-start(bf16[4,2,512]{2,1,0:T(2,128)(2,1)} %broadcast_in_dim.29), calls=%async_computation.11 | async-start | bytes 16384 | tf_op jit(solution)/shard_map/all_to_all | solution.py:35
where the time goes:
time: 203 us; the launch traced here: 202 us
  waiting for transfers between devices  84.1 us (41%)
  blocking collectives  50.2 us (25%)
  starting transfers between devices  39.4 us (19%)
  local copies, waits for them, and re-layouts  12.6 us (6%)
  other arithmetic  7.32 us (4%)
  matrix products  6.88 us (3%)
    all_to_all x4, waiting for transfers between devices, from_everyone(): return lax.all_to_all(copies, axis, split_axis=0, concat_axis=0, tiled=True)  33.2 us
    all_to_all x1, blocking collectives, on_device(): lax.all_to_all(normed, EP, split_axis=1, concat_axis=0, tiled=True)  29.7 us
    all_to_all x1, waiting for transfers between devices, sum_by_axis(): return jnp.sum(lax.all_to_all(own, far, 0, 0, tiled=True), axis=0)  20.1 us
    all_to_all x4, starting transfers between devices, from_everyone(): return lax.all_to_all(copies, axis, split_axis=0, concat_axis=0, tiled=True)  19 us
    all_to_all x2, blocking collectives, from_everyone(): return lax.all_to_all(copies, axis, split_axis=0, concat_axis=0, tiled=True)  15.6 us
    all_to_all x1, waiting for transfers between devices, on_device(): lax.all_to_all(outgoing.astype(jnp.bfloat16), EP, split_axis=0, concat_ax...  15.2 us
    all_to_all x1, waiting for transfers between devices, on_device(): lax.all_to_all(partial_out, EP, split_axis=0, concat_axis=1, tiled=True)  11.5 us
    all_to_all x1, starting transfers between devices, on_device(): lax.all_to_all(outgoing.astype(jnp.bfloat16), EP, split_axis=0, concat_ax...  6.79 us
  transfers between devices with their start and end apart: 8, of which 8 were waited for; matrix products, arithmetic and copies ran while one was open for 1% of the time, Pallas kernels for 0%

commit v1 on v0

v1 whole, which is shorter than its diff:
```python
import jax
import jax.numpy as jnp
from jax import lax
from jax.sharding import Mesh
from jax.sharding import PartitionSpec as P

CAP = 16
EP = ("ep_0", "ep_1", "ep_2")
FAR = ("ep_0", "ep_1")
SLAB = ("ep_1", "ep_2")
SLAB_TP = ("ep_1", "ep_2", "tp")
CHIPS = ("ep_2", "tp")

EPSILON = 1e-06
GATE_SCALE = 16.0
F32 = jnp.float32
BF16 = jnp.bfloat16


def exchange(blocks, axes, *later):
    came = lax.all_to_all(blocks, axes, split_axis=0, concat_axis=0, tiled=True)
    return lax.optimization_barrier((came, *later)) if later else came


def to_all(shard, count):
    return jnp.broadcast_to(shard[None], (count, *shard.shape))


def rms_scale(values, gain_vec):
    floats = values.astype(F32)
    return (
        floats
        * lax.rsqrt(jnp.mean(floats * floats, axis=-1, keepdims=True) + EPSILON)
        * gain_vec.astype(F32)
    )


def on_device(
    residual_in,
    gla_state,
    norm_gain,
    w_query,
    w_key,
    w_value,
    w_decay,
    decay_bias,
    head_gain,
    w_output,
    ffn_gain,
    router_group,
    router_expert,
    expert_ids,
    w_gate,
    w_up,
    w_down,
):
    depths, rows, cores = (lax.axis_size(a) for a in EP)
    heads = lax.axis_size("tp")
    slab = rows * cores
    parts = cores * heads
    far = depths * rows
    tokens = expert_ids.shape[0]
    seqs, width = residual_in.shape
    strip = w_query.shape[0]
    key_width, value_width = w_query.shape[1], w_value.shape[1]
    in_width = 3 * key_width + value_width
    held = depths * strip
    piece = width // parts
    place = lax.axis_index(SLAB)
    chip = lax.axis_index(FAR)
    core = lax.axis_index("ep_2")

    experts = chip * cores + jnp.arange(cores, dtype=jnp.int32)
    named = jnp.any(expert_ids[None] == experts[:, None, None], axis=2)
    slot_of = jnp.cumsum(named.astype(jnp.int32), axis=1) - 1
    slots = jnp.arange(CAP, dtype=jnp.int32)
    chosen_rows = named[:, None, :] & (slot_of[:, None, :] == slots[None, :, None])
    select = chosen_rows.astype(BF16).reshape(cores * CAP, tokens)
    expert = lax.axis_index(EP)
    own_int = lax.dynamic_index_in_dim(chosen_rows, core, 0, False).astype(jnp.int32)
    slot_ids = jnp.sum(own_int[:, :, None] * expert_ids[None], axis=1)
    rival_ids = jnp.where(slot_ids[:, 0] == expert, slot_ids[:, 1], slot_ids[:, 0])
    groups = router_group.shape[1]
    lanes = jnp.arange(router_expert.shape[0], dtype=jnp.int32)
    own_group = jnp.arange(groups, dtype=jnp.int32) == expert // (router_expert.shape[0] // groups)
    own_lane = (lanes == expert).astype(F32)
    rival_lane = (lanes[None] == rival_ids[:, None]).astype(F32)
    own_group = own_group.astype(F32)
    own_gain = norm_gain.reshape(depths, slab, strip)[:, place].reshape(held).astype(F32)
    res_float = residual_in.astype(F32)
    scale = lax.rsqrt(jnp.mean(res_float * res_float, axis=-1, keepdims=True) + EPSILON)
    strips = residual_in.reshape(seqs, depths, slab, strip).transpose(2, 0, 1, 3)
    strips = strips.reshape(slab, seqs, held)

    own_w = jnp.concatenate([w_query, w_key, w_value, w_decay, w_output.T], axis=1)
    tied = lax.optimization_barrier(
        (to_all(own_w, depths), strips, select, rival_lane, own_lane, own_group, own_gain, scale)
    )
    spread, strips, select, rival_lane, own_lane, own_group, own_gain, scale = tied
    gathered = exchange(spread, "ep_0").reshape(held, in_width + value_width)
    gathered, strips = lax.optimization_barrier((gathered, strips))
    slab_res = exchange(strips, SLAB).reshape(slab * seqs, held)
    lhs = (slab_res.astype(F32) * own_gain).astype(BF16)
    sums = jnp.dot(lhs, gathered[:, :in_width], preferred_element_type=F32).astype(BF16)
    arrived, head_gain, decay_bias = exchange(
        sums.reshape(slab, seqs, in_width), SLAB, head_gain, decay_bias
    )
    projected = arrived.astype(F32).sum(axis=0) * scale

    query = projected[:, :key_width].astype(BF16).astype(F32) * key_width ** (-0.5)
    key = projected[:, key_width : 2 * key_width].astype(BF16).astype(F32)
    value = projected[:, 2 * key_width : 2 * key_width + value_width].astype(BF16).astype(F32)
    decay_pre = projected[:, 2 * key_width + value_width :]
    alpha = jnp.exp(jax.nn.log_sigmoid(decay_pre + decay_bias) / GATE_SCALE)
    new_state = alpha[:, :, None] * gla_state[:, 0] + key[:, :, None] * value[:, None, :]
    read_out = jnp.sum(query[:, :, None] * new_state, axis=1)
    gated = rms_scale(read_out, head_gain).astype(BF16)
    gated, new_state = lax.optimization_barrier((gated, new_state))

    slab_heads, slab_res = exchange(to_all(gated, slab), SLAB, slab_res)
    slab_heads = slab_heads.reshape(slab * seqs, value_width)
    head_part = lax.dot_general(
        slab_heads,
        gathered[:, in_width:],
        (((1,), (1,)), ((), ())),
        preferred_element_type=F32,
    ).astype(BF16)

    def by_owner(columns):
        return columns.reshape(rows, cores * seqs, parts, strip)

    both = jnp.concatenate([by_owner(head_part), by_owner(slab_res)], axis=3)
    both = both.transpose(0, 2, 1, 3).reshape(rows * parts, cores * seqs, 2 * strip)
    came = exchange(both, SLAB_TP).reshape(slab, heads, cores * seqs, 2 * strip)
    attention = came[..., :strip].astype(F32).sum(axis=1)
    came_res = came[:, 0, :, strip:].astype(F32)
    hidden = (came_res + attention).astype(BF16)
    hidden = hidden.transpose(1, 0, 2).reshape(cores * seqs, piece)

    all_hidden = exchange(to_all(hidden, far), FAR).reshape(tokens, piece)
    slot_part = jnp.dot(select, all_hidden, preferred_element_type=F32).astype(BF16)
    outward = jnp.broadcast_to(
        slot_part.reshape(cores, 1, CAP, piece), (cores, heads, CAP, piece)
    ).reshape(parts, CAP, piece)
    slot_hidden, ffn_gain, router_group, router_expert = exchange(
        outward, CHIPS, ffn_gain, router_group, router_expert
    )
    slot_hidden = slot_hidden.transpose(1, 0, 2).reshape(CAP, width)
    slot_rows = rms_scale(slot_hidden, ffn_gain).astype(BF16)

    group_logits = jnp.dot(slot_rows, router_group, preferred_element_type=F32)
    group_logit = jnp.sum(group_logits * own_group[None], axis=1)
    group_share = 1.0 / jnp.sum(jnp.exp(group_logits - group_logit[:, None]), axis=1)
    expert_logits = lax.dot_general(
        slot_rows, router_expert, (((1,), (1,)), ((), ())), preferred_element_type=F32
    )
    chosen = jnp.sum(expert_logits * own_lane[None], axis=1)
    rival = jnp.sum(expert_logits * rival_lane, axis=1)
    slot_weight = group_share * jax.nn.sigmoid(chosen - rival)

    gate_out = jnp.dot(slot_rows, w_gate[0], preferred_element_type=F32)
    up_out = jnp.dot(slot_rows, w_up[0], preferred_element_type=F32)
    units = (jax.nn.silu(gate_out) * up_out).astype(BF16)
    output = jnp.dot(units, w_down[0], preferred_element_type=F32) * slot_weight[:, None]
    back = output.astype(BF16).reshape(CAP, parts, piece).transpose(1, 0, 2)
    summed = exchange(back, CHIPS).reshape(cores, heads, CAP, piece).astype(F32).sum(axis=1)
    dense = lax.dot_general(
        select,
        summed.astype(BF16).reshape(cores * CAP, piece),
        (((0,), (0,)), ((), ())),
        preferred_element_type=F32,
    ).astype(BF16)
    moe, hidden = exchange(dense.reshape(far, cores * seqs, piece), FAR, hidden)
    moe = moe.astype(F32).sum(axis=0)
    layer = (hidden.astype(F32) + moe).astype(BF16)
    last = jnp.broadcast_to(
        layer.reshape(cores, 1, seqs, piece), (cores, heads, seqs, piece)
    ).reshape(parts, seqs, piece)
    layer_out = exchange(last, CHIPS).transpose(1, 0, 2).reshape(seqs, width)
    return (layer_out, new_state[:, None])


def solution(mesh):
    torus = Mesh(mesh.devices.reshape(8, 8, 2, mesh.shape["tp"]), (*EP, "tp"))
    in_specs = (
        P(EP, None),
        P(EP, "tp", None, None),
        P(),
        P(EP, "tp"),
        P(EP, "tp"),
        P(EP, "tp"),
        P(EP, "tp"),
        P("tp"),
        P(),
        P("tp", EP),
        P(),
        P(),
        P(),
        P(),
        P(EP, None, "tp"),
        P(EP, None, "tp"),
        P(EP, "tp", None),
    )
    out_specs = (P(EP, None), P(EP, "tp", None, None))
    return jax.shard_map(
        on_device, mesh=torus, in_specs=in_specs, out_specs=out_specs, check_vma=False
    )
```

time: 203 us -> 152 us (0.75)
  blocking collectives: 50.2 us -> 135 us
  waiting for transfers between devices: 84.1 us -> 0 us
  starting transfers between devices: 39.4 us -> 0 us
  matrix products: 6.88 us -> 1.79 us
  other arithmetic: 7.32 us -> 3.56 us
  local copies, waits for them, and re-layouts: 12.6 us -> 9.35 us
    all_to_all x4 -> x10, blocking collectives: 50.2 us -> 135 us  [exchange(): came = lax.all_to_all(blocks, axes, split_axis=0, concat_axis=0, tiled=True)]
    all_to_all x8 -> x0, waiting for transfers between devices: 84.1 us -> none  [the longest x4 33.2 us: from_everyone(): return lax.all_to_all(copies, axis, split_axis=0, concat_axis=0, tiled=True)]
    all_to_all x8 -> x0, starting transfers between devices: 39.4 us -> none  [the longest x4 19 us: from_everyone(): return lax.all_to_all(copies, axis, split_axis=0, concat_axis=0, tiled=True)]
    unnamed x25 -> x40, local copies, waits for them, and re-layouts: 0.66 us -> 7.85 us
    dot_general x12 -> x8, matrix products: 6.88 us -> 1.79 us  [the longest x1 0.39 us: on_device(): lax.dot_general(slot_rows, router_expert, (((1,), (1,)), ((), ())), prefe...]
    broadcast_in_dim x6 -> x7, local copies, waits for them, and re-layouts: 3.74 us -> 0.23 us  [the longest x4 0.19 us: to_all(): return jnp.broadcast_to(shard[None], (count, *shard.shape))]
    another operation x5 -> x0, local copies, waits for them, and re-layouts: 2.57 us -> none  [the longest x2 1.57 us: in_order(): return jnp.moveaxis(blocks, 0, dim).reshape(shape)]
    transpose x2 -> x1, local copies, waits for them, and re-layouts: 2.38 us -> 0.01 us  [on_device(): hidden = hidden.transpose(1, 0, 2).reshape(cores * seqs, piece)]
  transfers between devices with their start and end apart: 8 -> 0, of which waited for: 8 -> 0; matrix products, arithmetic and copies ran while one was open for 1% -> 0% of each run, Pallas kernels for 0% -> 0%
where the time goes in v1:
time: 152 us; the launch traced here: 151 us
  blocking collectives  135 us (89%)
  local copies, waits for them, and re-layouts  9.35 us (6%)
  other arithmetic  3.56 us (2%)
  matrix products  1.79 us (1%)
    all_to_all x10, blocking collectives, exchange(): came = lax.all_to_all(blocks, axes, split_axis=0, concat_axis=0, tiled=True)  135 us
    unnamed x40, local copies, waits for them, and re-layouts  7.85 us

profile of v1, /device:TPU:1, one launch (start us, length us, event | category | flops | bytes accessed | tf_op | source)
XLA Modules:
  0.0 151.0 jit_solution(12794213691424385760)
XLA Ops:
  0.7 0.7 copy-done.5
  1.7 0.6 copy-done.10
  2.6 0.6 reduce-window.6
  3.2 0.2 slice_reduce_fusion
  3.4 0.2 reduce-window.9
  4.0 0.6 copy-done.14
  4.8 0.6 copy-done.11
  5.5 0.6 copy-done.12
  6.1 0.7 copy-done.8
  6.8 0.7 copy-done.13
  7.5 0.7 copy-done.9
  8.3 25.6 %all_to_all.50 = bf16[8,16,1792]{2,1,0:T(8,128)(2,1)S(1)} all-to-all(bf16[8,16,1792]{2,1,0:T(8,128)(2,1)S(1)} %broadcast_in_dim.18), channel_id=1, replica_groups=mesh['ep_0'=8,'ep_1'=8,'ep_2'=2,'tp'=4] {'ep_0'}, dimensions={0} | all-to-all | bytes 917504 | tf_op jit(solution)/shard_map/all_to_all | solution.py:21
  33.9 16.2 %all_to_all.51 = bf16[16,2,128]{2,1,0:T(2,128)(2,1)S(1)} all-to-all(bf16[16,2,128]{2,1,0:T(2,128)(2,1)S(1)} %copy.101), channel_id=1, replica_groups=mesh['ep_0'=8,'ep_1'=8,'ep_2'=2,'tp'=4] {'ep_1','ep_2'}, dimensions={0} | all-to-all | bytes 16384 | tf_op jit(solution)/shard_map/all_to_all | solution.py:21
  50.1 0.2 convolution_convert_fusion
  50.3 11.2 %all_to_all.52 = bf16[16,2,1280]{2,1,0:T(2,128)(2,1)S(1)} all-to-all(bf16[16,2,1280]{2,1,0:T(2,128)(2,1)S(1)} %reshape.204), channel_id=1, replica_groups=mesh['ep_0'=8,'ep_1'=8,'ep_2'=2,'tp'=4] {'ep_1','ep_2'}, dimensions={0} | all-to-all | bytes 163840 | tf_op jit(solution)/shard_map/all_to_all | solution.py:21
  61.7 0.7 copy-done.15
  62.4 0.7 copy-done.16
  63.1 1.2 multiply_reduce_fusion
  64.6 9.9 %all_to_all.53 = bf16[16,2,512]{2,1,0:T(2,128)(2,1)S(1)} all-to-all(bf16[16,2,512]{2,1,0:T(2,128)(2,1)S(1)} %broadcast_in_dim.19), channel_id=1, replica_groups=mesh['ep_0'=8,'ep_1'=8,'ep_2'=2,'tp'=4] {'ep_1','ep_2'}, dimensions={0} | all-to-all | bytes 65536 | tf_op jit(solution)/shard_map/all_to_all | solution.py:21
  75.0 14.5 %all_to_all.54 = bf16[64,4,32]{2,1,0:T(4,128)(2,1)S(1)} all-to-all(bf16[64,4,32]{2,1,0:T(4,128)(2,1)S(1)} %copy.103), channel_id=1, replica_groups=mesh['ep_0'=8,'ep_1'=8,'ep_2'=2,'tp'=4] {'ep_1','ep_2','tp'}, dimensions={0} | all-to-all | bytes 32768 | tf_op jit(solution)/shard_map/all_to_all | solution.py:21
  89.9 15.3 %all_to_all.55 = bf16[64,4,256]{2,1,0:T(4,128)(2,1)S(1)} all-to-all(bf16[64,4,256]{2,1,0:T(4,128)(2,1)S(1)} %broadcast_in_dim.21), channel_id=1, replica_groups=mesh['ep_0'=8,'ep_1'=8,'ep_2'=2,'tp'=4] {'ep_0','ep_1'}, dimensions={0} | all-to-all | bytes 262144 | tf_op jit(solution)/shard_map/all_to_all | solution.py:21
  105.4 10.0 %all_to_all.56 = bf16[8,16,256]{2,1,0:T(8,128)(2,1)S(1)} all-to-all(bf16[8,16,256]{2,1,0:T(8,128)(2,1)S(1)} %bitcast.105), channel_id=1, replica_groups=mesh['ep_0'=8,'ep_1'=8,'ep_2'=2,'tp'=4] {'ep_2','tp'}, dimensions={0} | all-to-all | bytes 131072 | tf_op jit(solution)/shard_map/all_to_all | solution.py:21
  115.7 0.2 fusion.6
  115.9 0.6 copy-done.6
  116.5 0.2 multiply_reduce_fusion.6
  116.7 0.4 multiply_reduce_fusion.3
  117.2 0.3 fusion
  117.5 7.9 %all_to_all.57 = bf16[8,16,256]{2,1,0:T(8,128)(2,1)S(1)} all-to-all(bf16[8,16,256]{2,1,0:T(8,128)(2,1)S(1)} %bitcast.107), channel_id=1, replica_groups=mesh['ep_0'=8,'ep_1'=8,'ep_2'=2,'tp'=4] {'ep_2','tp'}, dimensions={0} | all-to-all | bytes 131072 | tf_op jit(solution)/shard_map/all_to_all | solution.py:21
  125.4 0.2 convolution_convert_fusion.1
  125.6 15.4 %all_to_all.58 = bf16[64,4,256]{2,1,0:T(4,128)(2,1)S(1)} all-to-all(bf16[64,4,256]{2,1,0:T(4,128)(2,1)S(1)} %reshape.215), channel_id=1, replica_groups=mesh['ep_0'=8,'ep_1'=8,'ep_2'=2,'tp'=4] {'ep_0','ep_1'}, dimensions={0} | all-to-all | bytes 262144 | tf_op jit(solution)/shard_map/all_to_all | solution.py:21
  141.2 9.2 %all_to_all.59 = bf16[8,2,256]{2,1,0:T(2,128)(2,1)S(1)} all-to-all(bf16[8,2,256]{2,1,0:T(2,128)(2,1)S(1)} %bitcast.112), channel_id=1, replica_groups=mesh['ep_0'=8,'ep_1'=8,'ep_2'=2,'tp'=4] {'ep_2','tp'}, dimensions={0} | all-to-all | bytes 16384 | tf_op jit(solution)/shard_map/all_to_all | solution.py:21
  150.4 0.6 copy.143
  (99 shorter events, 3.2 us)
Async XLA Ops:
  0.6 116.5 %copy-start = (bf16[1,128,2048]{2,1,0:T(8,128)(2,1)S(1)}, bf16[1,128,2048]{2,1,0:T(8,128)(2,1)}, u32[]{:S(2)}) copy-start(bf16[1,128,2048]{2,1,0:T(8,128)(2,1)} %param.33) | copy-start | bytes 1572868
  0.7 0.8 copy-start.5
  1.7 0.7 copy-start.10
  3.9 0.7 copy-start.14
  4.7 0.7 copy-start.11
  5.4 0.7 copy-start.12
  6.1 0.7 copy-start.8
  6.8 0.7 copy-start.13
  7.5 0.7 copy-start.9
  8.3 54.8 %copy-start.1 = (f32[2,1,256,512]{3,2,1,0:T(8,128)S(1)}, f32[2,1,256,512]{3,2,1,0:T(8,128)}, u32[]{:S(2)}) copy-start(f32[2,1,256,512]{3,2,1,0:T(8,128)} %param.18) | copy-start | bytes 3145732
  61.7 0.7 copy-start.15
  62.4 0.7 copy-start.16
  105.2 10.1 %copy-start.7 = (bf16[2048]{0:T(1024)(128)(2,1)S(1)}, bf16[2048]{0:T(1024)(128)(2,1)}, u32[]{:S(2)}) copy-start(bf16[2048]{0:T(1024)(128)(2,1)} %param.27) | copy-start | bytes 12292
  105.4 10.3 %copy-start.2 = (bf16[1,2048,128]{2,1,0:T(8,128)(2,1)S(1)}, bf16[1,2048,128]{2,1,0:T(8,128)(2,1)}, u32[]{:S(2)}) copy-start(bf16[1,2048,128]{2,1,0:T(8,128)(2,1)} %param.31) | copy-start | bytes 1572868
  115.7 1.1 copy-start.3
  115.7 0.8 copy-start.6
  115.9 1.3 copy-start.4

commit v2 on v1

--- a/solution.py
+++ b/solution.py
@@ -1,6 +1,10 @@
+import functools
+
 import jax
 import jax.numpy as jnp
 from jax import lax
+from jax.experimental import pallas as pl
+from jax.experimental.pallas import tpu as pltpu
 from jax.sharding import Mesh
 from jax.sharding import PartitionSpec as P
 
@@ -33,6 +37,51 @@
         * lax.rsqrt(jnp.mean(floats * floats, axis=-1, keepdims=True) + EPSILON)
         * gain_vec.astype(F32)
     )
+
+
+def prepare(experts_of, *refs):
+    sources, (spread, select, rival, *kept), (ids, sems) = refs[:12], refs[12:-2], refs[-2:]
+    *weights, ids_in = sources[:6]
+    width = 0
+    copies = []
+    for source in weights:
+        place = spread.at[0, :, pl.ds(width, source.shape[1])]
+        width += source.shape[1]
+        copies.append(pltpu.make_async_copy(source, place, sems.at[len(copies)]))
+    copies.append(pltpu.make_async_copy(ids_in, ids, sems.at[len(copies)]))
+    for source, target in zip(sources[6:], kept, strict=True):
+        copies.append(pltpu.make_async_copy(source, target, sems.at[len(copies)]))
+    for copy in copies:
+        copy.start()
+    first, core = experts_of()
+    count = ids.shape[1]
+    row = lax.broadcasted_iota(jnp.int32, (count, count), 0)
+    col = lax.broadcasted_iota(jnp.int32, (count, count), 1)
+    upper = jnp.where(row <= col, 1.0, 0.0).astype(BF16)
+    copies[5].wait()
+    one, two = ids[0:1, :], ids[1:2, :]
+    experts = first + lax.broadcasted_iota(jnp.int32, (8, count), 0)
+    named = (one == experts) | (two == experts)
+    marks = jnp.where(named, 1.0, 0.0)
+    ends = jnp.dot(marks.astype(BF16), upper, preferred_element_type=F32)
+    slots = lax.broadcasted_iota(jnp.int32, (CAP, count), 0).astype(F32) + 1.0
+    both = (one + two).astype(F32)
+    own = first + core
+    others = jnp.zeros((CAP, 1), F32)
+    for c in range(select.shape[0] // CAP):
+        mine = jnp.where(ends[c : c + 1] == slots, marks[c : c + 1], 0.0)
+        select[CAP * c : CAP * (c + 1)] = mine.astype(BF16)
+        total = jnp.sum(mine * both, axis=1, keepdims=True)
+        others = jnp.where(core == c, total, others)
+    lanes = lax.broadcasted_iota(jnp.int32, rival.shape, 1)
+    rival[...] = jnp.where(lanes == others.astype(jnp.int32) - own, 1.0, 0.0)
+    for copy in copies[:5]:
+        copy.wait()
+    own_w = spread[0]
+    for depth in range(1, spread.shape[0]):
+        spread[depth] = own_w
+    for copy in copies[6:]:
+        copy.wait()
 
 
 def on_device(
@@ -70,21 +119,35 @@
     chip = lax.axis_index(FAR)
     core = lax.axis_index("ep_2")
 
-    experts = chip * cores + jnp.arange(cores, dtype=jnp.int32)
-    named = jnp.any(expert_ids[None] == experts[:, None, None], axis=2)
-    slot_of = jnp.cumsum(named.astype(jnp.int32), axis=1) - 1
-    slots = jnp.arange(CAP, dtype=jnp.int32)
-    chosen_rows = named[:, None, :] & (slot_of[:, None, :] == slots[None, :, None])
-    select = chosen_rows.astype(BF16).reshape(cores * CAP, tokens)
+    n_experts = router_expert.shape[0]
+
+    def experts_of():
+        return lax.axis_index(FAR) * cores, lax.axis_index("ep_2")
+
+    vmem = pl.BlockSpec(memory_space=pltpu.VMEM)
+    later = (residual_in, norm_gain, head_gain, ffn_gain, decay_bias, router_group.T)
+    shapes = [
+        pltpu.VMEM((depths, strip, in_width + value_width), BF16),
+        pltpu.VMEM((cores * CAP, tokens), BF16),
+        pltpu.VMEM((CAP, n_experts), F32),
+        *(pltpu.VMEM(a.shape, a.dtype) for a in later),
+    ]
+    spread, select, rival_lane, *later = pl.pallas_call(
+        functools.partial(prepare, experts_of),
+        out_shape=shapes,
+        in_specs=[pl.BlockSpec(memory_space=pl.ANY)] * 12,
+        out_specs=[vmem] * len(shapes),
+        scratch_shapes=[
+            pltpu.VMEM((expert_ids.shape[1], tokens), jnp.int32),
+            pltpu.SemaphoreType.DMA((12,)),
+        ],
+    )(w_query, w_key, w_value, w_decay, w_output.T, expert_ids.T, *later)
+    residual_in, norm_gain, head_gain, ffn_gain, decay_bias, group_rows = later
     expert = lax.axis_index(EP)
-    own_int = lax.dynamic_index_in_dim(chosen_rows, core, 0, False).astype(jnp.int32)
-    slot_ids = jnp.sum(own_int[:, :, None] * expert_ids[None], axis=1)
-    rival_ids = jnp.where(slot_ids[:, 0] == expert, slot_ids[:, 1], slot_ids[:, 0])
     groups = router_group.shape[1]
-    lanes = jnp.arange(router_expert.shape[0], dtype=jnp.int32)
-    own_group = jnp.arange(groups, dtype=jnp.int32) == expert // (router_expert.shape[0] // groups)
+    lanes = jnp.arange(n_experts, dtype=jnp.int32)
+    own_group = jnp.arange(groups, dtype=jnp.int32) == expert // (n_experts // groups)
     own_lane = (lanes == expert).astype(F32)
-    rival_lane = (lanes[None] == rival_ids[:, None]).astype(F32)
     own_group = own_group.astype(F32)
     own_gain = norm_gain.reshape(depths, slab, strip)[:, place].reshape(held).astype(F32)
     res_float = residual_in.astype(F32)
@@ -92,9 +155,8 @@
     strips = residual_in.reshape(seqs, depths, slab, strip).transpose(2, 0, 1, 3)
     strips = strips.reshape(slab, seqs, held)
 
-    own_w = jnp.concatenate([w_query, w_key, w_value, w_decay, w_output.T], axis=1)
     tied = lax.optimization_barrier(
-        (to_all(own_w, depths), strips, select, rival_lane, own_lane, own_group, own_gain, scale)
+        (spread, strips, select, rival_lane, own_lane, own_group, own_gain, scale)
     )
     spread, strips, select, rival_lane, own_lane, own_group, own_gain, scale = tied
     gathered = exchange(spread, "ep_0").reshape(held, in_width + value_width)
@@ -142,13 +204,13 @@
     outward = jnp.broadcast_to(
         slot_part.reshape(cores, 1, CAP, piece), (cores, heads, CAP, piece)
     ).reshape(parts, CAP, piece)
-    slot_hidden, ffn_gain, router_group, router_expert = exchange(
-        outward, CHIPS, ffn_gain, router_group, router_expert
-    )
+    slot_hidden, ffn_gain = exchange(outward, CHIPS, ffn_gain)
     slot_hidden = slot_hidden.transpose(1, 0, 2).reshape(CAP, width)
     slot_rows = rms_scale(slot_hidden, ffn_gain).astype(BF16)
 
-    group_logits = jnp.dot(slot_rows, router_group, preferred_element_type=F32)
+    group_logits = lax.dot_general(
+        slot_rows, group_rows, (((1,), (1,)), ((), ())), preferred_element_type=F32
+    )
     group_logit = jnp.sum(group_logits * own_group[None], axis=1)
     group_share = 1.0 / jnp.sum(jnp.exp(group_logits - group_logit[:, None]), axis=1)
     expert_logits = lax.dot_general(

time: 152 us -> 144 us (0.947)
  local copies, waits for them, and re-layouts: 9.35 us -> 2.35 us
    unnamed x40 -> x11, local copies, waits for them, and re-layouts: 7.85 us -> 1.2 us
where the time goes in v2:
time: 144 us
  blocking collectives  135 us (94%)
  local copies, waits for them, and re-layouts  2.35 us (2%)
  other arithmetic  2.32 us (2%)
  matrix products  1.79 us (1%)
    all_to_all x10, blocking collectives, exchange(): came = lax.all_to_all(blocks, axes, split_axis=0, concat_axis=0, tiled=True)  135 us

profile of v2, /device:TPU:1, one launch (start us, length us, event | category | flops | bytes accessed | tf_op | source)
XLA Modules:
  0.0 143.8 jit_solution(17754441554516390094)
XLA Ops:
  0.7 1.2 shard_map.176
  1.9 0.1 multiply_reduce_fusion.1
  2.0 0.1 reshape.157
  2.4 0.1 reshape.158
  2.5 25.6 %all_to_all.50 = bf16[8,16,1792]{2,1,0:T(8,128)(2,1)S(1)} all-to-all(bf16[8,16,1792]{2,1,0:T(8,128)(2,1)S(1)} %get-tuple-element.38), channel_id=1, replica_groups=mesh['ep_0'=8,'ep_1'=8,'ep_2'=2,'tp'=4] {'ep_0'}, dimensions={0} | all-to-all | bytes 917504 | tf_op jit(solution)/shard_map/all_to_all | solution.py:25
  28.1 16.2 %all_to_all.51 = bf16[16,2,128]{2,1,0:T(2,128)(2,1)S(1)} all-to-all(bf16[16,2,128]{2,1,0:T(2,128)(2,1)S(1)} %copy.87), channel_id=1, replica_groups=mesh['ep_0'=8,'ep_1'=8,'ep_2'=2,'tp'=4] {'ep_1','ep_2'}, dimensions={0} | all-to-all | bytes 16384 | tf_op jit(solution)/shard_map/all_to_all | solution.py:25
  44.3 0.2 convolution_convert_fusion
  44.5 11.2 %all_to_all.52 = bf16[16,2,1280]{2,1,0:T(2,128)(2,1)S(1)} all-to-all(bf16[16,2,1280]{2,1,0:T(2,128)(2,1)S(1)} %reshape.162), channel_id=1, replica_groups=mesh['ep_0'=8,'ep_1'=8,'ep_2'=2,'tp'=4] {'ep_1','ep_2'}, dimensions={0} | all-to-all | bytes 163840 | tf_op jit(solution)/shard_map/all_to_all | solution.py:25
  55.9 1.2 multiply_reduce_fusion
  57.2 0.1 multiply_reduce_fusion.4
  57.4 9.9 %all_to_all.53 = bf16[16,2,512]{2,1,0:T(2,128)(2,1)S(1)} all-to-all(bf16[16,2,512]{2,1,0:T(2,128)(2,1)S(1)} %broadcast_in_dim.16), channel_id=1, replica_groups=mesh['ep_0'=8,'ep_1'=8,'ep_2'=2,'tp'=4] {'ep_1','ep_2'}, dimensions={0} | all-to-all | bytes 65536 | tf_op jit(solution)/shard_map/all_to_all | solution.py:25
  67.4 0.1 convolution_convert_fusion.3
  67.5 0.1 reshape.164
  67.6 0.1 reshape.165
  67.7 0.1 copy_bitcast_fusion
  67.9 14.5 %all_to_all.54 = bf16[64,4,32]{2,1,0:T(4,128)(2,1)S(1)} all-to-all(bf16[64,4,32]{2,1,0:T(4,128)(2,1)S(1)} %copy.89), channel_id=1, replica_groups=mesh['ep_0'=8,'ep_1'=8,'ep_2'=2,'tp'=4] {'ep_1','ep_2','tp'}, dimensions={0} | all-to-all | bytes 32768 | tf_op jit(solution)/shard_map/all_to_all | solution.py:25
  82.4 0.1 slice.39
  82.6 0.1 broadcast_in_dim.17
  82.7 15.3 %all_to_all.55 = bf16[64,4,256]{2,1,0:T(4,128)(2,1)S(1)} all-to-all(bf16[64,4,256]{2,1,0:T(4,128)(2,1)S(1)} %broadcast_in_dim.18), channel_id=1, replica_groups=mesh['ep_0'=8,'ep_1'=8,'ep_2'=2,'tp'=4] {'ep_0','ep_1'}, dimensions={0} | all-to-all | bytes 262144 | tf_op jit(solution)/shard_map/all_to_all | solution.py:25
  98.1 0.1 convolution_convert_fusion.2
  98.3 10.0 %all_to_all.56 = bf16[8,16,256]{2,1,0:T(8,128)(2,1)S(1)} all-to-all(bf16[8,16,256]{2,1,0:T(8,128)(2,1)S(1)} %bitcast.88), channel_id=1, replica_groups=mesh['ep_0'=8,'ep_1'=8,'ep_2'=2,'tp'=4] {'ep_2','tp'}, dimensions={0} | all-to-all | bytes 131072 | tf_op jit(solution)/shard_map/all_to_all | solution.py:25
  108.2 0.1 fusion.9
  108.5 0.2 fusion.6
  108.7 0.2 multiply_reduce_fusion.5
  109.0 0.6 copy-done.3
  109.5 0.4 multiply_reduce_fusion.2
  110.0 0.3 fusion
  110.3 7.9 %all_to_all.57 = bf16[8,16,256]{2,1,0:T(8,128)(2,1)S(1)} all-to-all(bf16[8,16,256]{2,1,0:T(8,128)(2,1)S(1)} %bitcast.90), channel_id=1, replica_groups=mesh['ep_0'=8,'ep_1'=8,'ep_2'=2,'tp'=4] {'ep_2','tp'}, dimensions={0} | all-to-all | bytes 131072 | tf_op jit(solution)/shard_map/all_to_all | solution.py:25
  118.2 0.2 convolution_convert_fusion.1
  118.5 15.4 %all_to_all.58 = bf16[64,4,256]{2,1,0:T(4,128)(2,1)S(1)} all-to-all(bf16[64,4,256]{2,1,0:T(4,128)(2,1)S(1)} %reshape.173), channel_id=1, replica_groups=mesh['ep_0'=8,'ep_1'=8,'ep_2'=2,'tp'=4] {'ep_0','ep_1'}, dimensions={0} | all-to-all | bytes 262144 | tf_op jit(solution)/shard_map/all_to_all | solution.py:25
  134.0 9.2 %all_to_all.59 = bf16[8,2,256]{2,1,0:T(2,128)(2,1)S(1)} all-to-all(bf16[8,2,256]{2,1,0:T(2,128)(2,1)S(1)} %bitcast.95), channel_id=1, replica_groups=mesh['ep_0'=8,'ep_1'=8,'ep_2'=2,'tp'=4] {'ep_2','tp'}, dimensions={0} | all-to-all | bytes 16384 | tf_op jit(solution)/shard_map/all_to_all | solution.py:25
  143.2 0.6 copy.122
  (52 shorter events, 1.2 us)
Async XLA Ops:
  0.6 109.3 %copy-start = (bf16[1,128,2048]{2,1,0:T(8,128)(2,1)S(1)}, bf16[1,128,2048]{2,1,0:T(8,128)(2,1)}, u32[]{:S(2)}) copy-start(bf16[1,128,2048]{2,1,0:T(8,128)(2,1)} %param.33) | copy-start | bytes 1572868
  2.2 53.7 %copy-start.1 = (f32[2,1,256,512]{3,2,1,0:T(8,128)S(1)}, f32[2,1,256,512]{3,2,1,0:T(8,128)}, u32[]{:S(2)}) copy-start(f32[2,1,256,512]{3,2,1,0:T(8,128)} %param.18) | copy-start | bytes 3145732
  98.2 10.3 %copy-start.2 = (bf16[1,2048,128]{2,1,0:T(8,128)(2,1)S(1)}, bf16[1,2048,128]{2,1,0:T(8,128)(2,1)}, u32[]{:S(2)}) copy-start(bf16[1,2048,128]{2,1,0:T(8,128)(2,1)} %param.31) | copy-start | bytes 1572868
  108.5 1.0 copy-start.3
  108.7 1.2 copy-start.4

commit v3 on v2

--- a/solution.py
+++ b/solution.py
@@ -26,6 +26,10 @@
     return lax.optimization_barrier((came, *later)) if later else came
 
 
+def on_chip(array):
+    return pltpu.with_memory_space_constraint(array, pltpu.VMEM)
+
+
 def to_all(shard, count):
     return jnp.broadcast_to(shard[None], (count, *shard.shape))
 
@@ -40,7 +44,7 @@
 
 
 def prepare(experts_of, *refs):
-    sources, (spread, select, rival, *kept), (ids, sems) = refs[:12], refs[12:-2], refs[-2:]
+    sources, (spread, along, select, rival, *kept), (ids, sems) = refs[:13], refs[13:-2], refs[-2:]
     *weights, ids_in = sources[:6]
     width = 0
     copies = []
@@ -53,14 +57,16 @@
         copies.append(pltpu.make_async_copy(source, target, sems.at[len(copies)]))
     for copy in copies:
         copy.start()
-    first, core = experts_of()
+    first, core, place, slab = experts_of()
     count = ids.shape[1]
     row = lax.broadcasted_iota(jnp.int32, (count, count), 0)
     col = lax.broadcasted_iota(jnp.int32, (count, count), 1)
     upper = jnp.where(row <= col, 1.0, 0.0).astype(BF16)
     copies[5].wait()
     one, two = ids[0:1, :], ids[1:2, :]
-    experts = first + lax.broadcasted_iota(jnp.int32, (8, count), 0)
+    depths = spread.shape[0]
+    index = lax.broadcasted_iota(jnp.int32, (2 * depths, count), 0)
+    experts = jnp.where(index < depths, index * slab + place, index - depths + first)
     named = (one == experts) | (two == experts)
     marks = jnp.where(named, 1.0, 0.0)
     ends = jnp.dot(marks.astype(BF16), upper, preferred_element_type=F32)
@@ -68,8 +74,15 @@
     both = (one + two).astype(F32)
     own = first + core
     others = jnp.zeros((CAP, 1), F32)
+
+
+    def slots_of(at):
+        return jnp.where(ends[at : at + 1] == slots, marks[at : at + 1], 0.0)
+
+    for depth in range(depths):
+        along[CAP * depth : CAP * (depth + 1)] = slots_of(depth).astype(BF16)
     for c in range(select.shape[0] // CAP):
-        mine = jnp.where(ends[c : c + 1] == slots, marks[c : c + 1], 0.0)
+        mine = slots_of(depths + c)
         select[CAP * c : CAP * (c + 1)] = mine.astype(BF16)
         total = jnp.sum(mine * both, axis=1, keepdims=True)
         others = jnp.where(core == c, total, others)
@@ -82,6 +95,68 @@
         spread[depth] = own_w
     for copy in copies[6:]:
         copy.wait()
+
+
+def pack(heads_ref, held_ref, res_ref, out_ref):
+    value_width = heads_ref.shape[1]
+    part = lax.dot_general(
+        heads_ref[...],
+        held_ref[:, held_ref.shape[1] - value_width :],
+        (((1,), (1,)), ((), ())),
+        preferred_element_type=F32,
+    )
+    with_res = (lax.axis_index("tp") == 0).astype(F32)
+    part = part + res_ref[...].astype(F32) * with_res
+    lines, lanes = out_ref.shape[1:]
+    count = part.shape[0] // lines
+    size = lanes // count
+    group = lax.broadcasted_iota(jnp.int32, (lines, lanes), 1) // size
+    for quarter in range(count):
+        block = jnp.zeros((lines, lanes), F32)
+        for k in range(count):
+            rows = part[lines * k : lines * (k + 1)]
+            moved = pltpu.roll(rows, (size * (k - quarter)) % lanes, 1)
+            block = jnp.where(group == k, moved, block)
+        block = block.astype(BF16)
+        for at in range(out_ref.shape[0] // count):
+            out_ref[count * at + quarter] = block
+
+
+def dispatch(at_place, came_ref, along_ref, out_ref, hidden_ref, rows_ref, all_ref):
+    depth, row, core = at_place()
+    count, lines, lanes = came_ref.shape
+    heads = lanes // (2 * 16)
+    all_ref[...] = jnp.zeros_like(all_ref)
+    hidden = []
+    for at in range(count // heads):
+        total = came_ref[heads * at].astype(F32)
+        for head in range(1, heads):
+            total = total + came_ref[heads * at + head].astype(F32)
+        hidden.append(total.astype(BF16).astype(F32))
+    group = lax.broadcasted_iota(jnp.int32, (lines, lanes), 1) // 16
+    for k in range(heads):
+        for strip in range(2):
+            for half in range(2):
+                block = jnp.zeros((lines, lanes), F32)
+                for m in range(8):
+                    shift = (16 * m - 32 * k - 16 * strip) % lanes
+                    moved = pltpu.roll(hidden[8 * half + m], shift, 1)
+                    block = jnp.where(group == m, moved, block)
+                at = 256 * strip + 128 * half
+                rows_ref[lines * k : lines * (k + 1), at : at + lanes] = block
+    rows = rows_ref[...].astype(BF16)
+    size = rows.shape[0]
+    all_ref[pl.ds(pl.multiple_of(depth * size, size), size)] = rows
+    slots = jnp.dot(along_ref[...], all_ref[...], preferred_element_type=F32).astype(BF16)
+    for at in range(out_ref.shape[0]):
+        out_ref[at] = slots[CAP * at : CAP * (at + 1)]
+    own, piece = hidden_ref.shape
+    here = lax.broadcasted_iota(jnp.int32, (8, size), 0)
+    there = lax.broadcasted_iota(jnp.int32, (8, size), 1)
+    pick = jnp.where(there == here + own * row, 1.0, 0.0).astype(BF16)
+    mine = jnp.dot(pick, rows, preferred_element_type=F32)
+    mine = jnp.where(core == 0, mine[:, :piece], mine[:, piece:])
+    hidden_ref[...] = mine[:own].astype(BF16)
 
 
 def on_device(
@@ -122,27 +197,30 @@
     n_experts = router_expert.shape[0]
 
     def experts_of():
-        return lax.axis_index(FAR) * cores, lax.axis_index("ep_2")
+        core = lax.axis_index("ep_2")
+        return lax.axis_index(FAR) * cores, core, lax.axis_index(SLAB), slab
 
     vmem = pl.BlockSpec(memory_space=pltpu.VMEM)
     later = (residual_in, norm_gain, head_gain, ffn_gain, decay_bias, router_group.T)
+    later += (router_expert,)
     shapes = [
         pltpu.VMEM((depths, strip, in_width + value_width), BF16),
+        pltpu.VMEM((depths * CAP, tokens), BF16),
         pltpu.VMEM((cores * CAP, tokens), BF16),
         pltpu.VMEM((CAP, n_experts), F32),
         *(pltpu.VMEM(a.shape, a.dtype) for a in later),
     ]
-    spread, select, rival_lane, *later = pl.pallas_call(
+    spread, along, select, rival_lane, *later = pl.pallas_call(
         functools.partial(prepare, experts_of),
         out_shape=shapes,
-        in_specs=[pl.BlockSpec(memory_space=pl.ANY)] * 12,
+        in_specs=[pl.BlockSpec(memory_space=pl.ANY)] * 13,
         out_specs=[vmem] * len(shapes),
         scratch_shapes=[
             pltpu.VMEM((expert_ids.shape[1], tokens), jnp.int32),
-            pltpu.SemaphoreType.DMA((12,)),
+            pltpu.SemaphoreType.DMA((13,)),
         ],
     )(w_query, w_key, w_value, w_decay, w_output.T, expert_ids.T, *later)
-    residual_in, norm_gain, head_gain, ffn_gain, decay_bias, group_rows = later
+    residual_in, norm_gain, head_gain, ffn_gain, decay_bias, group_rows, router_expert = later
     expert = lax.axis_index(EP)
     groups = router_group.shape[1]
     lanes = jnp.arange(n_experts, dtype=jnp.int32)
@@ -156,9 +234,9 @@
     strips = strips.reshape(slab, seqs, held)
 
     tied = lax.optimization_barrier(
-        (spread, strips, select, rival_lane, own_lane, own_group, own_gain, scale)
-    )
-    spread, strips, select, rival_lane, own_lane, own_group, own_gain, scale = tied
+        (spread, strips, along, select, rival_lane, own_lane, own_group, own_gain, scale)
+    )
+    spread, strips, along, select, rival_lane, own_lane, own_group, own_gain, scale = tied
     gathered = exchange(spread, "ep_0").reshape(held, in_width + value_width)
     gathered, strips = lax.optimization_barrier((gathered, strips))
     slab_res = exchange(strips, SLAB).reshape(slab * seqs, held)
@@ -181,30 +259,33 @@
 
     slab_heads, slab_res = exchange(to_all(gated, slab), SLAB, slab_res)
     slab_heads = slab_heads.reshape(slab * seqs, value_width)
-    head_part = lax.dot_general(
-        slab_heads,
-        gathered[:, in_width:],
-        (((1,), (1,)), ((), ())),
-        preferred_element_type=F32,
-    ).astype(BF16)
-
-    def by_owner(columns):
-        return columns.reshape(rows, cores * seqs, parts, strip)
-
-    both = jnp.concatenate([by_owner(head_part), by_owner(slab_res)], axis=3)
-    both = both.transpose(0, 2, 1, 3).reshape(rows * parts, cores * seqs, 2 * strip)
-    came = exchange(both, SLAB_TP).reshape(slab, heads, cores * seqs, 2 * strip)
-    attention = came[..., :strip].astype(F32).sum(axis=1)
-    came_res = came[:, 0, :, strip:].astype(F32)
-    hidden = (came_res + attention).astype(BF16)
-    hidden = hidden.transpose(1, 0, 2).reshape(cores * seqs, piece)
-
-    all_hidden = exchange(to_all(hidden, far), FAR).reshape(tokens, piece)
-    slot_part = jnp.dot(select, all_hidden, preferred_element_type=F32).astype(BF16)
-    outward = jnp.broadcast_to(
-        slot_part.reshape(cores, 1, CAP, piece), (cores, heads, CAP, piece)
-    ).reshape(parts, CAP, piece)
-    slot_hidden, ffn_gain = exchange(outward, CHIPS, ffn_gain)
+    lines = slab * seqs // (128 // (held // heads))
+    came = pl.pallas_call(
+        pack,
+        out_shape=pltpu.VMEM((slab * heads, lines, held), BF16),
+        in_specs=[vmem] * 3,
+        out_specs=vmem,
+    )(*map(on_chip, (slab_heads, gathered, slab_res)))
+    came = exchange(came, SLAB_TP)
+
+    def at_place():
+        return lax.axis_index("ep_0"), lax.axis_index("ep_1"), lax.axis_index("ep_2")
+
+    outward, hidden = pl.pallas_call(
+        functools.partial(dispatch, at_place),
+        out_shape=[
+            pltpu.VMEM((depths, CAP, width // heads), BF16),
+            pltpu.VMEM((cores * seqs, piece), BF16),
+        ],
+        in_specs=[vmem] * 2,
+        out_specs=[vmem] * 2,
+        scratch_shapes=[
+            pltpu.VMEM((slab * seqs, width // heads), F32),
+            pltpu.VMEM((tokens, width // heads), BF16),
+        ],
+    )(on_chip(came), on_chip(along))
+    slot_part = exchange(outward, "ep_0").astype(F32).sum(axis=0).astype(BF16)
+    slot_hidden, ffn_gain = exchange(to_all(slot_part, heads), "tp", ffn_gain)
     slot_hidden = slot_hidden.transpose(1, 0, 2).reshape(CAP, width)
     slot_rows = rms_scale(slot_hidden, ffn_gain).astype(BF16)
 
@@ -224,7 +305,8 @@
     up_out = jnp.dot(slot_rows, w_up[0], preferred_element_type=F32)
     units = (jax.nn.silu(gate_out) * up_out).astype(BF16)
     output = jnp.dot(units, w_down[0], preferred_element_type=F32) * slot_weight[:, None]
-    back = output.astype(BF16).reshape(CAP, parts, piece).transpose(1, 0, 2)
+    back = output.astype(BF16).reshape(CAP, heads, cores, piece).transpose(2, 1, 0, 3)
+    back = back.reshape(parts, CAP, piece)
     summed = exchange(back, CHIPS).reshape(cores, heads, CAP, piece).astype(F32).sum(axis=1)
     dense = lax.dot_general(
         select,
@@ -238,7 +320,8 @@
     last = jnp.broadcast_to(
         layer.reshape(cores, 1, seqs, piece), (cores, heads, seqs, piece)
     ).reshape(parts, seqs, piece)
-    layer_out = exchange(last, CHIPS).transpose(1, 0, 2).reshape(seqs, width)
+    layer_out = exchange(last, CHIPS).reshape(cores, heads, seqs, piece)
+    layer_out = layer_out.transpose(2, 1, 0, 3).reshape(seqs, width)
     return (layer_out, new_state[:, None])
 
 

time: 144 us -> 140 us (0.972)
  blocking collectives: 135 us -> 131 us
    all_to_all x10, blocking collectives: 135 us -> 131 us  [exchange(): came = lax.all_to_all(blocks, axes, split_axis=0, concat_axis=0, tiled=True)]
where the time goes in v3:
time: 140 us
  blocking collectives  131 us (94%)
  other arithmetic  2.21 us (2%)
  Pallas kernels  1.93 us (1%)
  local copies, waits for them, and re-layouts  1.64 us (1%)
  matrix products  1.53 us (1%)
    all_to_all x10, blocking collectives, exchange(): came = lax.all_to_all(blocks, axes, split_axis=0, concat_axis=0, tiled=True)  131 us

profile of v3, /device:TPU:1, one launch (start us, length us, event | category | flops | bytes accessed | tf_op | source)
XLA Modules:
  0.0 139.6 jit_solution(1989297835802511457)
XLA Ops:
  0.7 1.4 shard_map.176
  2.0 0.1 multiply_reduce_fusion.1
  2.2 0.1 reshape.140
  2.3 0.1 reshape.142
  2.4 0.1 reshape.155
  2.6 0.1 reshape.141
  2.7 25.5 %all_to_all.50 = bf16[8,16,1792]{2,1,0:T(8,128)(2,1)S(1)} all-to-all(bf16[8,16,1792]{2,1,0:T(8,128)(2,1)S(1)} %get-tuple-element.44), channel_id=1, replica_groups=mesh['ep_0'=8,'ep_1'=8,'ep_2'=2,'tp'=4] {'ep_0'}, dimensions={0} | all-to-all | bytes 917504 | tf_op jit(solution)/shard_map/all_to_all | solution.py:25
  28.1 16.2 %all_to_all.51 = bf16[16,2,128]{2,1,0:T(2,128)(2,1)S(1)} all-to-all(bf16[16,2,128]{2,1,0:T(2,128)(2,1)S(1)} %reshape.141), channel_id=1, replica_groups=mesh['ep_0'=8,'ep_1'=8,'ep_2'=2,'tp'=4] {'ep_1','ep_2'}, dimensions={0} | all-to-all | bytes 16384 | tf_op jit(solution)/shard_map/all_to_all | solution.py:25
  44.3 0.2 convolution_convert_fusion
  44.5 11.2 %all_to_all.52 = bf16[16,2,1280]{2,1,0:T(2,128)(2,1)S(1)} all-to-all(bf16[16,2,1280]{2,1,0:T(2,128)(2,1)S(1)} %reshape.145), channel_id=1, replica_groups=mesh['ep_0'=8,'ep_1'=8,'ep_2'=2,'tp'=4] {'ep_1','ep_2'}, dimensions={0} | all-to-all | bytes 163840 | tf_op jit(solution)/shard_map/all_to_all | solution.py:25
  55.7 0.1 convert_reduce_fusion.1
  56.0 1.2 multiply_reduce_fusion
  57.2 0.1 multiply_reduce_fusion.4
  57.4 9.9 %all_to_all.53 = bf16[16,2,512]{2,1,0:T(2,128)(2,1)S(1)} all-to-all(bf16[16,2,512]{2,1,0:T(2,128)(2,1)S(1)} %broadcast_in_dim.10), channel_id=1, replica_groups=mesh['ep_0'=8,'ep_1'=8,'ep_2'=2,'tp'=4] {'ep_1','ep_2'}, dimensions={0} | all-to-all | bytes 65536 | tf_op jit(solution)/shard_map/all_to_all | solution.py:25
  67.4 0.2 shard_map.177
  67.6 15.3 %all_to_all.54.came_ref = bf16[64,8,128]{2,1,0:T(8,128)(2,1)S(1)} all-to-all(bf16[64,8,128]{2,1,0:T(8,128)(2,1)S(1)} %shard_map.177), channel_id=1, replica_groups=mesh['ep_0'=8,'ep_1'=8,'ep_2'=2,'tp'=4] {'ep_1','ep_2','tp'}, dimensions={0} | all-to-all | bytes 262144 | tf_op jit(solution)/shard_map/all_to_all | solution.py:25
  82.9 0.3 shard_map.178
  83.2 10.3 %all_to_all.55 = bf16[8,16,512]{2,1,0:T(8,128)(2,1)S(1)} all-to-all(bf16[8,16,512]{2,1,0:T(8,128)(2,1)S(1)} %get-tuple-element.59), channel_id=1, replica_groups=mesh['ep_0'=8,'ep_1'=8,'ep_2'=2,'tp'=4] {'ep_0'}, dimensions={0} | all-to-all | bytes 262144 | tf_op jit(solution)/shard_map/all_to_all | solution.py:25
  93.6 7.0 %all_to_all.56 = bf16[4,16,512]{2,1,0:T(8,128)(2,1)S(1)} all-to-all(bf16[4,16,512]{2,1,0:T(8,128)(2,1)S(1)} %broadcast_in_dim.11), channel_id=1, replica_groups=mesh['ep_0'=8,'ep_1'=8,'ep_2'=2,'tp'=4] {'tp'}, dimensions={0} | all-to-all | bytes 131072 | tf_op jit(solution)/shard_map/all_to_all | solution.py:25
  100.6 0.1 fusion.9
  100.7 0.1 fusion.12
  100.9 0.2 fusion.6
  101.0 0.2 multiply_reduce_fusion.5
  101.3 0.4 multiply_reduce_fusion.2
  101.7 0.4 copy-done.3
  102.1 0.3 fusion
  102.5 11.5 %all_to_all.57 = bf16[8,16,256]{2,1,0:T(8,128)(2,1)S(1)} all-to-all(bf16[8,16,256]{2,1,0:T(8,128)(2,1)S(1)} %bitcast.61), channel_id=1, replica_groups=mesh['ep_0'=8,'ep_1'=8,'ep_2'=2,'tp'=4] {'ep_2','tp'}, dimensions={0} | all-to-all | bytes 131072 | tf_op jit(solution)/shard_map/all_to_all | solution.py:25
  114.0 0.2 convolution_convert_fusion.1
  114.3 15.4 %all_to_all.58 = bf16[64,4,256]{2,1,0:T(4,128)(2,1)S(1)} all-to-all(bf16[64,4,256]{2,1,0:T(4,128)(2,1)S(1)} %reshape.151), channel_id=1, replica_groups=mesh['ep_0'=8,'ep_1'=8,'ep_2'=2,'tp'=4] {'ep_0','ep_1'}, dimensions={0} | all-to-all | bytes 262144 | tf_op jit(solution)/shard_map/all_to_all | solution.py:25
  129.7 0.1 convert_reduce_fusion
  129.8 9.2 %all_to_all.59 = bf16[8,2,256]{2,1,0:T(2,128)(2,1)S(1)} all-to-all(bf16[8,2,256]{2,1,0:T(2,128)(2,1)S(1)} %bitcast.63), channel_id=1, replica_groups=mesh['ep_0'=8,'ep_1'=8,'ep_2'=2,'tp'=4] {'ep_2','tp'}, dimensions={0} | all-to-all | bytes 16384 | tf_op jit(solution)/shard_map/all_to_all | solution.py:25
  139.0 0.6 reshape.154
  (40 shorter events, 0.6 us)
Async XLA Ops:
  0.6 101.1 %copy-start = (bf16[1,128,2048]{2,1,0:T(8,128)(2,1)S(1)}, bf16[1,128,2048]{2,1,0:T(8,128)(2,1)}, u32[]{:S(2)}) copy-start(bf16[1,128,2048]{2,1,0:T(8,128)(2,1)} %param.33) | copy-start | bytes 1572868
  2.3 53.6 %copy-start.1 = (f32[2,1,256,512]{3,2,1,0:T(8,128)S(1)}, f32[2,1,256,512]{3,2,1,0:T(8,128)}, u32[]{:S(2)}) copy-start(f32[2,1,256,512]{3,2,1,0:T(8,128)} %param.18) | copy-start | bytes 3145732
  93.6 7.3 %copy-start.2 = (bf16[1,2048,128]{2,1,0:T(8,128)(2,1)S(1)}, bf16[1,2048,128]{2,1,0:T(8,128)(2,1)}, u32[]{:S(2)}) copy-start(bf16[1,2048,128]{2,1,0:T(8,128)(2,1)} %param.31) | copy-start | bytes 1572868
  101.0 1.0 copy-start.3

commit v4 on v3

--- a/solution.py
+++ b/solution.py
@@ -13,7 +13,8 @@
 FAR = ("ep_0", "ep_1")
 SLAB = ("ep_1", "ep_2")
 SLAB_TP = ("ep_1", "ep_2", "tp")
-CHIPS = ("ep_2", "tp")
+CHIPS = ("tp", "ep_2")
+DEPTH_TP = ("ep_0", "tp")
 
 EPSILON = 1e-06
 GATE_SCALE = 16.0
@@ -34,17 +35,8 @@
     return jnp.broadcast_to(shard[None], (count, *shard.shape))
 
 
-def rms_scale(values, gain_vec):
-    floats = values.astype(F32)
-    return (
-        floats
-        * lax.rsqrt(jnp.mean(floats * floats, axis=-1, keepdims=True) + EPSILON)
-        * gain_vec.astype(F32)
-    )
-
-
 def prepare(experts_of, *refs):
-    sources, (spread, along, select, rival, *kept), (ids, sems) = refs[:13], refs[13:-2], refs[-2:]
+    sources, (spread, along, select, rival, *kept), (ids, sems) = refs[:12], refs[12:-2], refs[-2:]
     *weights, ids_in = sources[:6]
     width = 0
     copies = []
@@ -97,6 +89,86 @@
         copy.wait()
 
 
+def advance(came_ref, res_ref, bias_ref, gain_ref, old_ref, out_ref, new_ref, held_ref, sems):
+    seqs, key_width, value_width = old_ref.shape
+    total = came_ref[0].astype(F32)
+    for at in range(1, came_ref.shape[0]):
+        total = total + came_ref[at].astype(F32)
+    res = res_ref[...].astype(F32)
+    total = total * lax.rsqrt(jnp.mean(res * res, axis=1, keepdims=True) + EPSILON)
+    query = total[:, :key_width].astype(BF16).astype(F32) * key_width ** (-0.5)
+    key = total[:, key_width : 2 * key_width].astype(BF16).astype(F32)
+    value = total[:, 2 * key_width : 2 * key_width + value_width].astype(BF16).astype(F32)
+    pre = total[:, 2 * key_width + value_width :] + bias_ref[...]
+    log_decay = (jnp.minimum(pre, 0.0) - jnp.log1p(jnp.exp(-jnp.abs(pre)))) / GATE_SCALE
+    down = jnp.concatenate([query, key, jnp.exp(log_decay), jnp.zeros_like(query)], axis=0).T
+    copies = []
+    gated = []
+    for seq in range(seqs):
+        read = jnp.zeros((1, value_width), F32)
+        for at in range(0, key_width, 32):
+            block = down[at : at + 32]
+            query_col = block[:, seq : seq + 1]
+            key_col = block[:, seqs + seq : seqs + seq + 1]
+            alpha_col = block[:, 2 * seqs + seq : 2 * seqs + seq + 1]
+            new = alpha_col * old_ref[seq, at : at + 32] + key_col * value[seq : seq + 1]
+            held_ref[seq, at : at + 32] = new
+            read = read + jnp.sum(query_col * new, axis=0, keepdims=True)
+        copies.append(pltpu.make_async_copy(held_ref.at[seq], new_ref.at[seq], sems.at[seq]))
+        copies[-1].start()
+        mean = jnp.mean(read * read, axis=1, keepdims=True)
+        gated.append(read * lax.rsqrt(mean + EPSILON) * gain_ref[...])
+    gated = jnp.concatenate(gated, axis=0).astype(BF16)
+    for at in range(out_ref.shape[0]):
+        out_ref[at] = gated
+    for copy in copies:
+        copy.wait()
+
+
+def mix(
+    which,
+    expert_ref,
+    came_ref,
+    gain_ref,
+    group_ref,
+    rival_ref,
+    gate_ref,
+    up_ref,
+    down_ref,
+    out_ref,
+    rows_ref,
+):
+    expert = which()
+    count, slots, size = came_ref.shape
+    quarters = rows_ref.shape[1] // size
+    for quarter in range(quarters):
+        total = came_ref[quarter].astype(F32)
+        for at in range(quarters + quarter, count, quarters):
+            total = total + came_ref[at].astype(F32)
+        rows_ref[:, size * quarter : size * (quarter + 1)] = total
+    rows = rows_ref[...]
+    mean = jnp.mean(rows * rows, axis=1, keepdims=True)
+    rows = (rows * lax.rsqrt(mean + EPSILON) * gain_ref[...]).astype(BF16)
+    gate = jnp.dot(rows, gate_ref[...], preferred_element_type=F32)
+    up = jnp.dot(rows, up_ref[...], preferred_element_type=F32)
+    over = (((1,), (1,)), ((), ()))
+    groups = lax.dot_general(rows, group_ref[...], over, preferred_element_type=F32)
+    logits = lax.dot_general(rows, expert_ref[...], over, preferred_element_type=F32)
+    units = (gate * jax.nn.sigmoid(gate) * up).astype(BF16)
+    output = jnp.dot(units, down_ref[...], preferred_element_type=F32)
+    of_group = lax.broadcasted_iota(jnp.int32, groups.shape, 1)
+    own = of_group == expert // (logits.shape[1] // groups.shape[1])
+    group_logit = jnp.sum(jnp.where(own, groups, 0.0), axis=1, keepdims=True)
+    share = 1.0 / jnp.sum(jnp.exp(groups - group_logit), axis=1, keepdims=True)
+    lanes = lax.broadcasted_iota(jnp.int32, logits.shape, 1)
+    chosen = jnp.sum(jnp.where(lanes == expert, logits, 0.0), axis=1, keepdims=True)
+    rival = jnp.sum(logits * rival_ref[...], axis=1, keepdims=True)
+    output = (output * (share * jax.nn.sigmoid(chosen - rival))).astype(BF16)
+    piece = out_ref.shape[2]
+    for at in range(out_ref.shape[0]):
+        out_ref[at] = output[:, piece * at : piece * (at + 1)]
+
+
 def pack(heads_ref, held_ref, res_ref, out_ref):
     value_width = heads_ref.shape[1]
     part = lax.dot_general(
@@ -122,7 +194,7 @@
             out_ref[count * at + quarter] = block
 
 
-def dispatch(at_place, came_ref, along_ref, out_ref, hidden_ref, rows_ref, all_ref):
+def dispatch(at_place, came_ref, along_ref, _, out_ref, hidden_ref, rows_ref, all_ref):
     depth, row, core = at_place()
     count, lines, lanes = came_ref.shape
     heads = lanes // (2 * 16)
@@ -149,7 +221,8 @@
     all_ref[pl.ds(pl.multiple_of(depth * size, size), size)] = rows
     slots = jnp.dot(along_ref[...], all_ref[...], preferred_element_type=F32).astype(BF16)
     for at in range(out_ref.shape[0]):
-        out_ref[at] = slots[CAP * at : CAP * (at + 1)]
+        first = CAP * (at // heads)
+        out_ref[at] = slots[first : first + CAP]
     own, piece = hidden_ref.shape
     here = lax.broadcasted_iota(jnp.int32, (8, size), 0)
     there = lax.broadcasted_iota(jnp.int32, (8, size), 1)
@@ -202,7 +275,6 @@
 
     vmem = pl.BlockSpec(memory_space=pltpu.VMEM)
     later = (residual_in, norm_gain, head_gain, ffn_gain, decay_bias, router_group.T)
-    later += (router_expert,)
     shapes = [
         pltpu.VMEM((depths, strip, in_width + value_width), BF16),
         pltpu.VMEM((depths * CAP, tokens), BF16),
@@ -213,51 +285,48 @@
     spread, along, select, rival_lane, *later = pl.pallas_call(
         functools.partial(prepare, experts_of),
         out_shape=shapes,
-        in_specs=[pl.BlockSpec(memory_space=pl.ANY)] * 13,
+        in_specs=[pl.BlockSpec(memory_space=pl.ANY)] * 12,
         out_specs=[vmem] * len(shapes),
         scratch_shapes=[
             pltpu.VMEM((expert_ids.shape[1], tokens), jnp.int32),
-            pltpu.SemaphoreType.DMA((13,)),
+            pltpu.SemaphoreType.DMA((12,)),
         ],
     )(w_query, w_key, w_value, w_decay, w_output.T, expert_ids.T, *later)
-    residual_in, norm_gain, head_gain, ffn_gain, decay_bias, group_rows, router_expert = later
-    expert = lax.axis_index(EP)
-    groups = router_group.shape[1]
-    lanes = jnp.arange(n_experts, dtype=jnp.int32)
-    own_group = jnp.arange(groups, dtype=jnp.int32) == expert // (n_experts // groups)
-    own_lane = (lanes == expert).astype(F32)
-    own_group = own_group.astype(F32)
+    residual_in, norm_gain, head_gain, ffn_gain, decay_bias, group_rows = later
+    head_gain = head_gain.astype(F32)[None]
+    ffn_gain = ffn_gain.astype(F32)[None]
+    decay_bias = decay_bias[None]
     own_gain = norm_gain.reshape(depths, slab, strip)[:, place].reshape(held).astype(F32)
-    res_float = residual_in.astype(F32)
-    scale = lax.rsqrt(jnp.mean(res_float * res_float, axis=-1, keepdims=True) + EPSILON)
     strips = residual_in.reshape(seqs, depths, slab, strip).transpose(2, 0, 1, 3)
     strips = strips.reshape(slab, seqs, held)
 
     tied = lax.optimization_barrier(
-        (spread, strips, along, select, rival_lane, own_lane, own_group, own_gain, scale)
+        (spread, strips, along, select, rival_lane, own_gain)
+        + (head_gain, ffn_gain, decay_bias)
     )
-    spread, strips, along, select, rival_lane, own_lane, own_group, own_gain, scale = tied
+    spread, strips, along, select, rival_lane, own_gain, *tied = tied
+    head_gain, ffn_gain, decay_bias = tied
     gathered = exchange(spread, "ep_0").reshape(held, in_width + value_width)
     gathered, strips = lax.optimization_barrier((gathered, strips))
     slab_res = exchange(strips, SLAB).reshape(slab * seqs, held)
     lhs = (slab_res.astype(F32) * own_gain).astype(BF16)
     sums = jnp.dot(lhs, gathered[:, :in_width], preferred_element_type=F32).astype(BF16)
-    arrived, head_gain, decay_bias = exchange(
-        sums.reshape(slab, seqs, in_width), SLAB, head_gain, decay_bias
-    )
-    projected = arrived.astype(F32).sum(axis=0) * scale
-
-    query = projected[:, :key_width].astype(BF16).astype(F32) * key_width ** (-0.5)
-    key = projected[:, key_width : 2 * key_width].astype(BF16).astype(F32)
-    value = projected[:, 2 * key_width : 2 * key_width + value_width].astype(BF16).astype(F32)
-    decay_pre = projected[:, 2 * key_width + value_width :]
-    alpha = jnp.exp(jax.nn.log_sigmoid(decay_pre + decay_bias) / GATE_SCALE)
-    new_state = alpha[:, :, None] * gla_state[:, 0] + key[:, :, None] * value[:, None, :]
-    read_out = jnp.sum(query[:, :, None] * new_state, axis=1)
-    gated = rms_scale(read_out, head_gain).astype(BF16)
-    gated, new_state = lax.optimization_barrier((gated, new_state))
-
-    slab_heads, slab_res = exchange(to_all(gated, slab), SLAB, slab_res)
+    arrived = exchange(sums.reshape(slab, seqs, in_width), SLAB)
+    gated, new_state = pl.pallas_call(
+        advance,
+        out_shape=[
+            pltpu.VMEM((slab, seqs, value_width), BF16),
+            jax.ShapeDtypeStruct((seqs, key_width, value_width), F32),
+        ],
+        in_specs=[vmem] * 5,
+        out_specs=[vmem, pl.BlockSpec(memory_space=pl.ANY)],
+        scratch_shapes=[
+            pltpu.VMEM((seqs, key_width, value_width), F32),
+            pltpu.SemaphoreType.DMA((seqs,)),
+        ],
+    )(*map(on_chip, (arrived, residual_in, decay_bias, head_gain, gla_state[:, 0])))
+
+    slab_heads, slab_res = exchange(gated, SLAB, slab_res)
     slab_heads = slab_heads.reshape(slab * seqs, value_width)
     lines = slab * seqs // (128 // (held // heads))
     came = pl.pallas_call(
@@ -267,6 +336,7 @@
         out_specs=vmem,
     )(*map(on_chip, (slab_heads, gathered, slab_res)))
     came = exchange(came, SLAB_TP)
+    router = on_chip(router_expert)
 
     def at_place():
         return lax.axis_index("ep_0"), lax.axis_index("ep_1"), lax.axis_index("ep_2")
@@ -274,40 +344,27 @@
     outward, hidden = pl.pallas_call(
         functools.partial(dispatch, at_place),
         out_shape=[
-            pltpu.VMEM((depths, CAP, width // heads), BF16),
+            pltpu.VMEM((depths * heads, CAP, width // heads), BF16),
             pltpu.VMEM((cores * seqs, piece), BF16),
         ],
-        in_specs=[vmem] * 2,
+        in_specs=[vmem] * 3,
         out_specs=[vmem] * 2,
         scratch_shapes=[
             pltpu.VMEM((slab * seqs, width // heads), F32),
             pltpu.VMEM((tokens, width // heads), BF16),
         ],
-    )(on_chip(came), on_chip(along))
-    slot_part = exchange(outward, "ep_0").astype(F32).sum(axis=0).astype(BF16)
-    slot_hidden, ffn_gain = exchange(to_all(slot_part, heads), "tp", ffn_gain)
-    slot_hidden = slot_hidden.transpose(1, 0, 2).reshape(CAP, width)
-    slot_rows = rms_scale(slot_hidden, ffn_gain).astype(BF16)
-
-    group_logits = lax.dot_general(
-        slot_rows, group_rows, (((1,), (1,)), ((), ())), preferred_element_type=F32
-    )
-    group_logit = jnp.sum(group_logits * own_group[None], axis=1)
-    group_share = 1.0 / jnp.sum(jnp.exp(group_logits - group_logit[:, None]), axis=1)
-    expert_logits = lax.dot_general(
-        slot_rows, router_expert, (((1,), (1,)), ((), ())), preferred_element_type=F32
-    )
-    chosen = jnp.sum(expert_logits * own_lane[None], axis=1)
-    rival = jnp.sum(expert_logits * rival_lane, axis=1)
-    slot_weight = group_share * jax.nn.sigmoid(chosen - rival)
-
-    gate_out = jnp.dot(slot_rows, w_gate[0], preferred_element_type=F32)
-    up_out = jnp.dot(slot_rows, w_up[0], preferred_element_type=F32)
-    units = (jax.nn.silu(gate_out) * up_out).astype(BF16)
-    output = jnp.dot(units, w_down[0], preferred_element_type=F32) * slot_weight[:, None]
-    back = output.astype(BF16).reshape(CAP, heads, cores, piece).transpose(2, 1, 0, 3)
-    back = back.reshape(parts, CAP, piece)
-    summed = exchange(back, CHIPS).reshape(cores, heads, CAP, piece).astype(F32).sum(axis=1)
+    )(on_chip(came), on_chip(along), router)
+    came = exchange(outward, DEPTH_TP)
+    operands = (came, ffn_gain, group_rows, rival_lane)
+    operands += (w_gate[0], w_up[0], w_down[0])
+    back = pl.pallas_call(
+        functools.partial(mix, lambda: lax.axis_index(EP)),
+        out_shape=pltpu.VMEM((parts, CAP, piece), BF16),
+        in_specs=[vmem] * (1 + len(operands)),
+        out_specs=vmem,
+        scratch_shapes=[pltpu.VMEM((CAP, width), F32)],
+    )(router, *map(on_chip, operands))
+    summed = exchange(back, CHIPS).reshape(heads, cores, CAP, piece).astype(F32).sum(axis=0)
     dense = lax.dot_general(
         select,
         summed.astype(BF16).reshape(cores * CAP, piece),
@@ -317,11 +374,8 @@
     moe, hidden = exchange(dense.reshape(far, cores * seqs, piece), FAR, hidden)
     moe = moe.astype(F32).sum(axis=0)
     layer = (hidden.astype(F32) + moe).astype(BF16)
-    last = jnp.broadcast_to(
-        layer.reshape(cores, 1, seqs, piece), (cores, heads, seqs, piece)
-    ).reshape(parts, seqs, piece)
-    layer_out = exchange(last, CHIPS).reshape(cores, heads, seqs, piece)
-    layer_out = layer_out.transpose(2, 1, 0, 3).reshape(seqs, width)
+    last = to_all(layer.reshape(cores, seqs, piece), heads).reshape(parts, seqs, piece)
+    layer_out = exchange(last, CHIPS).transpose(1, 0, 2).reshape(seqs, width)
     return (layer_out, new_state[:, None])
 
 

time: 140 us -> 140 us (level)
  other arithmetic: 2.21 us -> 0.14 us
  blocking collectives: 131 us -> 133 us
  Pallas kernels: 1.93 us -> 3.9 us
    pallas_call x0 -> x2, Pallas kernels: none -> 2.17 us  [the longest x1 1.45 us: on_device(): pl.pallas_call(advance, out_shape=[pltpu.VMEM((slab, seqs, value_width),...]
    all_to_all x10 -> x9, blocking collectives: 131 us -> 133 us  [exchange(): came = lax.all_to_all(blocks, axes, split_axis=0, concat_axis=0, tiled=True)]
    reduce_sum x8 -> x1, other arithmetic: 1.77 us -> 0.01 us  [on_device(): exchange(back, CHIPS).reshape(heads, cores, CAP, piece).astype(F32)]
where the time goes in v4:
time: 140 us
  blocking collectives  133 us (95%)
  Pallas kernels  3.9 us (3%)
    all_to_all x9, blocking collectives, exchange(): came = lax.all_to_all(blocks, axes, split_axis=0, concat_axis=0, tiled=True)  133 us

profile of v4, /device:TPU:1, one launch (start us, length us, event | category | flops | bytes accessed | tf_op | source)
XLA Modules:
  0.0 139.8 jit_solution(12868269736825444493)
XLA Ops:
  0.6 1.2 shard_map.176
  1.8 0.0 copy-start.1
  1.8 0.1 reshape.46
  2.0 0.1 reshape.56
  2.0 0.1 reshape.44
  2.2 0.1 reshape.45
  2.3 25.5 %all_to_all.45 = bf16[8,16,1792]{2,1,0:T(8,128)(2,1)S(1)} all-to-all(bf16[8,16,1792]{2,1,0:T(8,128)(2,1)S(1)} %get-tuple-element.41), channel_id=1, replica_groups=mesh['ep_0'=8,'ep_1'=8,'ep_2'=2,'tp'=4] {'ep_0'}, dimensions={0} | all-to-all | bytes 917504 | tf_op jit(solution)/shard_map/all_to_all | solution.py:26
  27.7 16.2 %all_to_all.46 = bf16[16,2,128]{2,1,0:T(2,128)(2,1)S(1)} all-to-all(bf16[16,2,128]{2,1,0:T(2,128)(2,1)S(1)} %reshape.45), channel_id=1, replica_groups=mesh['ep_0'=8,'ep_1'=8,'ep_2'=2,'tp'=4] {'ep_1','ep_2'}, dimensions={0} | all-to-all | bytes 16384 | tf_op jit(solution)/shard_map/all_to_all | solution.py:26
  43.9 0.2 convolution_convert_fusion
  44.1 11.2 %all_to_all.47.came_ref = bf16[16,2,1280]{2,1,0:T(2,128)(2,1)S(1)} all-to-all(bf16[16,2,1280]{2,1,0:T(2,128)(2,1)S(1)} %reshape.49), channel_id=1, replica_groups=mesh['ep_0'=8,'ep_1'=8,'ep_2'=2,'tp'=4] {'ep_1','ep_2'}, dimensions={0} | all-to-all | bytes 163840 | tf_op jit(solution)/shard_map/all_to_all | solution.py:26
  55.4 0.0 copy-done.1
  55.4 1.5 %shard_map.177 = (bf16[16,2,512]{2,1,0:T(2,128)(2,1)S(1)}, f32[2,256,512]{2,1,0:T(8,128)}) custom-call(bf16[16,2,1280]{2,1,0:T(2,128)(2,1)S(1)} %all_to_all.47.came_ref, bf16[2,2048]{1,0:T(2,128)(2,1)S(1)} %get-tuple-element.32.res_ref, f32[1,256]{1,0:T(1,128)S(1)} %bitcast.36, f32[1,512]{1,0:T(1,128)S(1)} %bitcast.35, f32[2,256,512]{2,1,0:T(8,128)S(1)} %bitcast.28), custom_call_target="tpu_custom_call" | custom-call | tf_op jit(solution)/shard_map/pallas_call | solution.py:315
  56.8 0.0 copy-start
  56.8 10.0 %all_to_all.48 = bf16[16,2,512]{2,1,0:T(2,128)(2,1)S(1)} all-to-all(bf16[16,2,512]{2,1,0:T(2,128)(2,1)S(1)} %get-tuple-element.48), channel_id=1, replica_groups=mesh['ep_0'=8,'ep_1'=8,'ep_2'=2,'tp'=4] {'ep_1','ep_2'}, dimensions={0} | all-to-all | bytes 65536 | tf_op jit(solution)/shard_map/all_to_all | solution.py:26
  66.9 0.2 shard_map.178
  67.1 15.3 %all_to_all.49.came_ref = bf16[64,8,128]{2,1,0:T(8,128)(2,1)S(1)} all-to-all(bf16[64,8,128]{2,1,0:T(8,128)(2,1)S(1)} %shard_map.178), channel_id=1, replica_groups=mesh['ep_0'=8,'ep_1'=8,'ep_2'=2,'tp'=4] {'ep_1','ep_2','tp'}, dimensions={0} | all-to-all | bytes 262144 | tf_op jit(solution)/shard_map/all_to_all | solution.py:26
  82.4 0.0 copy-done
  82.4 0.0 copy-start.4
  82.4 0.3 shard_map.179
  82.8 0.0 copy-start.2
  82.8 0.0 copy-start.3
  82.8 18.3 %all_to_all.50.came_ref = bf16[32,16,512]{2,1,0:T(8,128)(2,1)S(1)} all-to-all(bf16[32,16,512]{2,1,0:T(8,128)(2,1)S(1)} %get-tuple-element.52), channel_id=1, replica_groups=mesh['ep_0'=8,'ep_1'=8,'ep_2'=2,'tp'=4] {'ep_0','tp'}, dimensions={0} | all-to-all | bytes 1048576 | tf_op jit(solution)/shard_map/all_to_all | solution.py:26
  101.1 0.0 copy-done.4
  101.1 0.0 copy-done.2
  101.1 0.0 copy-done.3
  101.1 0.7 shard_map.180
  101.8 11.8 %all_to_all.51 = bf16[8,16,256]{2,1,0:T(8,128)(2,1)S(1)} all-to-all(bf16[8,16,256]{2,1,0:T(8,128)(2,1)S(1)} %shard_map.180), channel_id=1, replica_groups=mesh['ep_0'=8,'ep_1'=8,'ep_2'=2,'tp'=4] {'tp','ep_2'}, dimensions={0} | all-to-all | bytes 131072 | tf_op jit(solution)/shard_map/all_to_all | solution.py:26
  113.6 0.2 convolution_convert_fusion.1
  113.9 16.0 %all_to_all.52 = bf16[64,4,256]{2,1,0:T(4,128)(2,1)S(1)} all-to-all(bf16[64,4,256]{2,1,0:T(4,128)(2,1)S(1)} %reshape.53), channel_id=1, replica_groups=mesh['ep_0'=8,'ep_1'=8,'ep_2'=2,'tp'=4] {'ep_0','ep_1'}, dimensions={0} | all-to-all | bytes 262144 | tf_op jit(solution)/shard_map/all_to_all | solution.py:26
  129.9 0.1 convert_reduce_fusion
  130.0 9.2 %all_to_all.53 = bf16[8,2,256]{2,1,0:T(2,128)(2,1)S(1)} all-to-all(bf16[8,2,256]{2,1,0:T(2,128)(2,1)S(1)} %bitcast.40), channel_id=1, replica_groups=mesh['ep_0'=8,'ep_1'=8,'ep_2'=2,'tp'=4] {'tp','ep_2'}, dimensions={0} | all-to-all | bytes 16384 | tf_op jit(solution)/shard_map/all_to_all | solution.py:26
  139.2 0.6 copy.28
  (11 shorter events, 0.2 us)
Async XLA Ops:
  1.8 53.5 %copy-start.1 = (f32[2,1,256,512]{3,2,1,0:T(8,128)S(1)}, f32[2,1,256,512]{3,2,1,0:T(8,128)}, u32[]{:S(2)}) copy-start(f32[2,1,256,512]{3,2,1,0:T(8,128)} %param.18) | copy-start | bytes 3145732
  56.8 25.6 %copy-start = (bf16[128,2048]{1,0:T(8,128)(2,1)S(1)}, bf16[128,2048]{1,0:T(8,128)(2,1)}, u32[]{:S(2)}) copy-start(bf16[128,2048]{1,0:T(8,128)(2,1)} %expert_ref.1) | copy-start | bytes 1572868
  82.4 18.7 %copy-start.4 = (bf16[1,128,2048]{2,1,0:T(8,128)(2,1)S(1)}, bf16[1,128,2048]{2,1,0:T(8,128)(2,1)}, u32[]{:S(2)}) copy-start(bf16[1,128,2048]{2,1,0:T(8,128)(2,1)} %param.33) | copy-start | bytes 1572868
  82.8 18.3 %copy-start.2 = (bf16[1,2048,128]{2,1,0:T(8,128)(2,1)S(1)}, bf16[1,2048,128]{2,1,0:T(8,128)(2,1)}, u32[]{:S(2)}) copy-start(bf16[1,2048,128]{2,1,0:T(8,128)(2,1)} %param.31) | copy-start | bytes 1572868
  82.8 18.3 %copy-start.3 = (bf16[1,2048,128]{2,1,0:T(8,128)(2,1)S(1)}, bf16[1,2048,128]{2,1,0:T(8,128)(2,1)}, u32[]{:S(2)}) copy-start(bf16[1,2048,128]{2,1,0:T(8,128)(2,1)} %param.32) | copy-start | bytes 1572868

commit v5 on v4

--- a/solution.py
+++ b/solution.py
@@ -14,7 +14,6 @@
 SLAB = ("ep_1", "ep_2")
 SLAB_TP = ("ep_1", "ep_2", "tp")
 CHIPS = ("tp", "ep_2")
-DEPTH_TP = ("ep_0", "tp")
 
 EPSILON = 1e-06
 GATE_SCALE = 16.0
@@ -56,9 +55,11 @@
     upper = jnp.where(row <= col, 1.0, 0.0).astype(BF16)
     copies[5].wait()
     one, two = ids[0:1, :], ids[1:2, :]
-    depths = spread.shape[0]
-    index = lax.broadcasted_iota(jnp.int32, (2 * depths, count), 0)
-    experts = jnp.where(index < depths, index * slab + place, index - depths + first)
+    spans = along.shape[0] // CAP
+    cores = select.shape[0] // CAP
+    index = lax.broadcasted_iota(jnp.int32, (spans + 8, count), 0)
+    experts = index // cores * slab + place - core + index % cores
+    experts = jnp.where(index < spans, experts, index - spans + first)
     named = (one == experts) | (two == experts)
     marks = jnp.where(named, 1.0, 0.0)
     ends = jnp.dot(marks.astype(BF16), upper, preferred_element_type=F32)
@@ -71,10 +72,10 @@
     def slots_of(at):
         return jnp.where(ends[at : at + 1] == slots, marks[at : at + 1], 0.0)
 
-    for depth in range(depths):
-        along[CAP * depth : CAP * (depth + 1)] = slots_of(depth).astype(BF16)
-    for c in range(select.shape[0] // CAP):
-        mine = slots_of(depths + c)
+    for span in range(spans):
+        along[CAP * span : CAP * (span + 1)] = slots_of(span).astype(BF16)
+    for c in range(cores):
+        mine = slots_of(spans + c)
         select[CAP * c : CAP * (c + 1)] = mine.astype(BF16)
         total = jnp.sum(mine * both, axis=1, keepdims=True)
         others = jnp.where(core == c, total, others)
@@ -113,9 +114,15 @@
             alpha_col = block[:, 2 * seqs + seq : 2 * seqs + seq + 1]
             new = alpha_col * old_ref[seq, at : at + 32] + key_col * value[seq : seq + 1]
             held_ref[seq, at : at + 32] = new
+            if at % 64:
+                rows = pl.ds(at - 32, 64)
+                copies.append(
+                    pltpu.make_async_copy(
+                        held_ref.at[seq, rows], new_ref.at[seq, rows], sems.at[len(copies)]
+                    )
+                )
+                copies[-1].start()
             read = read + jnp.sum(query_col * new, axis=0, keepdims=True)
-        copies.append(pltpu.make_async_copy(held_ref.at[seq], new_ref.at[seq], sems.at[seq]))
-        copies[-1].start()
         mean = jnp.mean(read * read, axis=1, keepdims=True)
         gated.append(read * lax.rsqrt(mean + EPSILON) * gain_ref[...])
     gated = jnp.concatenate(gated, axis=0).astype(BF16)
@@ -139,13 +146,9 @@
     rows_ref,
 ):
     expert = which()
-    count, slots, size = came_ref.shape
-    quarters = rows_ref.shape[1] // size
-    for quarter in range(quarters):
-        total = came_ref[quarter].astype(F32)
-        for at in range(quarters + quarter, count, quarters):
-            total = total + came_ref[at].astype(F32)
-        rows_ref[:, size * quarter : size * (quarter + 1)] = total
+    size = came_ref.shape[2]
+    for at in range(came_ref.shape[0]):
+        rows_ref[:, size * at : size * (at + 1)] = came_ref[at].astype(F32)
     rows = rows_ref[...]
     mean = jnp.mean(rows * rows, axis=1, keepdims=True)
     rows = (rows * lax.rsqrt(mean + EPSILON) * gain_ref[...]).astype(BF16)
@@ -180,56 +183,60 @@
     with_res = (lax.axis_index("tp") == 0).astype(F32)
     part = part + res_ref[...].astype(F32) * with_res
     lines, lanes = out_ref.shape[1:]
-    count = part.shape[0] // lines
-    size = lanes // count
-    group = lax.broadcasted_iota(jnp.int32, (lines, lanes), 1) // size
-    for quarter in range(count):
-        block = jnp.zeros((lines, lanes), F32)
-        for k in range(count):
-            rows = part[lines * k : lines * (k + 1)]
-            moved = pltpu.roll(rows, (size * (k - quarter)) % lanes, 1)
-            block = jnp.where(group == k, moved, block)
-        block = block.astype(BF16)
-        for at in range(out_ref.shape[0] // count):
-            out_ref[count * at + quarter] = block
+    eighths = part.shape[0] // lines
+    size = lanes // eighths
+    group = lax.broadcasted_iota(jnp.int32, (2 * lines, lanes), 1) // size
+    lower = lax.broadcasted_iota(jnp.int32, (2 * lines, lanes), 0) // lines
+    for eighth in range(eighths):
+        block = jnp.zeros((2 * lines, lanes), F32)
+        for k in range(0, eighths, 2):
+            rows = part[lines * k : lines * (k + 2)]
+            for low in range(2):
+                moved = pltpu.roll(rows, (size * (k + low - eighth)) % lanes, 1)
+                block = jnp.where((group == k + low) & (lower == low), moved, block)
+        block = (block[:lines] + block[lines:]).astype(BF16)
+        quarter, core = eighth // 2, eighth % 2
+        for row in range(out_ref.shape[0] // eighths):
+            out_ref[eighths * row + eighths // 2 * core + quarter] = block
 
 
 def dispatch(at_place, came_ref, along_ref, _, out_ref, hidden_ref, rows_ref, all_ref):
-    depth, row, core = at_place()
+    depth, row = at_place()
     count, lines, lanes = came_ref.shape
-    heads = lanes // (2 * 16)
+    eighths = rows_ref.shape[0] // lines
+    size = lanes // eighths
+    heads = eighths // 2
     all_ref[...] = jnp.zeros_like(all_ref)
     hidden = []
     for at in range(count // heads):
         total = came_ref[heads * at].astype(F32)
         for head in range(1, heads):
             total = total + came_ref[heads * at + head].astype(F32)
-        hidden.append(total.astype(BF16).astype(F32))
-    group = lax.broadcasted_iota(jnp.int32, (lines, lanes), 1) // 16
-    for k in range(heads):
-        for strip in range(2):
-            for half in range(2):
-                block = jnp.zeros((lines, lanes), F32)
-                for m in range(8):
-                    shift = (16 * m - 32 * k - 16 * strip) % lanes
-                    moved = pltpu.roll(hidden[8 * half + m], shift, 1)
-                    block = jnp.where(group == m, moved, block)
-                at = 256 * strip + 128 * half
-                rows_ref[lines * k : lines * (k + 1), at : at + lanes] = block
+        total = total.astype(BF16).astype(F32)
+        both = jnp.concatenate([total, total], axis=0)
+        back = pltpu.roll(both, lanes - size, 1)
+        lower = lax.broadcasted_iota(jnp.int32, both.shape, 0) // lines
+        hidden.append(jnp.where(lower == 0, both, back))
+    group = lax.broadcasted_iota(jnp.int32, (2 * lines, lanes), 1) // size
+    for k in range(0, eighths, 2):
+        for half in range(2):
+            block = jnp.zeros((2 * lines, lanes), F32)
+            for m in range(eighths):
+                moved = pltpu.roll(hidden[eighths * half + m], (size * (m - k)) % lanes, 1)
+                block = jnp.where(group == m, moved, block)
+            rows_ref[lines * k : lines * (k + 2), lanes * half : lanes * (half + 1)] = block
     rows = rows_ref[...].astype(BF16)
-    size = rows.shape[0]
-    all_ref[pl.ds(pl.multiple_of(depth * size, size), size)] = rows
+    own = hidden_ref.shape[0]
+    slab = rows.shape[0]
+    all_ref[pl.ds(pl.multiple_of(depth * slab, slab), slab)] = rows
     slots = jnp.dot(along_ref[...], all_ref[...], preferred_element_type=F32).astype(BF16)
+    span = out_ref.shape[1]
     for at in range(out_ref.shape[0]):
-        first = CAP * (at // heads)
-        out_ref[at] = slots[first : first + CAP]
-    own, piece = hidden_ref.shape
-    here = lax.broadcasted_iota(jnp.int32, (8, size), 0)
-    there = lax.broadcasted_iota(jnp.int32, (8, size), 1)
+        out_ref[at] = slots[span * at : span * (at + 1)]
+    here = lax.broadcasted_iota(jnp.int32, (8, slab), 0)
+    there = lax.broadcasted_iota(jnp.int32, (8, slab), 1)
     pick = jnp.where(there == here + own * row, 1.0, 0.0).astype(BF16)
-    mine = jnp.dot(pick, rows, preferred_element_type=F32)
-    mine = jnp.where(core == 0, mine[:, :piece], mine[:, piece:])
-    hidden_ref[...] = mine[:own].astype(BF16)
+    hidden_ref[...] = jnp.dot(pick, rows, preferred_element_type=F32)[:own].astype(BF16)
 
 
 def on_device(
@@ -277,7 +284,7 @@
     later = (residual_in, norm_gain, head_gain, ffn_gain, decay_bias, router_group.T)
     shapes = [
         pltpu.VMEM((depths, strip, in_width + value_width), BF16),
-        pltpu.VMEM((depths * CAP, tokens), BF16),
+        pltpu.VMEM((depths * cores * CAP, tokens), BF16),
         pltpu.VMEM((cores * CAP, tokens), BF16),
         pltpu.VMEM((CAP, n_experts), F32),
         *(pltpu.VMEM(a.shape, a.dtype) for a in later),
@@ -322,13 +329,13 @@
         out_specs=[vmem, pl.BlockSpec(memory_space=pl.ANY)],
         scratch_shapes=[
             pltpu.VMEM((seqs, key_width, value_width), F32),
-            pltpu.SemaphoreType.DMA((seqs,)),
+            pltpu.SemaphoreType.DMA((seqs * key_width // 64,)),
         ],
     )(*map(on_chip, (arrived, residual_in, decay_bias, head_gain, gla_state[:, 0])))
 
     slab_heads, slab_res = exchange(gated, SLAB, slab_res)
     slab_heads = slab_heads.reshape(slab * seqs, value_width)
-    lines = slab * seqs // (128 // (held // heads))
+    lines = slab * seqs // parts
     came = pl.pallas_call(
         pack,
         out_shape=pltpu.VMEM((slab * heads, lines, held), BF16),
@@ -339,22 +346,24 @@
     router = on_chip(router_expert)
 
     def at_place():
-        return lax.axis_index("ep_0"), lax.axis_index("ep_1"), lax.axis_index("ep_2")
+        return lax.axis_index("ep_0"), lax.axis_index("ep_1")
 
     outward, hidden = pl.pallas_call(
         functools.partial(dispatch, at_place),
         out_shape=[
-            pltpu.VMEM((depths * heads, CAP, width // heads), BF16),
+            pltpu.VMEM((depths, cores * CAP, piece), BF16),
             pltpu.VMEM((cores * seqs, piece), BF16),
         ],
         in_specs=[vmem] * 3,
         out_specs=[vmem] * 2,
         scratch_shapes=[
-            pltpu.VMEM((slab * seqs, width // heads), F32),
-            pltpu.VMEM((tokens, width // heads), BF16),
+            pltpu.VMEM((slab * seqs, piece), F32),
+            pltpu.VMEM((tokens, piece), BF16),
         ],
     )(on_chip(came), on_chip(along), router)
-    came = exchange(outward, DEPTH_TP)
+    slot_part = exchange(outward, "ep_0").astype(F32).sum(axis=0).astype(BF16)
+    slot_part = to_all(slot_part.reshape(cores, CAP, piece), heads)
+    came = exchange(slot_part.reshape(parts, CAP, piece), CHIPS)
     operands = (came, ffn_gain, group_rows, rival_lane)
     operands += (w_gate[0], w_up[0], w_down[0])
     back = pl.pallas_call(

time: 140 us -> 137 us (0.979)
  blocking collectives: 133 us -> 130 us
    all_to_all x9 -> x10, blocking collectives: 133 us -> 130 us  [exchange(): came = lax.all_to_all(blocks, axes, split_axis=0, concat_axis=0, tiled=True)]
where the time goes in v5:
time: 137 us; the launch traced here: 136 us
  blocking collectives  130 us (95%)
  Pallas kernels  3.9 us (3%)
    all_to_all x10, blocking collectives, exchange(): came = lax.all_to_all(blocks, axes, split_axis=0, concat_axis=0, tiled=True)  130 us

profile of v5, /device:TPU:1, one launch (start us, length us, event | category | flops | bytes accessed | tf_op | source)
XLA Modules:
  0.0 136.1 jit_solution(14022488733246250476)
XLA Ops:
  0.6 1.1 shard_map.176
  1.8 0.0 copy-start.1
  1.8 0.1 reshape.50
  2.0 0.1 reshape.61
  2.0 0.1 reshape.48
  2.2 0.1 reshape.49
  2.3 25.5 %all_to_all.50 = bf16[8,16,1792]{2,1,0:T(8,128)(2,1)S(1)} all-to-all(bf16[8,16,1792]{2,1,0:T(8,128)(2,1)S(1)} %get-tuple-element.41), channel_id=1, replica_groups=mesh['ep_0'=8,'ep_1'=8,'ep_2'=2,'tp'=4] {'ep_0'}, dimensions={0} | all-to-all | bytes 917504 | tf_op jit(solution)/shard_map/all_to_all | solution.py:25
  27.7 16.2 %all_to_all.51 = bf16[16,2,128]{2,1,0:T(2,128)(2,1)S(1)} all-to-all(bf16[16,2,128]{2,1,0:T(2,128)(2,1)S(1)} %reshape.49), channel_id=1, replica_groups=mesh['ep_0'=8,'ep_1'=8,'ep_2'=2,'tp'=4] {'ep_1','ep_2'}, dimensions={0} | all-to-all | bytes 16384 | tf_op jit(solution)/shard_map/all_to_all | solution.py:25
  43.9 0.2 convolution_convert_fusion
  44.1 11.2 %all_to_all.52.came_ref = bf16[16,2,1280]{2,1,0:T(2,128)(2,1)S(1)} all-to-all(bf16[16,2,1280]{2,1,0:T(2,128)(2,1)S(1)} %reshape.53), channel_id=1, replica_groups=mesh['ep_0'=8,'ep_1'=8,'ep_2'=2,'tp'=4] {'ep_1','ep_2'}, dimensions={0} | all-to-all | bytes 163840 | tf_op jit(solution)/shard_map/all_to_all | solution.py:25
  55.3 0.0 copy-done.1
  55.3 1.5 %shard_map.177 = (bf16[16,2,512]{2,1,0:T(2,128)(2,1)S(1)}, f32[2,256,512]{2,1,0:T(8,128)}) custom-call(bf16[16,2,1280]{2,1,0:T(2,128)(2,1)S(1)} %all_to_all.52.came_ref, bf16[2,2048]{1,0:T(2,128)(2,1)S(1)} %get-tuple-element.32.res_ref, f32[1,256]{1,0:T(1,128)S(1)} %bitcast.38, f32[1,512]{1,0:T(1,128)S(1)} %bitcast.37, f32[2,256,512]{2,1,0:T(8,128)S(1)} %bitcast.30), custom_call_target="tpu_custom_call" | custom-call | tf_op jit(solution)/shard_map/pallas_call | solution.py:322
  56.8 0.0 copy-start
  56.8 10.0 %all_to_all.53 = bf16[16,2,512]{2,1,0:T(2,128)(2,1)S(1)} all-to-all(bf16[16,2,512]{2,1,0:T(2,128)(2,1)S(1)} %get-tuple-element.48), channel_id=1, replica_groups=mesh['ep_0'=8,'ep_1'=8,'ep_2'=2,'tp'=4] {'ep_1','ep_2'}, dimensions={0} | all-to-all | bytes 65536 | tf_op jit(solution)/shard_map/all_to_all | solution.py:25
  66.9 0.0 copy-start.4
  66.9 0.3 shard_map.178
  67.1 14.5 %all_to_all.54.came_ref = bf16[64,4,128]{2,1,0:T(4,128)(2,1)S(1)} all-to-all(bf16[64,4,128]{2,1,0:T(4,128)(2,1)S(1)} %shard_map.178), channel_id=1, replica_groups=mesh['ep_0'=8,'ep_1'=8,'ep_2'=2,'tp'=4] {'ep_1','ep_2','tp'}, dimensions={0} | all-to-all | bytes 131072 | tf_op jit(solution)/shard_map/all_to_all | solution.py:25
  81.7 0.0 copy-done
  81.7 0.0 copy-start.2
  81.7 0.4 shard_map.179
  82.1 10.4 %all_to_all.55 = bf16[8,32,256]{2,1,0:T(8,128)(2,1)S(1)} all-to-all(bf16[8,32,256]{2,1,0:T(8,128)(2,1)S(1)} %get-tuple-element.52), channel_id=1, replica_groups=mesh['ep_0'=8,'ep_1'=8,'ep_2'=2,'tp'=4] {'ep_0'}, dimensions={0} | all-to-all | bytes 262144 | tf_op jit(solution)/shard_map/all_to_all | solution.py:25
  92.5 9.5 %all_to_all.56.came_ref = bf16[8,16,256]{2,1,0:T(8,128)(2,1)S(1)} all-to-all(bf16[8,16,256]{2,1,0:T(8,128)(2,1)S(1)} %bitcast.40), channel_id=1, replica_groups=mesh['ep_0'=8,'ep_1'=8,'ep_2'=2,'tp'=4] {'tp','ep_2'}, dimensions={0} | all-to-all | bytes 131072 | tf_op jit(solution)/shard_map/all_to_all | solution.py:25
  102.1 0.0 copy-done.4
  102.1 0.0 copy-done.2
  102.1 0.0 copy-done.3
  102.1 0.7 shard_map.180
  102.7 8.0 %all_to_all.57 = bf16[8,16,256]{2,1,0:T(8,128)(2,1)S(1)} all-to-all(bf16[8,16,256]{2,1,0:T(8,128)(2,1)S(1)} %shard_map.180), channel_id=1, replica_groups=mesh['ep_0'=8,'ep_1'=8,'ep_2'=2,'tp'=4] {'tp','ep_2'}, dimensions={0} | all-to-all | bytes 131072 | tf_op jit(solution)/shard_map/all_to_all | solution.py:25
  110.8 0.2 convolution_convert_fusion.1
  111.0 15.3 %all_to_all.58 = bf16[64,4,256]{2,1,0:T(4,128)(2,1)S(1)} all-to-all(bf16[64,4,256]{2,1,0:T(4,128)(2,1)S(1)} %reshape.58), channel_id=1, replica_groups=mesh['ep_0'=8,'ep_1'=8,'ep_2'=2,'tp'=4] {'ep_0','ep_1'}, dimensions={0} | all-to-all | bytes 262144 | tf_op jit(solution)/shard_map/all_to_all | solution.py:25
  126.3 0.1 convert_reduce_fusion
  126.5 9.0 %all_to_all.59 = bf16[8,2,256]{2,1,0:T(2,128)(2,1)S(1)} all-to-all(bf16[8,2,256]{2,1,0:T(2,128)(2,1)S(1)} %bitcast.44), channel_id=1, replica_groups=mesh['ep_0'=8,'ep_1'=8,'ep_2'=2,'tp'=4] {'tp','ep_2'}, dimensions={0} | all-to-all | bytes 16384 | tf_op jit(solution)/shard_map/all_to_all | solution.py:25
  135.5 0.6 copy.28
  (14 shorter events, 0.2 us)
Async XLA Ops:
  1.8 53.6 %copy-start.1 = (f32[2,1,256,512]{3,2,1,0:T(8,128)S(1)}, f32[2,1,256,512]{3,2,1,0:T(8,128)}, u32[]{:S(2)}) copy-start(f32[2,1,256,512]{3,2,1,0:T(8,128)} %param.18) | copy-start | bytes 3145732
  56.8 24.9 %copy-start = (bf16[128,2048]{1,0:T(8,128)(2,1)S(1)}, bf16[128,2048]{1,0:T(8,128)(2,1)}, u32[]{:S(2)}) copy-start(bf16[128,2048]{1,0:T(8,128)(2,1)} %expert_ref.1) | copy-start | bytes 1572868
  66.9 35.2 %copy-start.4 = (bf16[1,128,2048]{2,1,0:T(8,128)(2,1)S(1)}, bf16[1,128,2048]{2,1,0:T(8,128)(2,1)}, u32[]{:S(2)}) copy-start(bf16[1,128,2048]{2,1,0:T(8,128)(2,1)} %param.33) | copy-start | bytes 1572868
  81.7 20.4 %copy-start.2 = (bf16[1,2048,128]{2,1,0:T(8,128)(2,1)S(1)}, bf16[1,2048,128]{2,1,0:T(8,128)(2,1)}, u32[]{:S(2)}) copy-start(bf16[1,2048,128]{2,1,0:T(8,128)(2,1)} %param.31) | copy-start | bytes 1572868
  81.7 20.4 %copy-start.3 = (bf16[1,2048,128]{2,1,0:T(8,128)(2,1)S(1)}, bf16[1,2048,128]{2,1,0:T(8,128)(2,1)}, u32[]{:S(2)}) copy-start(bf16[1,2048,128]{2,1,0:T(8,128)(2,1)} %param.32) | copy-start | bytes 1572868

commit v6 on v5

--- a/solution.py
+++ b/solution.py
@@ -8,6 +8,7 @@
 from jax.sharding import Mesh
 from jax.sharding import PartitionSpec as P
 
+
 CAP = 16
 EP = ("ep_0", "ep_1", "ep_2")
 FAR = ("ep_0", "ep_1")
@@ -40,9 +41,11 @@
     width = 0
     copies = []
     for source in weights:
-        place = spread.at[0, :, pl.ds(width, source.shape[1])]
+        for depth in range(spread.shape[0]):
+            place = spread.at[depth, :, pl.ds(width, source.shape[1])]
+            copies.append(pltpu.make_async_copy(source, place, sems.at[len(copies)]))
         width += source.shape[1]
-        copies.append(pltpu.make_async_copy(source, place, sems.at[len(copies)]))
+    spreads = len(copies)
     copies.append(pltpu.make_async_copy(ids_in, ids, sems.at[len(copies)]))
     for source, target in zip(sources[6:], kept, strict=True):
         copies.append(pltpu.make_async_copy(source, target, sems.at[len(copies)]))
@@ -53,7 +56,7 @@
     row = lax.broadcasted_iota(jnp.int32, (count, count), 0)
     col = lax.broadcasted_iota(jnp.int32, (count, count), 1)
     upper = jnp.where(row <= col, 1.0, 0.0).astype(BF16)
-    copies[5].wait()
+    copies[spreads].wait()
     one, two = ids[0:1, :], ids[1:2, :]
     spans = along.shape[0] // CAP
     cores = select.shape[0] // CAP
@@ -81,13 +84,21 @@
         others = jnp.where(core == c, total, others)
     lanes = lax.broadcasted_iota(jnp.int32, rival.shape, 1)
     rival[...] = jnp.where(lanes == others.astype(jnp.int32) - own, 1.0, 0.0)
-    for copy in copies[:5]:
+    for copy in copies[:spreads] + copies[spreads + 1 :]:
         copy.wait()
-    own_w = spread[0]
-    for depth in range(1, spread.shape[0]):
-        spread[depth] = own_w
-    for copy in copies[6:]:
-        copy.wait()
+
+
+def strips_of(place_of, slab, strip, rows_ref, gain_ref, lhs_ref, res_ref):
+    place = place_of()
+    width, held = rows_ref.shape[1], res_ref.shape[1]
+    feature = lax.broadcasted_iota(jnp.int32, (width, held), 0)
+    lane = lax.broadcasted_iota(jnp.int32, (width, held), 1)
+    taken = feature == lane // strip * (slab * strip) + place * strip + lane % strip
+    pick = jnp.where(taken, 1.0, 0.0).astype(BF16)
+    rows = rows_ref[...]
+    scaled = (rows.astype(F32) * gain_ref[...]).astype(BF16)
+    res_ref[...] = jnp.dot(rows, pick, preferred_element_type=F32).astype(BF16)
+    lhs_ref[...] = jnp.dot(scaled, pick, preferred_element_type=F32).astype(BF16)
 
 
 def advance(came_ref, res_ref, bias_ref, gain_ref, old_ref, out_ref, new_ref, held_ref, sems):
@@ -270,9 +281,6 @@
     in_width = 3 * key_width + value_width
     held = depths * strip
     piece = width // parts
-    place = lax.axis_index(SLAB)
-    chip = lax.axis_index(FAR)
-    core = lax.axis_index("ep_2")
 
     n_experts = router_expert.shape[0]
 
@@ -283,7 +291,7 @@
     vmem = pl.BlockSpec(memory_space=pltpu.VMEM)
     later = (residual_in, norm_gain, head_gain, ffn_gain, decay_bias, router_group.T)
     shapes = [
-        pltpu.VMEM((depths, strip, in_width + value_width), BF16),
+        jax.ShapeDtypeStruct((depths, strip, in_width + value_width), BF16),
         pltpu.VMEM((depths * cores * CAP, tokens), BF16),
         pltpu.VMEM((cores * CAP, tokens), BF16),
         pltpu.VMEM((CAP, n_experts), F32),
@@ -293,30 +301,34 @@
         functools.partial(prepare, experts_of),
         out_shape=shapes,
         in_specs=[pl.BlockSpec(memory_space=pl.ANY)] * 12,
-        out_specs=[vmem] * len(shapes),
+        out_specs=[pl.BlockSpec(memory_space=pl.ANY)] + [vmem] * (len(shapes) - 1),
         scratch_shapes=[
             pltpu.VMEM((expert_ids.shape[1], tokens), jnp.int32),
-            pltpu.SemaphoreType.DMA((12,)),
+            pltpu.SemaphoreType.DMA((5 * depths + 7,)),
         ],
     )(w_query, w_key, w_value, w_decay, w_output.T, expert_ids.T, *later)
     residual_in, norm_gain, head_gain, ffn_gain, decay_bias, group_rows = later
     head_gain = head_gain.astype(F32)[None]
     ffn_gain = ffn_gain.astype(F32)[None]
     decay_bias = decay_bias[None]
-    own_gain = norm_gain.reshape(depths, slab, strip)[:, place].reshape(held).astype(F32)
-    strips = residual_in.reshape(seqs, depths, slab, strip).transpose(2, 0, 1, 3)
-    strips = strips.reshape(slab, seqs, held)
+    norm_gain = norm_gain.astype(F32)[None]
 
     tied = lax.optimization_barrier(
-        (spread, strips, along, select, rival_lane, own_gain)
+        (spread, residual_in, along, select, rival_lane, norm_gain)
         + (head_gain, ffn_gain, decay_bias)
     )
-    spread, strips, along, select, rival_lane, own_gain, *tied = tied
+    spread, residual_in, along, select, rival_lane, norm_gain, *tied = tied
     head_gain, ffn_gain, decay_bias = tied
-    gathered = exchange(spread, "ep_0").reshape(held, in_width + value_width)
-    gathered, strips = lax.optimization_barrier((gathered, strips))
-    slab_res = exchange(strips, SLAB).reshape(slab * seqs, held)
-    lhs = (slab_res.astype(F32) * own_gain).astype(BF16)
+    gathered = exchange(spread, "ep_0")
+    rows_in = lax.all_gather(residual_in, SLAB, axis=0, tiled=True)
+    lhs, slab_res = pl.pallas_call(
+        functools.partial(strips_of, lambda: lax.axis_index(SLAB), slab, strip),
+        out_shape=[pltpu.VMEM((slab * seqs, held), BF16)] * 2,
+        in_specs=[vmem] * 2,
+        out_specs=[vmem] * 2,
+    )(on_chip(rows_in), on_chip(norm_gain))
+    gathered, lhs, slab_res = lax.optimization_barrier((gathered, lhs, slab_res))
+    gathered = gathered.reshape(held, in_width + value_width)
     sums = jnp.dot(lhs, gathered[:, :in_width], preferred_element_type=F32).astype(BF16)
     arrived = exchange(sums.reshape(slab, seqs, in_width), SLAB)
     gated, new_state = pl.pallas_call(

time: 137 us -> 145 us (1.058)
  blocking collectives: 130 us -> 113 us
  Pallas kernels: 3.9 us -> 18.6 us
  starting transfers between devices: 0 us -> 11 us
    all_to_all x10 -> x8, blocking collectives: 130 us -> 93.8 us  [exchange(): came = lax.all_to_all(blocks, axes, split_axis=0, concat_axis=0, tiled=True)]
    all_gather x0 -> x1, blocking collectives: none -> 18.7 us  [on_device(): rows_in = lax.all_gather(residual_in, SLAB, axis=0, tiled=True)]
    pallas_call x1, Pallas kernels: 1.15 us -> 15.4 us  [on_device(): pl.pallas_call(functools.partial(prepare, experts_of), out_shape=shapes,...]
    all_to_all x0 -> x1, starting transfers between devices: none -> 11 us  [exchange(): came = lax.all_to_all(blocks, axes, split_axis=0, concat_axis=0, tiled=True)]
  transfers between devices with their start and end apart: 0 -> 1, of which waited for: 0 -> 0; matrix products, arithmetic and copies ran while one was open for 0% -> 0% of each run, Pallas kernels for 0% -> 0%
where the time goes in v6:
time: 145 us; the launch traced here: 144 us
  blocking collectives  113 us (78%)
  Pallas kernels  18.6 us (13%)
  starting transfers between devices  11 us (8%)
    all_to_all x8, blocking collectives, exchange(): came = lax.all_to_all(blocks, axes, split_axis=0, concat_axis=0, tiled=True)  93.8 us
    all_gather x1, blocking collectives, on_device(): rows_in = lax.all_gather(residual_in, SLAB, axis=0, tiled=True)  18.7 us
    pallas_call x1, Pallas kernels, on_device(): pl.pallas_call(functools.partial(prepare, experts_of), out_shape=shapes,...  15.4 us
    all_to_all x1, starting transfers between devices, exchange(): came = lax.all_to_all(blocks, axes, split_axis=0, concat_axis=0, tiled=True)  11 us
  transfers between devices with their start and end apart: 1, of which 0 were waited for; matrix products, arithmetic and copies ran while one was open for 0% of the time, Pallas kernels for 0%

profile of v6, /device:TPU:1, one launch (start us, length us, event | category | flops | bytes accessed | tf_op | source)
XLA Modules:
  0.0 144.2 jit_solution(10590845218977572227)
XLA Ops:
  0.6 15.4 %shard_map.176 = (bf16[8,16,1792]{2,1,0:T(8,128)(2,1)}, bf16[256,256]{1,0:T(8,128)(2,1)S(1)}, bf16[32,256]{1,0:T(8,128)(2,1)S(1)}, f32[16,128]{1,0:T(8,128)S(1)}...) custom-call(bf16[16,256]{1,0:T(8,128)(2,1)} %refs_0_.1, ...), custom_call_target="tpu_custom_call" | custom-call | tf_op jit(solution)/shard_map/pallas_call | solution.py:300
  16.1 0.0 copy-start.1
  16.1 11.0 %all-to-all-start = ((bf16[8,16,1792]{2,1,0:T(8,128)(2,1)}), bf16[8,16,1792]{2,1,0:T(8,128)(2,1)S(1)}, u32[]{:S(2)}, u32[]{:S(2)}) async-start(bf16[8,16,1792]{2,1,0:T(8,128)(2,1)} %get-tuple-element.44), calls=%async_computation | async-start | bytes 917504 | tf_op jit(solution)/shard_map/all_to_all | solution.py:26
  27.1 18.7 %all-gather = bf16[16,2,2048]{2,1,0:T(2,128)(2,1)S(1)} all-gather(bf16[1,2,2048]{2,1,0:T(2,128)(2,1)S(1)} %bitcast.35), channel_id=1, replica_groups=mesh['ep_0'=8,'ep_1'=8,'ep_2'=2,'tp'=4] {'ep_1','ep_2'}, dimensions={0}, use_global_device_ids=true | all-gather | bytes 139264 | tf_op jit(solution)/shard_map/all_gather | solution.py:323
  45.8 0.1 reshape.46.rows_ref
  45.9 0.4 shard_map.177
  46.3 0.0 all-to-all-done
  46.3 0.2 convolution_convert_fusion
  46.5 12.9 %all_to_all.45.came_ref = bf16[16,2,1280]{2,1,0:T(2,128)(2,1)S(1)} all-to-all(bf16[16,2,1280]{2,1,0:T(2,128)(2,1)S(1)} %reshape.34), channel_id=1, replica_groups=mesh['ep_0'=8,'ep_1'=8,'ep_2'=2,'tp'=4] {'ep_1','ep_2'}, dimensions={0} | all-to-all | bytes 163840 | tf_op jit(solution)/shard_map/all_to_all | solution.py:26
  59.4 0.0 copy-done.1
  59.4 1.5 %shard_map.178 = (bf16[16,2,512]{2,1,0:T(2,128)(2,1)S(1)}, f32[2,256,512]{2,1,0:T(8,128)}) custom-call(bf16[16,2,1280]{2,1,0:T(2,128)(2,1)S(1)} %all_to_all.45.came_ref, bf16[2,2048]{1,0:T(2,128)(2,1)S(1)} %get-tuple-element.45.res_ref, f32[1,256]{1,0:T(1,128)S(1)} %bitcast.37, f32[1,512]{1,0:T(1,128)S(1)} %bitcast.36, f32[2,256,512]{2,1,0:T(8,128)S(1)} %bitcast.29), custom_call_target="tpu_custom_call" | custom-call | tf_op jit(solution)/shard_map/pallas_call | solution.py:334
  60.9 0.0 copy-start
  60.9 10.0 %all_to_all.46 = bf16[16,2,512]{2,1,0:T(2,128)(2,1)S(1)} all-to-all(bf16[16,2,512]{2,1,0:T(2,128)(2,1)S(1)} %get-tuple-element.53), channel_id=1, replica_groups=mesh['ep_0'=8,'ep_1'=8,'ep_2'=2,'tp'=4] {'ep_1','ep_2'}, dimensions={0} | all-to-all | bytes 65536 | tf_op jit(solution)/shard_map/all_to_all | solution.py:26
  70.9 0.0 copy-start.4
  70.9 0.3 shard_map.179
  71.2 14.5 %all_to_all.47.came_ref = bf16[64,4,128]{2,1,0:T(4,128)(2,1)S(1)} all-to-all(bf16[64,4,128]{2,1,0:T(4,128)(2,1)S(1)} %shard_map.179), channel_id=1, replica_groups=mesh['ep_0'=8,'ep_1'=8,'ep_2'=2,'tp'=4] {'ep_1','ep_2','tp'}, dimensions={0} | all-to-all | bytes 131072 | tf_op jit(solution)/shard_map/all_to_all | solution.py:26
  85.7 0.0 copy-done
  85.7 0.0 copy-start.2
  85.7 0.0 copy-start.3
  85.7 0.4 shard_map.180
  86.1 14.2 %all_to_all.48 = bf16[8,32,256]{2,1,0:T(8,128)(2,1)S(1)} all-to-all(bf16[8,32,256]{2,1,0:T(8,128)(2,1)S(1)} %get-tuple-element.58), channel_id=1, replica_groups=mesh['ep_0'=8,'ep_1'=8,'ep_2'=2,'tp'=4] {'ep_0'}, dimensions={0} | all-to-all | bytes 262144 | tf_op jit(solution)/shard_map/all_to_all | solution.py:26
  100.3 9.9 %all_to_all.49.came_ref = bf16[8,16,256]{2,1,0:T(8,128)(2,1)S(1)} all-to-all(bf16[8,16,256]{2,1,0:T(8,128)(2,1)S(1)} %bitcast.39), channel_id=1, replica_groups=mesh['ep_0'=8,'ep_1'=8,'ep_2'=2,'tp'=4] {'tp','ep_2'}, dimensions={0} | all-to-all | bytes 131072 | tf_op jit(solution)/shard_map/all_to_all | solution.py:26
  110.2 0.0 copy-done.4
  110.2 0.0 copy-done.2
  110.2 0.0 copy-done.3
  110.2 0.7 shard_map.181
  110.9 8.0 %all_to_all.50 = bf16[8,16,256]{2,1,0:T(8,128)(2,1)S(1)} all-to-all(bf16[8,16,256]{2,1,0:T(8,128)(2,1)S(1)} %shard_map.181), channel_id=1, replica_groups=mesh['ep_0'=8,'ep_1'=8,'ep_2'=2,'tp'=4] {'tp','ep_2'}, dimensions={0} | all-to-all | bytes 131072 | tf_op jit(solution)/shard_map/all_to_all | solution.py:26
  118.9 0.2 convolution_convert_fusion.1
  119.2 15.3 %all_to_all.51 = bf16[64,4,256]{2,1,0:T(4,128)(2,1)S(1)} all-to-all(bf16[64,4,256]{2,1,0:T(4,128)(2,1)S(1)} %reshape.39), channel_id=1, replica_groups=mesh['ep_0'=8,'ep_1'=8,'ep_2'=2,'tp'=4] {'ep_0','ep_1'}, dimensions={0} | all-to-all | bytes 262144 | tf_op jit(solution)/shard_map/all_to_all | solution.py:26
  134.5 0.1 convert_reduce_fusion
  134.6 9.0 %all_to_all.52 = bf16[8,2,256]{2,1,0:T(2,128)(2,1)S(1)} all-to-all(bf16[8,2,256]{2,1,0:T(2,128)(2,1)S(1)} %bitcast.42), channel_id=1, replica_groups=mesh['ep_0'=8,'ep_1'=8,'ep_2'=2,'tp'=4] {'tp','ep_2'}, dimensions={0} | all-to-all | bytes 16384 | tf_op jit(solution)/shard_map/all_to_all | solution.py:26
  143.6 0.6 copy.23
  (12 shorter events, 0.2 us)
Async XLA Ops:
  16.1 43.3 %copy-start.1 = (f32[2,1,256,512]{3,2,1,0:T(8,128)S(1)}, f32[2,1,256,512]{3,2,1,0:T(8,128)}, u32[]{:S(2)}) copy-start(f32[2,1,256,512]{3,2,1,0:T(8,128)} %param.18) | copy-start | bytes 3145732
  16.1 30.2 %all-to-all-start = ((bf16[8,16,1792]{2,1,0:T(8,128)(2,1)}), bf16[8,16,1792]{2,1,0:T(8,128)(2,1)S(1)}, u32[]{:S(2)}, u32[]{:S(2)}) async-start(bf16[8,16,1792]{2,1,0:T(8,128)(2,1)} %get-tuple-element.44), calls=%async_computation | async-start | bytes 917504 | tf_op jit(solution)/shard_map/all_to_all | solution.py:26
  60.9 24.8 %copy-start = (bf16[128,2048]{1,0:T(8,128)(2,1)S(1)}, bf16[128,2048]{1,0:T(8,128)(2,1)}, u32[]{:S(2)}) copy-start(bf16[128,2048]{1,0:T(8,128)(2,1)} %expert_ref.1) | copy-start | bytes 1572868
  70.9 39.3 %copy-start.4 = (bf16[1,128,2048]{2,1,0:T(8,128)(2,1)S(1)}, bf16[1,128,2048]{2,1,0:T(8,128)(2,1)}, u32[]{:S(2)}) copy-start(bf16[1,128,2048]{2,1,0:T(8,128)(2,1)} %param.33) | copy-start | bytes 1572868
  85.7 24.5 %copy-start.2 = (bf16[1,2048,128]{2,1,0:T(8,128)(2,1)S(1)}, bf16[1,2048,128]{2,1,0:T(8,128)(2,1)}, u32[]{:S(2)}) copy-start(bf16[1,2048,128]{2,1,0:T(8,128)(2,1)} %param.31) | copy-start | bytes 1572868
  85.7 24.5 %copy-start.3 = (bf16[1,2048,128]{2,1,0:T(8,128)(2,1)S(1)}, bf16[1,2048,128]{2,1,0:T(8,128)(2,1)}, u32[]{:S(2)}) copy-start(bf16[1,2048,128]{2,1,0:T(8,128)(2,1)} %param.32) | copy-start | bytes 1572868

commit v7 on v6

--- a/solution.py
+++ b/solution.py
@@ -36,16 +36,16 @@
 
 
 def prepare(experts_of, *refs):
-    sources, (spread, along, select, rival, *kept), (ids, sems) = refs[:12], refs[12:-2], refs[-2:]
+    sources, (spread, along, select, rival, *kept) = refs[:12], refs[12:-3]
+    own_w, ids, sems = refs[-3:]
     *weights, ids_in = sources[:6]
     width = 0
     copies = []
     for source in weights:
-        for depth in range(spread.shape[0]):
-            place = spread.at[depth, :, pl.ds(width, source.shape[1])]
-            copies.append(pltpu.make_async_copy(source, place, sems.at[len(copies)]))
+        place = own_w.at[:, pl.ds(width, source.shape[1])]
+        copies.append(pltpu.make_async_copy(source, place, sems.at[len(copies)]))
         width += source.shape[1]
-    spreads = len(copies)
+    fetched = len(copies)
     copies.append(pltpu.make_async_copy(ids_in, ids, sems.at[len(copies)]))
     for source, target in zip(sources[6:], kept, strict=True):
         copies.append(pltpu.make_async_copy(source, target, sems.at[len(copies)]))
@@ -56,7 +56,14 @@
     row = lax.broadcasted_iota(jnp.int32, (count, count), 0)
     col = lax.broadcasted_iota(jnp.int32, (count, count), 1)
     upper = jnp.where(row <= col, 1.0, 0.0).astype(BF16)
-    copies[spreads].wait()
+    for copy in copies[:fetched]:
+        copy.wait()
+    spreads = []
+    for depth in range(spread.shape[0]):
+        sem = sems.at[len(copies) + depth]
+        spreads.append(pltpu.make_async_copy(own_w, spread.at[depth], sem))
+        spreads[-1].start()
+    copies[fetched].wait()
     one, two = ids[0:1, :], ids[1:2, :]
     spans = along.shape[0] // CAP
     cores = select.shape[0] // CAP
@@ -84,7 +91,7 @@
         others = jnp.where(core == c, total, others)
     lanes = lax.broadcasted_iota(jnp.int32, rival.shape, 1)
     rival[...] = jnp.where(lanes == others.astype(jnp.int32) - own, 1.0, 0.0)
-    for copy in copies[:spreads] + copies[spreads + 1 :]:
+    for copy in copies[fetched + 1 :] + spreads:
         copy.wait()
 
 
@@ -103,9 +110,10 @@
 
 def advance(came_ref, res_ref, bias_ref, gain_ref, old_ref, out_ref, new_ref, held_ref, sems):
     seqs, key_width, value_width = old_ref.shape
-    total = came_ref[0].astype(F32)
-    for at in range(1, came_ref.shape[0]):
-        total = total + came_ref[at].astype(F32)
+    count = came_ref.shape[0]
+    seq_of = lax.broadcasted_iota(jnp.int32, (8, count), 1) % seqs
+    pick = jnp.where(seq_of == lax.broadcasted_iota(jnp.int32, (8, count), 0), 1.0, 0.0)
+    total = jnp.dot(pick.astype(BF16), came_ref[...], preferred_element_type=F32)[:seqs]
     res = res_ref[...].astype(F32)
     total = total * lax.rsqrt(jnp.mean(res * res, axis=1, keepdims=True) + EPSILON)
     query = total[:, :key_width].astype(BF16).astype(F32) * key_width ** (-0.5)
@@ -117,7 +125,7 @@
     copies = []
     gated = []
     for seq in range(seqs):
-        read = jnp.zeros((1, value_width), F32)
+        read = jnp.zeros((8, value_width), F32)
         for at in range(0, key_width, 32):
             block = down[at : at + 32]
             query_col = block[:, seq : seq + 1]
@@ -133,7 +141,8 @@
                     )
                 )
                 copies[-1].start()
-            read = read + jnp.sum(query_col * new, axis=0, keepdims=True)
+            read = read + jnp.sum((query_col * new).reshape(4, 8, value_width), axis=0)
+        read = jnp.sum(read, axis=0, keepdims=True)
         mean = jnp.mean(read * read, axis=1, keepdims=True)
         gated.append(read * lax.rsqrt(mean + EPSILON) * gain_ref[...])
     gated = jnp.concatenate(gated, axis=0).astype(BF16)
@@ -303,8 +312,9 @@
         in_specs=[pl.BlockSpec(memory_space=pl.ANY)] * 12,
         out_specs=[pl.BlockSpec(memory_space=pl.ANY)] + [vmem] * (len(shapes) - 1),
         scratch_shapes=[
+            pltpu.VMEM((strip, in_width + value_width), BF16),
             pltpu.VMEM((expert_ids.shape[1], tokens), jnp.int32),
-            pltpu.SemaphoreType.DMA((5 * depths + 7,)),
+            pltpu.SemaphoreType.DMA((12 + depths,)),
         ],
     )(w_query, w_key, w_value, w_decay, w_output.T, expert_ids.T, *later)
     residual_in, norm_gain, head_gain, ffn_gain, decay_bias, group_rows = later
@@ -343,7 +353,7 @@
             pltpu.VMEM((seqs, key_width, value_width), F32),
             pltpu.SemaphoreType.DMA((seqs * key_width // 64,)),
         ],
-    )(*map(on_chip, (arrived, residual_in, decay_bias, head_gain, gla_state[:, 0])))
+    )(*map(on_chip, (arrived.reshape(slab * seqs, in_width), residual_in, decay_bias, head_gain, gla_state[:, 0])))
 
     slab_heads, slab_res = exchange(gated, SLAB, slab_res)
     slab_heads = slab_heads.reshape(slab * seqs, value_width)

time: 145 us -> 131 us (0.903)
  Pallas kernels: 18.6 us -> 4.92 us
    pallas_call x1, Pallas kernels: 15.4 us -> 1.72 us  [on_device(): pl.pallas_call(functools.partial(prepare, experts_of), out_shape=shapes,...]
where the time goes in v7:
time: 131 us
  blocking collectives  113 us (86%)
  starting transfers between devices  11 us (8%)
  Pallas kernels  4.92 us (4%)
    all_to_all x8, blocking collectives, exchange(): came = lax.all_to_all(blocks, axes, split_axis=0, concat_axis=0, tiled=True)  93.8 us
    all_gather x1, blocking collectives, on_device(): rows_in = lax.all_gather(residual_in, SLAB, axis=0, tiled=True)  18.7 us
    all_to_all x1, starting transfers between devices, exchange(): came = lax.all_to_all(blocks, axes, split_axis=0, concat_axis=0, tiled=True)  11 us
  transfers between devices with their start and end apart: 1, of which 0 were waited for; matrix products, arithmetic and copies ran while one was open for 0% of the time, Pallas kernels for 0%

profile of v7, /device:TPU:1, one launch (start us, length us, event | category | flops | bytes accessed | tf_op | source)
XLA Modules:
  0.0 130.6 jit_solution(17462281959782726121)
XLA Ops:
  0.6 1.7 %shard_map.176 = (bf16[8,16,1792]{2,1,0:T(8,128)(2,1)}, bf16[256,256]{1,0:T(8,128)(2,1)S(1)}, bf16[32,256]{1,0:T(8,128)(2,1)S(1)}, f32[16,128]{1,0:T(8,128)S(1)}...) custom-call(bf16[16,256]{1,0:T(8,128)(2,1)} %refs_0_.1, ...), custom_call_target="tpu_custom_call" | custom-call | tf_op jit(solution)/shard_map/pallas_call | solution.py:309
  2.4 0.0 copy-start.1
  2.4 11.0 %all-to-all-start = ((bf16[8,16,1792]{2,1,0:T(8,128)(2,1)}), bf16[8,16,1792]{2,1,0:T(8,128)(2,1)S(1)}, u32[]{:S(2)}, u32[]{:S(2)}) async-start(bf16[8,16,1792]{2,1,0:T(8,128)(2,1)} %get-tuple-element.44), calls=%async_computation | async-start | bytes 917504 | tf_op jit(solution)/shard_map/all_to_all | solution.py:26
  13.4 18.7 %all-gather = bf16[16,2,2048]{2,1,0:T(2,128)(2,1)S(1)} all-gather(bf16[1,2,2048]{2,1,0:T(2,128)(2,1)S(1)} %bitcast.35), channel_id=1, replica_groups=mesh['ep_0'=8,'ep_1'=8,'ep_2'=2,'tp'=4] {'ep_1','ep_2'}, dimensions={0}, use_global_device_ids=true | all-gather | bytes 139264 | tf_op jit(solution)/shard_map/all_gather | solution.py:333
  32.1 0.1 reshape.50.rows_ref
  32.2 0.4 shard_map.177
  32.6 0.0 all-to-all-done
  32.6 0.2 convolution_convert_fusion
  32.8 12.9 %all_to_all.45 = bf16[16,2,1280]{2,1,0:T(2,128)(2,1)S(1)} all-to-all(bf16[16,2,1280]{2,1,0:T(2,128)(2,1)S(1)} %reshape.37), channel_id=1, replica_groups=mesh['ep_0'=8,'ep_1'=8,'ep_2'=2,'tp'=4] {'ep_1','ep_2'}, dimensions={0} | all-to-all | bytes 163840 | tf_op jit(solution)/shard_map/all_to_all | solution.py:26
  45.7 0.0 copy-done.1
  45.7 1.5 %shard_map.178 = (bf16[16,2,512]{2,1,0:T(2,128)(2,1)S(1)}, f32[2,256,512]{2,1,0:T(8,128)}) custom-call(bf16[32,1280]{1,0:T(8,128)(2,1)S(1)} %reshape.38.came_ref, bf16[2,2048]{1,0:T(2,128)(2,1)S(1)} %get-tuple-element.45.res_ref, f32[1,256]{1,0:T(1,128)S(1)} %bitcast.37, f32[1,512]{1,0:T(1,128)S(1)} %bitcast.36, f32[2,256,512]{2,1,0:T(8,128)S(1)} %bitcast.29), custom_call_target="tpu_custom_call" | custom-call | tf_op jit(solution)/shard_map/pallas_call | solution.py:344
  47.3 0.0 copy-start
  47.3 10.0 %all_to_all.46 = bf16[16,2,512]{2,1,0:T(2,128)(2,1)S(1)} all-to-all(bf16[16,2,512]{2,1,0:T(2,128)(2,1)S(1)} %get-tuple-element.53), channel_id=1, replica_groups=mesh['ep_0'=8,'ep_1'=8,'ep_2'=2,'tp'=4] {'ep_1','ep_2'}, dimensions={0} | all-to-all | bytes 65536 | tf_op jit(solution)/shard_map/all_to_all | solution.py:26
  57.3 0.0 copy-start.4
  57.3 0.3 shard_map.179
  57.6 14.5 %all_to_all.47.came_ref = bf16[64,4,128]{2,1,0:T(4,128)(2,1)S(1)} all-to-all(bf16[64,4,128]{2,1,0:T(4,128)(2,1)S(1)} %shard_map.179), channel_id=1, replica_groups=mesh['ep_0'=8,'ep_1'=8,'ep_2'=2,'tp'=4] {'ep_1','ep_2','tp'}, dimensions={0} | all-to-all | bytes 131072 | tf_op jit(solution)/shard_map/all_to_all | solution.py:26
  72.1 0.0 copy-done
  72.1 0.0 copy-start.2
  72.1 0.0 copy-start.3
  72.1 0.4 shard_map.180
  72.5 14.2 %all_to_all.48 = bf16[8,32,256]{2,1,0:T(8,128)(2,1)S(1)} all-to-all(bf16[8,32,256]{2,1,0:T(8,128)(2,1)S(1)} %get-tuple-element.58), channel_id=1, replica_groups=mesh['ep_0'=8,'ep_1'=8,'ep_2'=2,'tp'=4] {'ep_0'}, dimensions={0} | all-to-all | bytes 262144 | tf_op jit(solution)/shard_map/all_to_all | solution.py:26
  86.7 9.9 %all_to_all.49.came_ref = bf16[8,16,256]{2,1,0:T(8,128)(2,1)S(1)} all-to-all(bf16[8,16,256]{2,1,0:T(8,128)(2,1)S(1)} %bitcast.39), channel_id=1, replica_groups=mesh['ep_0'=8,'ep_1'=8,'ep_2'=2,'tp'=4] {'tp','ep_2'}, dimensions={0} | all-to-all | bytes 131072 | tf_op jit(solution)/shard_map/all_to_all | solution.py:26
  96.6 0.0 copy-done.4
  96.6 0.0 copy-done.2
  96.6 0.0 copy-done.3
  96.6 0.7 shard_map.181
  97.3 8.0 %all_to_all.50 = bf16[8,16,256]{2,1,0:T(8,128)(2,1)S(1)} all-to-all(bf16[8,16,256]{2,1,0:T(8,128)(2,1)S(1)} %shard_map.181), channel_id=1, replica_groups=mesh['ep_0'=8,'ep_1'=8,'ep_2'=2,'tp'=4] {'tp','ep_2'}, dimensions={0} | all-to-all | bytes 131072 | tf_op jit(solution)/shard_map/all_to_all | solution.py:26
  105.3 0.2 convolution_convert_fusion.1
  105.5 15.3 %all_to_all.51 = bf16[64,4,256]{2,1,0:T(4,128)(2,1)S(1)} all-to-all(bf16[64,4,256]{2,1,0:T(4,128)(2,1)S(1)} %reshape.43), channel_id=1, replica_groups=mesh['ep_0'=8,'ep_1'=8,'ep_2'=2,'tp'=4] {'ep_0','ep_1'}, dimensions={0} | all-to-all | bytes 262144 | tf_op jit(solution)/shard_map/all_to_all | solution.py:26
  120.9 0.1 convert_reduce_fusion
  121.0 9.0 %all_to_all.52 = bf16[8,2,256]{2,1,0:T(2,128)(2,1)S(1)} all-to-all(bf16[8,2,256]{2,1,0:T(2,128)(2,1)S(1)} %bitcast.42), channel_id=1, replica_groups=mesh['ep_0'=8,'ep_1'=8,'ep_2'=2,'tp'=4] {'tp','ep_2'}, dimensions={0} | all-to-all | bytes 16384 | tf_op jit(solution)/shard_map/all_to_all | solution.py:26
  130.0 0.6 copy.23
  (13 shorter events, 0.2 us)
Async XLA Ops:
  2.4 43.3 %copy-start.1 = (f32[2,1,256,512]{3,2,1,0:T(8,128)S(1)}, f32[2,1,256,512]{3,2,1,0:T(8,128)}, u32[]{:S(2)}) copy-start(f32[2,1,256,512]{3,2,1,0:T(8,128)} %param.18) | copy-start | bytes 3145732
  2.4 30.2 %all-to-all-start = ((bf16[8,16,1792]{2,1,0:T(8,128)(2,1)}), bf16[8,16,1792]{2,1,0:T(8,128)(2,1)S(1)}, u32[]{:S(2)}, u32[]{:S(2)}) async-start(bf16[8,16,1792]{2,1,0:T(8,128)(2,1)} %get-tuple-element.44), calls=%async_computation | async-start | bytes 917504 | tf_op jit(solution)/shard_map/all_to_all | solution.py:26
  47.3 24.8 %copy-start = (bf16[128,2048]{1,0:T(8,128)(2,1)S(1)}, bf16[128,2048]{1,0:T(8,128)(2,1)}, u32[]{:S(2)}) copy-start(bf16[128,2048]{1,0:T(8,128)(2,1)} %expert_ref.1) | copy-start | bytes 1572868
  57.3 39.3 %copy-start.4 = (bf16[1,128,2048]{2,1,0:T(8,128)(2,1)S(1)}, bf16[1,128,2048]{2,1,0:T(8,128)(2,1)}, u32[]{:S(2)}) copy-start(bf16[1,128,2048]{2,1,0:T(8,128)(2,1)} %param.33) | copy-start | bytes 1572868
  72.1 24.5 %copy-start.2 = (bf16[1,2048,128]{2,1,0:T(8,128)(2,1)S(1)}, bf16[1,2048,128]{2,1,0:T(8,128)(2,1)}, u32[]{:S(2)}) copy-start(bf16[1,2048,128]{2,1,0:T(8,128)(2,1)} %param.31) | copy-start | bytes 1572868
  72.1 24.5 %copy-start.3 = (bf16[1,2048,128]{2,1,0:T(8,128)(2,1)S(1)}, bf16[1,2048,128]{2,1,0:T(8,128)(2,1)}, u32[]{:S(2)}) copy-start(bf16[1,2048,128]{2,1,0:T(8,128)(2,1)} %param.32) | copy-start | bytes 1572868

commit v8 on v7

--- a/solution.py
+++ b/solution.py
@@ -35,8 +35,8 @@
     return jnp.broadcast_to(shard[None], (count, *shard.shape))
 
 
-def prepare(experts_of, *refs):
-    sources, (spread, along, select, rival, *kept) = refs[:12], refs[12:-3]
+def prepare(experts_of, strip, *refs):
+    sources, (spread, pick, along, select, rival, *kept) = refs[:12], refs[12:-3]
     own_w, ids, sems = refs[-3:]
     *weights, ids_in = sources[:6]
     width = 0
@@ -56,6 +56,13 @@
     row = lax.broadcasted_iota(jnp.int32, (count, count), 0)
     col = lax.broadcasted_iota(jnp.int32, (count, count), 1)
     upper = jnp.where(row <= col, 1.0, 0.0).astype(BF16)
+    feature = lax.broadcasted_iota(jnp.int32, (pick.shape[0] // spread.shape[0], 128), 0)
+    lane = lax.broadcasted_iota(jnp.int32, feature.shape, 1)
+    within = feature - place * strip == lane % strip
+    for depth in range(spread.shape[0]):
+        taken = within & (lane // strip == depth)
+        at = feature.shape[0] * depth
+        pick[at : at + feature.shape[0]] = jnp.where(taken, 1.0, 0.0).astype(BF16)
     for copy in copies[:fetched]:
         copy.wait()
     spreads = []
@@ -95,14 +102,9 @@
         copy.wait()
 
 
-def strips_of(place_of, slab, strip, rows_ref, gain_ref, lhs_ref, res_ref):
-    place = place_of()
-    width, held = rows_ref.shape[1], res_ref.shape[1]
-    feature = lax.broadcasted_iota(jnp.int32, (width, held), 0)
-    lane = lax.broadcasted_iota(jnp.int32, (width, held), 1)
-    taken = feature == lane // strip * (slab * strip) + place * strip + lane % strip
-    pick = jnp.where(taken, 1.0, 0.0).astype(BF16)
+def strips_of(rows_ref, gain_ref, pick_ref, lhs_ref, res_ref):
     rows = rows_ref[...]
+    pick = pick_ref[...]
     scaled = (rows.astype(F32) * gain_ref[...]).astype(BF16)
     res_ref[...] = jnp.dot(rows, pick, preferred_element_type=F32).astype(BF16)
     lhs_ref[...] = jnp.dot(scaled, pick, preferred_element_type=F32).astype(BF16)
@@ -125,23 +127,21 @@
     copies = []
     gated = []
     for seq in range(seqs):
+        for at in range(0, key_width, 64):
+            rows = slice(at, at + 64)
+            key_col = down[rows, seqs + seq : seqs + seq + 1]
+            alpha_col = down[rows, 2 * seqs + seq : 2 * seqs + seq + 1]
+            new = alpha_col * old_ref[seq, rows] + key_col * value[seq : seq + 1]
+            held_ref[seq, rows] = new
+            source, target = held_ref.at[seq, pl.ds(at, 64)], new_ref.at[seq, pl.ds(at, 64)]
+            copies.append(pltpu.make_async_copy(source, target, sems.at[len(copies)]))
+            copies[-1].start()
+    for seq in range(seqs):
         read = jnp.zeros((8, value_width), F32)
-        for at in range(0, key_width, 32):
-            block = down[at : at + 32]
-            query_col = block[:, seq : seq + 1]
-            key_col = block[:, seqs + seq : seqs + seq + 1]
-            alpha_col = block[:, 2 * seqs + seq : 2 * seqs + seq + 1]
-            new = alpha_col * old_ref[seq, at : at + 32] + key_col * value[seq : seq + 1]
-            held_ref[seq, at : at + 32] = new
-            if at % 64:
-                rows = pl.ds(at - 32, 64)
-                copies.append(
-                    pltpu.make_async_copy(
-                        held_ref.at[seq, rows], new_ref.at[seq, rows], sems.at[len(copies)]
-                    )
-                )
-                copies[-1].start()
-            read = read + jnp.sum((query_col * new).reshape(4, 8, value_width), axis=0)
+        for at in range(0, key_width, 64):
+            rows = slice(at, at + 64)
+            part = down[rows, seq : seq + 1] * held_ref[seq, rows]
+            read = read + jnp.sum(part.reshape(8, 8, value_width), axis=0)
         read = jnp.sum(read, axis=0, keepdims=True)
         mean = jnp.mean(read * read, axis=1, keepdims=True)
         gated.append(read * lax.rsqrt(mean + EPSILON) * gain_ref[...])
@@ -301,13 +301,14 @@
     later = (residual_in, norm_gain, head_gain, ffn_gain, decay_bias, router_group.T)
     shapes = [
         jax.ShapeDtypeStruct((depths, strip, in_width + value_width), BF16),
+        pltpu.VMEM((width, held), BF16),
         pltpu.VMEM((depths * cores * CAP, tokens), BF16),
         pltpu.VMEM((cores * CAP, tokens), BF16),
         pltpu.VMEM((CAP, n_experts), F32),
         *(pltpu.VMEM(a.shape, a.dtype) for a in later),
     ]
-    spread, along, select, rival_lane, *later = pl.pallas_call(
-        functools.partial(prepare, experts_of),
+    spread, pick, along, select, rival_lane, *later = pl.pallas_call(
+        functools.partial(prepare, experts_of, strip),
         out_shape=shapes,
         in_specs=[pl.BlockSpec(memory_space=pl.ANY)] * 12,
         out_specs=[pl.BlockSpec(memory_space=pl.ANY)] + [vmem] * (len(shapes) - 1),
@@ -324,19 +325,19 @@
     norm_gain = norm_gain.astype(F32)[None]
 
     tied = lax.optimization_barrier(
-        (spread, residual_in, along, select, rival_lane, norm_gain)
+        (spread, residual_in, pick, along, select, rival_lane, norm_gain)
         + (head_gain, ffn_gain, decay_bias)
     )
-    spread, residual_in, along, select, rival_lane, norm_gain, *tied = tied
+    spread, residual_in, pick, along, select, rival_lane, norm_gain, *tied = tied
     head_gain, ffn_gain, decay_bias = tied
     gathered = exchange(spread, "ep_0")
     rows_in = lax.all_gather(residual_in, SLAB, axis=0, tiled=True)
     lhs, slab_res = pl.pallas_call(
-        functools.partial(strips_of, lambda: lax.axis_index(SLAB), slab, strip),
+        strips_of,
         out_shape=[pltpu.VMEM((slab * seqs, held), BF16)] * 2,
-        in_specs=[vmem] * 2,
+        in_specs=[vmem] * 3,
         out_specs=[vmem] * 2,
-    )(on_chip(rows_in), on_chip(norm_gain))
+    )(on_chip(rows_in), on_chip(norm_gain), on_chip(pick))
     gathered, lhs, slab_res = lax.optimization_barrier((gathered, lhs, slab_res))
     gathered = gathered.reshape(held, in_width + value_width)
     sums = jnp.dot(lhs, gathered[:, :in_width], preferred_element_type=F32).astype(BF16)

time: 131 us -> 131 us (level)
  no operation moved by 1% of the time
where the time goes in v8:
time: 131 us; the launch traced here: 130 us
  blocking collectives  113 us (86%)
  starting transfers between devices  10.9 us (8%)
  Pallas kernels  4.81 us (4%)
    all_to_all x8, blocking collectives, exchange(): came = lax.all_to_all(blocks, axes, split_axis=0, concat_axis=0, tiled=True)  93.8 us
    all_gather x1, blocking collectives, on_device(): rows_in = lax.all_gather(residual_in, SLAB, axis=0, tiled=True)  18.9 us
    all_to_all x1, starting transfers between devices, exchange(): came = lax.all_to_all(blocks, axes, split_axis=0, concat_axis=0, tiled=True)  10.9 us
  transfers between devices with their start and end apart: 1, of which 0 were waited for; matrix products, arithmetic and copies ran while one was open for 0% of the time, Pallas kernels for 0%

profile of v8, /device:TPU:1, one launch (start us, length us, event | category | flops | bytes accessed | tf_op | source)
XLA Modules:
  0.0 130.5 jit_solution(14031421728626516888)
XLA Ops:
  0.6 1.7 %shard_map.176 = (bf16[8,16,1792]{2,1,0:T(8,128)(2,1)}, bf16[2048,128]{1,0:T(8,128)(2,1)S(1)}, bf16[256,256]{1,0:T(8,128)(2,1)S(1)}, bf16[32,256]{1,0:T(8,128)(2...) custom-call(bf16[16,256]{1,0:T(8,128)(2,1)} %refs_0_.1, ...), custom_call_target="tpu_custom_call" | custom-call | tf_op jit(solution)/shard_map/pallas_call | solution.py:310
  2.4 10.9 %all-to-all-start = ((bf16[8,16,1792]{2,1,0:T(8,128)(2,1)}), bf16[8,16,1792]{2,1,0:T(8,128)(2,1)S(1)}, u32[]{:S(2)}, u32[]{:S(2)}) async-start(bf16[8,16,1792]{2,1,0:T(8,128)(2,1)} %get-tuple-element.47), calls=%async_computation | async-start | bytes 917504 | tf_op jit(solution)/shard_map/all_to_all | solution.py:26
  13.3 0.0 copy-start.1
  13.3 18.9 %all-gather = bf16[16,2,2048]{2,1,0:T(2,128)(2,1)S(1)} all-gather(bf16[1,2,2048]{2,1,0:T(2,128)(2,1)S(1)} %bitcast.35), channel_id=1, replica_groups=mesh['ep_0'=8,'ep_1'=8,'ep_2'=2,'tp'=4] {'ep_1','ep_2'}, dimensions={0}, use_global_device_ids=true | all-gather | bytes 139264 | tf_op jit(solution)/shard_map/all_gather | solution.py:334
  32.1 0.1 reshape.50.rows_ref
  32.2 0.3 shard_map.177
  32.5 0.0 all-to-all-done
  32.5 0.2 convolution_convert_fusion
  32.7 12.9 %all_to_all.45 = bf16[16,2,1280]{2,1,0:T(2,128)(2,1)S(1)} all-to-all(bf16[16,2,1280]{2,1,0:T(2,128)(2,1)S(1)} %reshape.37), channel_id=1, replica_groups=mesh['ep_0'=8,'ep_1'=8,'ep_2'=2,'tp'=4] {'ep_1','ep_2'}, dimensions={0} | all-to-all | bytes 163840 | tf_op jit(solution)/shard_map/all_to_all | solution.py:26
  45.6 0.0 copy-done.1
  45.6 1.5 %shard_map.178 = (bf16[16,2,512]{2,1,0:T(2,128)(2,1)S(1)}, f32[2,256,512]{2,1,0:T(8,128)}) custom-call(bf16[32,1280]{1,0:T(8,128)(2,1)S(1)} %reshape.38.came_ref, bf16[2,2048]{1,0:T(2,128)(2,1)S(1)} %get-tuple-element.48.res_ref, f32[1,256]{1,0:T(1,128)S(1)} %bitcast.37, f32[1,512]{1,0:T(1,128)S(1)} %bitcast.36, f32[2,256,512]{2,1,0:T(8,128)S(1)} %bitcast.29), custom_call_target="tpu_custom_call" | custom-call | tf_op jit(solution)/shard_map/pallas_call | solution.py:345
  47.1 0.0 copy-start
  47.1 10.0 %all_to_all.46 = bf16[16,2,512]{2,1,0:T(2,128)(2,1)S(1)} all-to-all(bf16[16,2,512]{2,1,0:T(2,128)(2,1)S(1)} %get-tuple-element.57), channel_id=1, replica_groups=mesh['ep_0'=8,'ep_1'=8,'ep_2'=2,'tp'=4] {'ep_1','ep_2'}, dimensions={0} | all-to-all | bytes 65536 | tf_op jit(solution)/shard_map/all_to_all | solution.py:26
  57.2 0.0 copy-start.4
  57.2 0.3 shard_map.179
  57.4 14.5 %all_to_all.47.came_ref = bf16[64,4,128]{2,1,0:T(4,128)(2,1)S(1)} all-to-all(bf16[64,4,128]{2,1,0:T(4,128)(2,1)S(1)} %shard_map.179), channel_id=1, replica_groups=mesh['ep_0'=8,'ep_1'=8,'ep_2'=2,'tp'=4] {'ep_1','ep_2','tp'}, dimensions={0} | all-to-all | bytes 131072 | tf_op jit(solution)/shard_map/all_to_all | solution.py:26
  72.0 0.0 copy-done
  72.0 0.0 copy-start.2
  72.0 0.0 copy-start.3
  72.0 0.4 shard_map.180
  72.3 14.2 %all_to_all.48 = bf16[8,32,256]{2,1,0:T(8,128)(2,1)S(1)} all-to-all(bf16[8,32,256]{2,1,0:T(8,128)(2,1)S(1)} %get-tuple-element.62), channel_id=1, replica_groups=mesh['ep_0'=8,'ep_1'=8,'ep_2'=2,'tp'=4] {'ep_0'}, dimensions={0} | all-to-all | bytes 262144 | tf_op jit(solution)/shard_map/all_to_all | solution.py:26
  86.6 9.9 %all_to_all.49.came_ref = bf16[8,16,256]{2,1,0:T(8,128)(2,1)S(1)} all-to-all(bf16[8,16,256]{2,1,0:T(8,128)(2,1)S(1)} %bitcast.39), channel_id=1, replica_groups=mesh['ep_0'=8,'ep_1'=8,'ep_2'=2,'tp'=4] {'tp','ep_2'}, dimensions={0} | all-to-all | bytes 131072 | tf_op jit(solution)/shard_map/all_to_all | solution.py:26
  96.5 0.0 copy-done.4
  96.5 0.0 copy-done.2
  96.5 0.0 copy-done.3
  96.5 0.7 shard_map.181
  97.1 8.0 %all_to_all.50 = bf16[8,16,256]{2,1,0:T(8,128)(2,1)S(1)} all-to-all(bf16[8,16,256]{2,1,0:T(8,128)(2,1)S(1)} %shard_map.181), channel_id=1, replica_groups=mesh['ep_0'=8,'ep_1'=8,'ep_2'=2,'tp'=4] {'tp','ep_2'}, dimensions={0} | all-to-all | bytes 131072 | tf_op jit(solution)/shard_map/all_to_all | solution.py:26
  105.2 0.2 convolution_convert_fusion.1
  105.4 15.3 %all_to_all.51 = bf16[64,4,256]{2,1,0:T(4,128)(2,1)S(1)} all-to-all(bf16[64,4,256]{2,1,0:T(4,128)(2,1)S(1)} %reshape.43), channel_id=1, replica_groups=mesh['ep_0'=8,'ep_1'=8,'ep_2'=2,'tp'=4] {'ep_0','ep_1'}, dimensions={0} | all-to-all | bytes 262144 | tf_op jit(solution)/shard_map/all_to_all | solution.py:26
  120.8 0.1 convert_reduce_fusion
  120.9 9.0 %all_to_all.52 = bf16[8,2,256]{2,1,0:T(2,128)(2,1)S(1)} all-to-all(bf16[8,2,256]{2,1,0:T(2,128)(2,1)S(1)} %bitcast.42), channel_id=1, replica_groups=mesh['ep_0'=8,'ep_1'=8,'ep_2'=2,'tp'=4] {'tp','ep_2'}, dimensions={0} | all-to-all | bytes 16384 | tf_op jit(solution)/shard_map/all_to_all | solution.py:26
  129.9 0.6 copy.23
  (13 shorter events, 0.2 us)
Async XLA Ops:
  2.4 30.1 %all-to-all-start = ((bf16[8,16,1792]{2,1,0:T(8,128)(2,1)}), bf16[8,16,1792]{2,1,0:T(8,128)(2,1)S(1)}, u32[]{:S(2)}, u32[]{:S(2)}) async-start(bf16[8,16,1792]{2,1,0:T(8,128)(2,1)} %get-tuple-element.47), calls=%async_computation | async-start | bytes 917504 | tf_op jit(solution)/shard_map/all_to_all | solution.py:26
  13.3 32.3 %copy-start.1 = (f32[2,1,256,512]{3,2,1,0:T(8,128)S(1)}, f32[2,1,256,512]{3,2,1,0:T(8,128)}, u32[]{:S(2)}) copy-start(f32[2,1,256,512]{3,2,1,0:T(8,128)} %param.18) | copy-start | bytes 3145732
  47.1 24.8 %copy-start = (bf16[128,2048]{1,0:T(8,128)(2,1)S(1)}, bf16[128,2048]{1,0:T(8,128)(2,1)}, u32[]{:S(2)}) copy-start(bf16[128,2048]{1,0:T(8,128)(2,1)} %expert_ref.1) | copy-start | bytes 1572868
  57.2 39.3 %copy-start.4 = (bf16[1,128,2048]{2,1,0:T(8,128)(2,1)S(1)}, bf16[1,128,2048]{2,1,0:T(8,128)(2,1)}, u32[]{:S(2)}) copy-start(bf16[1,128,2048]{2,1,0:T(8,128)(2,1)} %param.33) | copy-start | bytes 1572868
  72.0 24.5 %copy-start.2 = (bf16[1,2048,128]{2,1,0:T(8,128)(2,1)S(1)}, bf16[1,2048,128]{2,1,0:T(8,128)(2,1)}, u32[]{:S(2)}) copy-start(bf16[1,2048,128]{2,1,0:T(8,128)(2,1)} %param.31) | copy-start | bytes 1572868
  72.0 24.5 %copy-start.3 = (bf16[1,2048,128]{2,1,0:T(8,128)(2,1)S(1)}, bf16[1,2048,128]{2,1,0:T(8,128)(2,1)}, u32[]{:S(2)}) copy-start(bf16[1,2048,128]{2,1,0:T(8,128)(2,1)} %param.32) | copy-start | bytes 1572868

commit v9 on v8

--- a/solution.py
+++ b/solution.py
@@ -29,6 +29,11 @@
 
 def on_chip(array):
     return pltpu.with_memory_space_constraint(array, pltpu.VMEM)
+
+
+def kernel_call(body, **settings):
+    params = pltpu.CompilerParams(vmem_limit_bytes=6 * 2**20)
+    return pl.pallas_call(body, compiler_params=params, **settings)
 
 
 def to_all(shard, count):
@@ -110,7 +115,7 @@
     lhs_ref[...] = jnp.dot(scaled, pick, preferred_element_type=F32).astype(BF16)
 
 
-def advance(came_ref, res_ref, bias_ref, gain_ref, old_ref, out_ref, new_ref, held_ref, sems):
+def advance(came_ref, res_ref, bias_ref, gain_ref, old_ref, out_ref, held_ref):
     seqs, key_width, value_width = old_ref.shape
     count = came_ref.shape[0]
     seq_of = lax.broadcasted_iota(jnp.int32, (8, count), 1) % seqs
@@ -124,7 +129,6 @@
     pre = total[:, 2 * key_width + value_width :] + bias_ref[...]
     log_decay = (jnp.minimum(pre, 0.0) - jnp.log1p(jnp.exp(-jnp.abs(pre)))) / GATE_SCALE
     down = jnp.concatenate([query, key, jnp.exp(log_decay), jnp.zeros_like(query)], axis=0).T
-    copies = []
     gated = []
     for seq in range(seqs):
         for at in range(0, key_width, 64):
@@ -133,9 +137,6 @@
             alpha_col = down[rows, 2 * seqs + seq : 2 * seqs + seq + 1]
             new = alpha_col * old_ref[seq, rows] + key_col * value[seq : seq + 1]
             held_ref[seq, rows] = new
-            source, target = held_ref.at[seq, pl.ds(at, 64)], new_ref.at[seq, pl.ds(at, 64)]
-            copies.append(pltpu.make_async_copy(source, target, sems.at[len(copies)]))
-            copies[-1].start()
     for seq in range(seqs):
         read = jnp.zeros((8, value_width), F32)
         for at in range(0, key_width, 64):
@@ -148,8 +149,6 @@
     gated = jnp.concatenate(gated, axis=0).astype(BF16)
     for at in range(out_ref.shape[0]):
         out_ref[at] = gated
-    for copy in copies:
-        copy.wait()
 
 
 def mix(
@@ -162,9 +161,17 @@
     gate_ref,
     up_ref,
     down_ref,
+    state_ref,
     out_ref,
+    new_ref,
     rows_ref,
+    router_ref,
+    sems,
 ):
+    fetch = pltpu.make_async_copy(expert_ref, router_ref, sems.at[0])
+    fetch.start()
+    copy = pltpu.make_async_copy(state_ref, new_ref, sems.at[1])
+    copy.start()
     expert = which()
     size = came_ref.shape[2]
     for at in range(came_ref.shape[0]):
@@ -176,9 +183,10 @@
     up = jnp.dot(rows, up_ref[...], preferred_element_type=F32)
     over = (((1,), (1,)), ((), ()))
     groups = lax.dot_general(rows, group_ref[...], over, preferred_element_type=F32)
-    logits = lax.dot_general(rows, expert_ref[...], over, preferred_element_type=F32)
     units = (gate * jax.nn.sigmoid(gate) * up).astype(BF16)
     output = jnp.dot(units, down_ref[...], preferred_element_type=F32)
+    fetch.wait()
+    logits = lax.dot_general(rows, router_ref[...], over, preferred_element_type=F32)
     of_group = lax.broadcasted_iota(jnp.int32, groups.shape, 1)
     own = of_group == expert // (logits.shape[1] // groups.shape[1])
     group_logit = jnp.sum(jnp.where(own, groups, 0.0), axis=1, keepdims=True)
@@ -190,9 +198,10 @@
     piece = out_ref.shape[2]
     for at in range(out_ref.shape[0]):
         out_ref[at] = output[:, piece * at : piece * (at + 1)]
-
-
-def pack(heads_ref, held_ref, res_ref, out_ref):
+    copy.wait()
+
+
+def pack(heads_ref, held_ref, res_ref, _, out_ref, __):
     value_width = heads_ref.shape[1]
     part = lax.dot_general(
         heads_ref[...],
@@ -220,7 +229,7 @@
             out_ref[eighths * row + eighths // 2 * core + quarter] = block
 
 
-def dispatch(at_place, came_ref, along_ref, _, out_ref, hidden_ref, rows_ref, all_ref):
+def dispatch(at_place, came_ref, along_ref, _, out_ref, hidden_ref, __, rows_ref, all_ref):
     depth, row = at_place()
     count, lines, lanes = came_ref.shape
     eighths = rows_ref.shape[0] // lines
@@ -332,7 +341,7 @@
     head_gain, ffn_gain, decay_bias = tied
     gathered = exchange(spread, "ep_0")
     rows_in = lax.all_gather(residual_in, SLAB, axis=0, tiled=True)
-    lhs, slab_res = pl.pallas_call(
+    lhs, slab_res = kernel_call(
         strips_of,
         out_shape=[pltpu.VMEM((slab * seqs, held), BF16)] * 2,
         in_specs=[vmem] * 3,
@@ -342,60 +351,66 @@
     gathered = gathered.reshape(held, in_width + value_width)
     sums = jnp.dot(lhs, gathered[:, :in_width], preferred_element_type=F32).astype(BF16)
     arrived = exchange(sums.reshape(slab, seqs, in_width), SLAB)
-    gated, new_state = pl.pallas_call(
+    gated, new_state = kernel_call(
         advance,
         out_shape=[
             pltpu.VMEM((slab, seqs, value_width), BF16),
-            jax.ShapeDtypeStruct((seqs, key_width, value_width), F32),
+            pltpu.VMEM((seqs, key_width, value_width), F32),
         ],
         in_specs=[vmem] * 5,
-        out_specs=[vmem, pl.BlockSpec(memory_space=pl.ANY)],
-        scratch_shapes=[
-            pltpu.VMEM((seqs, key_width, value_width), F32),
-            pltpu.SemaphoreType.DMA((seqs * key_width // 64,)),
-        ],
+        out_specs=[vmem] * 2,
     )(*map(on_chip, (arrived.reshape(slab * seqs, in_width), residual_in, decay_bias, head_gain, gla_state[:, 0])))
 
     slab_heads, slab_res = exchange(gated, SLAB, slab_res)
     slab_heads = slab_heads.reshape(slab * seqs, value_width)
     lines = slab * seqs // parts
-    came = pl.pallas_call(
+    state = pltpu.VMEM(new_state.shape, F32)
+    came, new_state = kernel_call(
         pack,
-        out_shape=pltpu.VMEM((slab * heads, lines, held), BF16),
-        in_specs=[vmem] * 3,
-        out_specs=vmem,
-    )(*map(on_chip, (slab_heads, gathered, slab_res)))
+        out_shape=[pltpu.VMEM((slab * heads, lines, held), BF16), state],
+        in_specs=[vmem] * 4,
+        out_specs=[vmem] * 2,
+        input_output_aliases={3: 1},
+    )(*map(on_chip, (slab_heads, gathered, slab_res, new_state)))
     came = exchange(came, SLAB_TP)
-    router = on_chip(router_expert)
 
     def at_place():
         return lax.axis_index("ep_0"), lax.axis_index("ep_1")
 
-    outward, hidden = pl.pallas_call(
+    outward, hidden, new_state = kernel_call(
         functools.partial(dispatch, at_place),
         out_shape=[
             pltpu.VMEM((depths, cores * CAP, piece), BF16),
             pltpu.VMEM((cores * seqs, piece), BF16),
+            state,
         ],
         in_specs=[vmem] * 3,
-        out_specs=[vmem] * 2,
+        out_specs=[vmem] * 3,
         scratch_shapes=[
             pltpu.VMEM((slab * seqs, piece), F32),
             pltpu.VMEM((tokens, piece), BF16),
         ],
-    )(on_chip(came), on_chip(along), router)
+        input_output_aliases={2: 2},
+    )(on_chip(came), on_chip(along), on_chip(new_state))
     slot_part = exchange(outward, "ep_0").astype(F32).sum(axis=0).astype(BF16)
     slot_part = to_all(slot_part.reshape(cores, CAP, piece), heads)
     came = exchange(slot_part.reshape(parts, CAP, piece), CHIPS)
     operands = (came, ffn_gain, group_rows, rival_lane)
-    operands += (w_gate[0], w_up[0], w_down[0])
-    back = pl.pallas_call(
+    operands += (w_gate[0], w_up[0], w_down[0], new_state)
+    back, new_state = kernel_call(
         functools.partial(mix, lambda: lax.axis_index(EP)),
-        out_shape=pltpu.VMEM((parts, CAP, piece), BF16),
-        in_specs=[vmem] * (1 + len(operands)),
-        out_specs=vmem,
-        scratch_shapes=[pltpu.VMEM((CAP, width), F32)],
-    )(router, *map(on_chip, operands))
+        out_shape=[
+            pltpu.VMEM((parts, CAP, piece), BF16),
+            jax.ShapeDtypeStruct(new_state.shape, F32),
+        ],
+        in_specs=[pl.BlockSpec(memory_space=pl.ANY)] + [vmem] * len(operands),
+        out_specs=[vmem, pl.BlockSpec(memory_space=pl.ANY)],
+        scratch_shapes=[
+            pltpu.VMEM((CAP, width), F32),
+            pltpu.VMEM(router_expert.shape, BF16),
+            pltpu.SemaphoreType.DMA((2,)),
+        ],
+    )(router_expert, *map(on_chip, operands))
     summed = exchange(back, CHIPS).reshape(heads, cores, CAP, piece).astype(F32).sum(axis=0)
     dense = lax.dot_general(
         select,

time: 131 us -> 131 us (level)
  no operation moved by 1% of the time
where the time goes in v9:
time: 131 us; the launch traced here: 130 us
  blocking collectives  113 us (86%)
  starting transfers between devices  10.9 us (8%)
  Pallas kernels  4.46 us (3%)
    all_to_all x8, blocking collectives, exchange(): came = lax.all_to_all(blocks, axes, split_axis=0, concat_axis=0, tiled=True)  93.8 us
    all_gather x1, blocking collectives, on_device(): rows_in = lax.all_gather(residual_in, SLAB, axis=0, tiled=True)  18.9 us
    all_to_all x1, starting transfers between devices, exchange(): came = lax.all_to_all(blocks, axes, split_axis=0, concat_axis=0, tiled=True)  10.9 us
  transfers between devices with their start and end apart: 1, of which 0 were waited for; matrix products, arithmetic and copies ran while one was open for 0% of the time, Pallas kernels for 0%

profile of v9, /device:TPU:1, one launch (start us, length us, event | category | flops | bytes accessed | tf_op | source)
XLA Modules:
  0.0 130.1 jit_solution(13024385336400979323)
XLA Ops:
  0.6 1.7 %shard_map.176 = (bf16[8,16,1792]{2,1,0:T(8,128)(2,1)}, bf16[2048,128]{1,0:T(8,128)(2,1)S(1)}, bf16[256,256]{1,0:T(8,128)(2,1)S(1)}, bf16[32,256]{1,0:T(8,128)(2...) custom-call(bf16[16,256]{1,0:T(8,128)(2,1)} %refs_0_.1, ...), custom_call_target="tpu_custom_call" | custom-call | tf_op jit(solution)/shard_map/pallas_call | solution.py:319
  2.4 10.9 %all-to-all-start = ((bf16[8,16,1792]{2,1,0:T(8,128)(2,1)}), bf16[8,16,1792]{2,1,0:T(8,128)(2,1)S(1)}, u32[]{:S(2)}, u32[]{:S(2)}) async-start(bf16[8,16,1792]{2,1,0:T(8,128)(2,1)} %get-tuple-element.52), calls=%async_computation | async-start | bytes 917504 | tf_op jit(solution)/shard_map/all_to_all | solution.py:26
  13.3 0.0 copy-start
  13.3 18.9 %all-gather = bf16[16,2,2048]{2,1,0:T(2,128)(2,1)S(1)} all-gather(bf16[1,2,2048]{2,1,0:T(2,128)(2,1)S(1)} %bitcast.35), channel_id=1, replica_groups=mesh['ep_0'=8,'ep_1'=8,'ep_2'=2,'tp'=4] {'ep_1','ep_2'}, dimensions={0}, use_global_device_ids=true | all-gather | bytes 139264 | tf_op jit(solution)/shard_map/all_gather | solution.py:343
  32.1 0.1 reshape.50.rows_ref
  32.2 0.3 shard_map.177
  32.5 0.0 all-to-all-done
  32.5 0.2 convolution_convert_fusion
  32.7 12.9 %all_to_all.45 = bf16[16,2,1280]{2,1,0:T(2,128)(2,1)S(1)} all-to-all(bf16[16,2,1280]{2,1,0:T(2,128)(2,1)S(1)} %reshape.37), channel_id=1, replica_groups=mesh['ep_0'=8,'ep_1'=8,'ep_2'=2,'tp'=4] {'ep_1','ep_2'}, dimensions={0} | all-to-all | bytes 163840 | tf_op jit(solution)/shard_map/all_to_all | solution.py:26
  45.6 0.0 copy-done
  45.6 0.7 shard_map.178
  46.3 9.9 %all_to_all.46 = bf16[16,2,512]{2,1,0:T(2,128)(2,1)S(1)} all-to-all(bf16[16,2,512]{2,1,0:T(2,128)(2,1)S(1)} %get-tuple-element.62), channel_id=1, replica_groups=mesh['ep_0'=8,'ep_1'=8,'ep_2'=2,'tp'=4] {'ep_1','ep_2'}, dimensions={0} | all-to-all | bytes 65536 | tf_op jit(solution)/shard_map/all_to_all | solution.py:26
  56.2 0.0 copy-start.4
  56.2 0.3 shard_map.179
  56.5 14.5 %all_to_all.47.came_ref = bf16[64,4,128]{2,1,0:T(4,128)(2,1)S(1)} all-to-all(bf16[64,4,128]{2,1,0:T(4,128)(2,1)S(1)} %get-tuple-element.67), channel_id=1, replica_groups=mesh['ep_0'=8,'ep_1'=8,'ep_2'=2,'tp'=4] {'ep_1','ep_2','tp'}, dimensions={0} | all-to-all | bytes 131072 | tf_op jit(solution)/shard_map/all_to_all | solution.py:26
  71.0 0.0 copy-start.2
  71.0 0.0 copy-start.3
  71.0 0.4 shard_map.180
  71.4 0.0 copy-start.1
  71.4 14.3 %all_to_all.48 = bf16[8,32,256]{2,1,0:T(8,128)(2,1)S(1)} all-to-all(bf16[8,32,256]{2,1,0:T(8,128)(2,1)S(1)} %get-tuple-element.70), channel_id=1, replica_groups=mesh['ep_0'=8,'ep_1'=8,'ep_2'=2,'tp'=4] {'ep_0'}, dimensions={0} | all-to-all | bytes 262144 | tf_op jit(solution)/shard_map/all_to_all | solution.py:26
  85.7 9.9 %all_to_all.49.came_ref = bf16[8,16,256]{2,1,0:T(8,128)(2,1)S(1)} all-to-all(bf16[8,16,256]{2,1,0:T(8,128)(2,1)S(1)} %bitcast.39), channel_id=1, replica_groups=mesh['ep_0'=8,'ep_1'=8,'ep_2'=2,'tp'=4] {'tp','ep_2'}, dimensions={0} | all-to-all | bytes 131072 | tf_op jit(solution)/shard_map/all_to_all | solution.py:26
  95.6 0.0 copy-done.4
  95.6 0.0 copy-done.2
  95.6 0.0 copy-done.3
  95.6 0.0 copy-done.1
  95.7 1.2 shard_map.181
  96.8 8.0 %all_to_all.50 = bf16[8,16,256]{2,1,0:T(8,128)(2,1)S(1)} all-to-all(bf16[8,16,256]{2,1,0:T(8,128)(2,1)S(1)} %get-tuple-element.75), channel_id=1, replica_groups=mesh['ep_0'=8,'ep_1'=8,'ep_2'=2,'tp'=4] {'tp','ep_2'}, dimensions={0} | all-to-all | bytes 131072 | tf_op jit(solution)/shard_map/all_to_all | solution.py:26
  104.8 0.2 convolution_convert_fusion.1
  105.1 15.3 %all_to_all.51 = bf16[64,4,256]{2,1,0:T(4,128)(2,1)S(1)} all-to-all(bf16[64,4,256]{2,1,0:T(4,128)(2,1)S(1)} %reshape.43), channel_id=1, replica_groups=mesh['ep_0'=8,'ep_1'=8,'ep_2'=2,'tp'=4] {'ep_0','ep_1'}, dimensions={0} | all-to-all | bytes 262144 | tf_op jit(solution)/shard_map/all_to_all | solution.py:26
  120.4 0.1 convert_reduce_fusion
  120.5 9.0 %all_to_all.52 = bf16[8,2,256]{2,1,0:T(2,128)(2,1)S(1)} all-to-all(bf16[8,2,256]{2,1,0:T(2,128)(2,1)S(1)} %bitcast.42), channel_id=1, replica_groups=mesh['ep_0'=8,'ep_1'=8,'ep_2'=2,'tp'=4] {'tp','ep_2'}, dimensions={0} | all-to-all | bytes 16384 | tf_op jit(solution)/shard_map/all_to_all | solution.py:26
  129.6 0.6 copy.27
  (13 shorter events, 0.2 us)
Async XLA Ops:
  2.4 30.1 %all-to-all-start = ((bf16[8,16,1792]{2,1,0:T(8,128)(2,1)}), bf16[8,16,1792]{2,1,0:T(8,128)(2,1)S(1)}, u32[]{:S(2)}, u32[]{:S(2)}) async-start(bf16[8,16,1792]{2,1,0:T(8,128)(2,1)} %get-tuple-element.52), calls=%async_computation | async-start | bytes 917504 | tf_op jit(solution)/shard_map/all_to_all | solution.py:26
  13.3 32.3 %copy-start = (f32[2,1,256,512]{3,2,1,0:T(8,128)S(1)}, f32[2,1,256,512]{3,2,1,0:T(8,128)}, u32[]{:S(2)}) copy-start(f32[2,1,256,512]{3,2,1,0:T(8,128)} %param.18) | copy-start | bytes 3145732
  56.2 39.5 %copy-start.4 = (bf16[1,128,2048]{2,1,0:T(8,128)(2,1)S(1)}, bf16[1,128,2048]{2,1,0:T(8,128)(2,1)}, u32[]{:S(2)}) copy-start(bf16[1,128,2048]{2,1,0:T(8,128)(2,1)} %param.33) | copy-start | bytes 1572868
  71.0 24.7 %copy-start.2 = (bf16[1,2048,128]{2,1,0:T(8,128)(2,1)S(1)}, bf16[1,2048,128]{2,1,0:T(8,128)(2,1)}, u32[]{:S(2)}) copy-start(bf16[1,2048,128]{2,1,0:T(8,128)(2,1)} %param.31) | copy-start | bytes 1572868
  71.0 24.7 %copy-start.3 = (bf16[1,2048,128]{2,1,0:T(8,128)(2,1)S(1)}, bf16[1,2048,128]{2,1,0:T(8,128)(2,1)}, u32[]{:S(2)}) copy-start(bf16[1,2048,128]{2,1,0:T(8,128)(2,1)} %param.32) | copy-start | bytes 1572868
  71.4 24.3 %copy-start.1 = (bf16[128,2048]{1,0:T(8,128)(2,1)S(1)}, bf16[128,2048]{1,0:T(8,128)(2,1)}, u32[]{:S(2)}) copy-start(bf16[128,2048]{1,0:T(8,128)(2,1)} %expert_ref.1) | copy-start | bytes 1572868

commit v10 on v9

--- a/solution.py
+++ b/solution.py
@@ -170,8 +170,12 @@
 ):
     fetch = pltpu.make_async_copy(expert_ref, router_ref, sems.at[0])
     fetch.start()
-    copy = pltpu.make_async_copy(state_ref, new_ref, sems.at[1])
-    copy.start()
+    copies = []
+    for seq in range(state_ref.shape[0]):
+        for at in range(0, state_ref.shape[1], 64):
+            source, target = state_ref.at[seq, pl.ds(at, 64)], new_ref.at[seq, pl.ds(at, 64)]
+            copies.append(pltpu.make_async_copy(source, target, sems.at[1 + len(copies)]))
+            copies[-1].start()
     expert = which()
     size = came_ref.shape[2]
     for at in range(came_ref.shape[0]):
@@ -181,24 +185,34 @@
     rows = (rows * lax.rsqrt(mean + EPSILON) * gain_ref[...]).astype(BF16)
     gate = jnp.dot(rows, gate_ref[...], preferred_element_type=F32)
     up = jnp.dot(rows, up_ref[...], preferred_element_type=F32)
-    over = (((1,), (1,)), ((), ()))
-    groups = lax.dot_general(rows, group_ref[...], over, preferred_element_type=F32)
+    floats = rows.astype(F32)
+    count = group_ref.shape[0]
+    group_rows = group_ref[...].astype(F32)
+    groups = [
+        jnp.sum(floats * group_rows[at : at + 1], axis=1, keepdims=True) for at in range(count)
+    ]
     units = (gate * jax.nn.sigmoid(gate) * up).astype(BF16)
     output = jnp.dot(units, down_ref[...], preferred_element_type=F32)
+    experts = router_ref.shape[0]
+    own = expert // (experts // count)
+    group_logit = groups[0]
+    for at in range(1, count):
+        group_logit = jnp.where(own == at, groups[at], group_logit)
+    total = jnp.zeros_like(group_logit)
+    for logit in groups:
+        total = total + jnp.exp(logit - group_logit)
+    share = 1.0 / total
+    lanes = lax.broadcasted_iota(jnp.int32, rival_ref.shape, 1)
+    apart = jnp.where(lanes == expert, 1.0, 0.0) - rival_ref[...]
     fetch.wait()
-    logits = lax.dot_general(rows, router_ref[...], over, preferred_element_type=F32)
-    of_group = lax.broadcasted_iota(jnp.int32, groups.shape, 1)
-    own = of_group == expert // (logits.shape[1] // groups.shape[1])
-    group_logit = jnp.sum(jnp.where(own, groups, 0.0), axis=1, keepdims=True)
-    share = 1.0 / jnp.sum(jnp.exp(groups - group_logit), axis=1, keepdims=True)
-    lanes = lax.broadcasted_iota(jnp.int32, logits.shape, 1)
-    chosen = jnp.sum(jnp.where(lanes == expert, logits, 0.0), axis=1, keepdims=True)
-    rival = jnp.sum(logits * rival_ref[...], axis=1, keepdims=True)
-    output = (output * (share * jax.nn.sigmoid(chosen - rival))).astype(BF16)
+    apart = jnp.dot(apart.astype(BF16), router_ref[...], preferred_element_type=F32)
+    lead = jnp.sum(floats * apart, axis=1, keepdims=True)
+    output = (output * (share * jax.nn.sigmoid(lead))).astype(BF16)
     piece = out_ref.shape[2]
     for at in range(out_ref.shape[0]):
         out_ref[at] = output[:, piece * at : piece * (at + 1)]
-    copy.wait()
+    for copy in copies:
+        copy.wait()
 
 
 def pack(heads_ref, held_ref, res_ref, _, out_ref, __):
@@ -408,7 +422,7 @@
         scratch_shapes=[
             pltpu.VMEM((CAP, width), F32),
             pltpu.VMEM(router_expert.shape, BF16),
-            pltpu.SemaphoreType.DMA((2,)),
+            pltpu.SemaphoreType.DMA((1 + seqs * key_width // 64,)),
         ],
     )(router_expert, *map(on_chip, operands))
     summed = exchange(back, CHIPS).reshape(heads, cores, CAP, piece).astype(F32).sum(axis=0)

time: 131 us -> 131 us (level)
  no operation moved by 1% of the time
where the time goes in v10:
time: 131 us; the launch traced here: 130 us
  blocking collectives  113 us (86%)
  starting transfers between devices  10.9 us (8%)
  Pallas kernels  4.59 us (4%)
    all_to_all x8, blocking collectives, exchange(): came = lax.all_to_all(blocks, axes, split_axis=0, concat_axis=0, tiled=True)  93.8 us
    all_gather x1, blocking collectives, on_device(): rows_in = lax.all_gather(residual_in, SLAB, axis=0, tiled=True)  18.9 us
    all_to_all x1, starting transfers between devices, exchange(): came = lax.all_to_all(blocks, axes, split_axis=0, concat_axis=0, tiled=True)  10.9 us
  transfers between devices with their start and end apart: 1, of which 0 were waited for; matrix products, arithmetic and copies ran while one was open for 0% of the time, Pallas kernels for 0%

profile of v10, /device:TPU:1, one launch (start us, length us, event | category | flops | bytes accessed | tf_op | source)
XLA Modules:
  0.0 130.3 jit_solution(3820685717323122948)
XLA Ops:
  0.6 1.7 %shard_map.176 = (bf16[8,16,1792]{2,1,0:T(8,128)(2,1)}, bf16[2048,128]{1,0:T(8,128)(2,1)S(1)}, bf16[256,256]{1,0:T(8,128)(2,1)S(1)}, bf16[32,256]{1,0:T(8,128)(2...) custom-call(bf16[16,256]{1,0:T(8,128)(2,1)} %refs_0_.1, ...), custom_call_target="tpu_custom_call" | custom-call | tf_op jit(solution)/shard_map/pallas_call | solution.py:333
  2.4 10.9 %all-to-all-start = ((bf16[8,16,1792]{2,1,0:T(8,128)(2,1)}), bf16[8,16,1792]{2,1,0:T(8,128)(2,1)S(1)}, u32[]{:S(2)}, u32[]{:S(2)}) async-start(bf16[8,16,1792]{2,1,0:T(8,128)(2,1)} %get-tuple-element.52), calls=%async_computation | async-start | bytes 917504 | tf_op jit(solution)/shard_map/all_to_all | solution.py:26
  13.3 0.0 copy-start
  13.3 18.9 %all-gather = bf16[16,2,2048]{2,1,0:T(2,128)(2,1)S(1)} all-gather(bf16[1,2,2048]{2,1,0:T(2,128)(2,1)S(1)} %bitcast.35), channel_id=1, replica_groups=mesh['ep_0'=8,'ep_1'=8,'ep_2'=2,'tp'=4] {'ep_1','ep_2'}, dimensions={0}, use_global_device_ids=true | all-gather | bytes 139264 | tf_op jit(solution)/shard_map/all_gather | solution.py:357
  32.1 0.1 reshape.50.rows_ref
  32.2 0.3 shard_map.177
  32.5 0.0 all-to-all-done
  32.5 0.2 convolution_convert_fusion
  32.7 12.9 %all_to_all.45 = bf16[16,2,1280]{2,1,0:T(2,128)(2,1)S(1)} all-to-all(bf16[16,2,1280]{2,1,0:T(2,128)(2,1)S(1)} %reshape.37), channel_id=1, replica_groups=mesh['ep_0'=8,'ep_1'=8,'ep_2'=2,'tp'=4] {'ep_1','ep_2'}, dimensions={0} | all-to-all | bytes 163840 | tf_op jit(solution)/shard_map/all_to_all | solution.py:26
  45.6 0.0 copy-done
  45.6 0.7 shard_map.178
  46.3 9.9 %all_to_all.46 = bf16[16,2,512]{2,1,0:T(2,128)(2,1)S(1)} all-to-all(bf16[16,2,512]{2,1,0:T(2,128)(2,1)S(1)} %get-tuple-element.62), channel_id=1, replica_groups=mesh['ep_0'=8,'ep_1'=8,'ep_2'=2,'tp'=4] {'ep_1','ep_2'}, dimensions={0} | all-to-all | bytes 65536 | tf_op jit(solution)/shard_map/all_to_all | solution.py:26
  56.2 0.0 copy-start.4
  56.2 0.3 shard_map.179
  56.5 14.5 %all_to_all.47.came_ref = bf16[64,4,128]{2,1,0:T(4,128)(2,1)S(1)} all-to-all(bf16[64,4,128]{2,1,0:T(4,128)(2,1)S(1)} %get-tuple-element.67), channel_id=1, replica_groups=mesh['ep_0'=8,'ep_1'=8,'ep_2'=2,'tp'=4] {'ep_1','ep_2','tp'}, dimensions={0} | all-to-all | bytes 131072 | tf_op jit(solution)/shard_map/all_to_all | solution.py:26
  71.0 0.0 copy-start.2
  71.0 0.0 copy-start.3
  71.0 0.4 shard_map.180
  71.4 0.0 copy-start.1
  71.4 14.3 %all_to_all.48 = bf16[8,32,256]{2,1,0:T(8,128)(2,1)S(1)} all-to-all(bf16[8,32,256]{2,1,0:T(8,128)(2,1)S(1)} %get-tuple-element.70), channel_id=1, replica_groups=mesh['ep_0'=8,'ep_1'=8,'ep_2'=2,'tp'=4] {'ep_0'}, dimensions={0} | all-to-all | bytes 262144 | tf_op jit(solution)/shard_map/all_to_all | solution.py:26
  85.7 9.9 %all_to_all.49.came_ref = bf16[8,16,256]{2,1,0:T(8,128)(2,1)S(1)} all-to-all(bf16[8,16,256]{2,1,0:T(8,128)(2,1)S(1)} %bitcast.39), channel_id=1, replica_groups=mesh['ep_0'=8,'ep_1'=8,'ep_2'=2,'tp'=4] {'tp','ep_2'}, dimensions={0} | all-to-all | bytes 131072 | tf_op jit(solution)/shard_map/all_to_all | solution.py:26
  95.6 0.0 copy-done.4
  95.6 0.0 copy-done.2
  95.6 0.0 copy-done.3
  95.6 0.0 copy-done.1
  95.7 1.3 shard_map.181
  96.9 8.0 %all_to_all.50 = bf16[8,16,256]{2,1,0:T(8,128)(2,1)S(1)} all-to-all(bf16[8,16,256]{2,1,0:T(8,128)(2,1)S(1)} %get-tuple-element.75), channel_id=1, replica_groups=mesh['ep_0'=8,'ep_1'=8,'ep_2'=2,'tp'=4] {'tp','ep_2'}, dimensions={0} | all-to-all | bytes 131072 | tf_op jit(solution)/shard_map/all_to_all | solution.py:26
  105.0 0.2 convolution_convert_fusion.1
  105.2 15.3 %all_to_all.51 = bf16[64,4,256]{2,1,0:T(4,128)(2,1)S(1)} all-to-all(bf16[64,4,256]{2,1,0:T(4,128)(2,1)S(1)} %reshape.43), channel_id=1, replica_groups=mesh['ep_0'=8,'ep_1'=8,'ep_2'=2,'tp'=4] {'ep_0','ep_1'}, dimensions={0} | all-to-all | bytes 262144 | tf_op jit(solution)/shard_map/all_to_all | solution.py:26
  120.6 0.1 convert_reduce_fusion
  120.7 9.0 %all_to_all.52 = bf16[8,2,256]{2,1,0:T(2,128)(2,1)S(1)} all-to-all(bf16[8,2,256]{2,1,0:T(2,128)(2,1)S(1)} %bitcast.42), channel_id=1, replica_groups=mesh['ep_0'=8,'ep_1'=8,'ep_2'=2,'tp'=4] {'tp','ep_2'}, dimensions={0} | all-to-all | bytes 16384 | tf_op jit(solution)/shard_map/all_to_all | solution.py:26
  129.7 0.6 copy.27
  (13 shorter events, 0.2 us)
Async XLA Ops:
  2.4 30.1 %all-to-all-start = ((bf16[8,16,1792]{2,1,0:T(8,128)(2,1)}), bf16[8,16,1792]{2,1,0:T(8,128)(2,1)S(1)}, u32[]{:S(2)}, u32[]{:S(2)}) async-start(bf16[8,16,1792]{2,1,0:T(8,128)(2,1)} %get-tuple-element.52), calls=%async_computation | async-start | bytes 917504 | tf_op jit(solution)/shard_map/all_to_all | solution.py:26
  13.3 32.3 %copy-start = (f32[2,1,256,512]{3,2,1,0:T(8,128)S(1)}, f32[2,1,256,512]{3,2,1,0:T(8,128)}, u32[]{:S(2)}) copy-start(f32[2,1,256,512]{3,2,1,0:T(8,128)} %param.18) | copy-start | bytes 3145732
  56.2 39.5 %copy-start.4 = (bf16[1,128,2048]{2,1,0:T(8,128)(2,1)S(1)}, bf16[1,128,2048]{2,1,0:T(8,128)(2,1)}, u32[]{:S(2)}) copy-start(bf16[1,128,2048]{2,1,0:T(8,128)(2,1)} %param.33) | copy-start | bytes 1572868
  71.0 24.7 %copy-start.2 = (bf16[1,2048,128]{2,1,0:T(8,128)(2,1)S(1)}, bf16[1,2048,128]{2,1,0:T(8,128)(2,1)}, u32[]{:S(2)}) copy-start(bf16[1,2048,128]{2,1,0:T(8,128)(2,1)} %param.31) | copy-start | bytes 1572868
  71.0 24.7 %copy-start.3 = (bf16[1,2048,128]{2,1,0:T(8,128)(2,1)S(1)}, bf16[1,2048,128]{2,1,0:T(8,128)(2,1)}, u32[]{:S(2)}) copy-start(bf16[1,2048,128]{2,1,0:T(8,128)(2,1)} %param.32) | copy-start | bytes 1572868
  71.4 24.3 %copy-start.1 = (bf16[128,2048]{1,0:T(8,128)(2,1)S(1)}, bf16[128,2048]{1,0:T(8,128)(2,1)}, u32[]{:S(2)}) copy-start(bf16[128,2048]{1,0:T(8,128)(2,1)} %expert_ref.1) | copy-start | bytes 1572868

commit v11 on v10

--- a/solution.py
+++ b/solution.py
@@ -153,7 +153,7 @@
 
 def mix(
     which,
-    expert_ref,
+    router_ref,
     came_ref,
     gain_ref,
     group_ref,
@@ -165,16 +165,13 @@
     out_ref,
     new_ref,
     rows_ref,
-    router_ref,
     sems,
 ):
-    fetch = pltpu.make_async_copy(expert_ref, router_ref, sems.at[0])
-    fetch.start()
     copies = []
     for seq in range(state_ref.shape[0]):
         for at in range(0, state_ref.shape[1], 64):
             source, target = state_ref.at[seq, pl.ds(at, 64)], new_ref.at[seq, pl.ds(at, 64)]
-            copies.append(pltpu.make_async_copy(source, target, sems.at[1 + len(copies)]))
+            copies.append(pltpu.make_async_copy(source, target, sems.at[len(copies)]))
             copies[-1].start()
     expert = which()
     size = came_ref.shape[2]
@@ -204,7 +201,6 @@
     share = 1.0 / total
     lanes = lax.broadcasted_iota(jnp.int32, rival_ref.shape, 1)
     apart = jnp.where(lanes == expert, 1.0, 0.0) - rival_ref[...]
-    fetch.wait()
     apart = jnp.dot(apart.astype(BF16), router_ref[...], preferred_element_type=F32)
     lead = jnp.sum(floats * apart, axis=1, keepdims=True)
     output = (output * (share * jax.nn.sigmoid(lead))).astype(BF16)
@@ -409,7 +405,7 @@
     slot_part = exchange(outward, "ep_0").astype(F32).sum(axis=0).astype(BF16)
     slot_part = to_all(slot_part.reshape(cores, CAP, piece), heads)
     came = exchange(slot_part.reshape(parts, CAP, piece), CHIPS)
-    operands = (came, ffn_gain, group_rows, rival_lane)
+    operands = (router_expert, came, ffn_gain, group_rows, rival_lane)
     operands += (w_gate[0], w_up[0], w_down[0], new_state)
     back, new_state = kernel_call(
         functools.partial(mix, lambda: lax.axis_index(EP)),
@@ -417,14 +413,13 @@
             pltpu.VMEM((parts, CAP, piece), BF16),
             jax.ShapeDtypeStruct(new_state.shape, F32),
         ],
-        in_specs=[pl.BlockSpec(memory_space=pl.ANY)] + [vmem] * len(operands),
+        in_specs=[vmem] * len(operands),
         out_specs=[vmem, pl.BlockSpec(memory_space=pl.ANY)],
         scratch_shapes=[
             pltpu.VMEM((CAP, width), F32),
-            pltpu.VMEM(router_expert.shape, BF16),
-            pltpu.SemaphoreType.DMA((1 + seqs * key_width // 64,)),
-        ],
-    )(router_expert, *map(on_chip, operands))
+            pltpu.SemaphoreType.DMA((seqs * key_width // 64,)),
+        ],
+    )(*map(on_chip, operands))
     summed = exchange(back, CHIPS).reshape(heads, cores, CAP, piece).astype(F32).sum(axis=0)
     dense = lax.dot_general(
         select,

time: 131 us -> 131 us (level)
  no operation moved by 1% of the time
where the time goes in v11:
time: 131 us; the launch traced here: 130 us
  blocking collectives  113 us (86%)
  starting transfers between devices  10.9 us (8%)
  Pallas kernels  4.68 us (4%)
    all_to_all x8, blocking collectives, exchange(): came = lax.all_to_all(blocks, axes, split_axis=0, concat_axis=0, tiled=True)  93.8 us
    all_gather x1, blocking collectives, on_device(): rows_in = lax.all_gather(residual_in, SLAB, axis=0, tiled=True)  18.9 us
    all_to_all x1, starting transfers between devices, exchange(): came = lax.all_to_all(blocks, axes, split_axis=0, concat_axis=0, tiled=True)  10.9 us
  transfers between devices with their start and end apart: 1, of which 0 were waited for; matrix products, arithmetic and copies ran while one was open for 0% of the time, Pallas kernels for 0%

profile of v11, /device:TPU:1, one launch (start us, length us, event | category | flops | bytes accessed | tf_op | source)
XLA Modules:
  0.0 130.4 jit_solution(4127914996545473309)
XLA Ops:
  0.6 1.7 %shard_map.176 = (bf16[8,16,1792]{2,1,0:T(8,128)(2,1)}, bf16[2048,128]{1,0:T(8,128)(2,1)S(1)}, bf16[256,256]{1,0:T(8,128)(2,1)S(1)}, bf16[32,256]{1,0:T(8,128)(2...) custom-call(bf16[16,256]{1,0:T(8,128)(2,1)} %refs_0_.1, ...), custom_call_target="tpu_custom_call" | custom-call | tf_op jit(solution)/shard_map/pallas_call | solution.py:329
  2.4 10.9 %all-to-all-start = ((bf16[8,16,1792]{2,1,0:T(8,128)(2,1)}), bf16[8,16,1792]{2,1,0:T(8,128)(2,1)S(1)}, u32[]{:S(2)}, u32[]{:S(2)}) async-start(bf16[8,16,1792]{2,1,0:T(8,128)(2,1)} %get-tuple-element.52), calls=%async_computation | async-start | bytes 917504 | tf_op jit(solution)/shard_map/all_to_all | solution.py:26
  13.3 0.0 copy-start
  13.3 18.9 %all-gather = bf16[16,2,2048]{2,1,0:T(2,128)(2,1)S(1)} all-gather(bf16[1,2,2048]{2,1,0:T(2,128)(2,1)S(1)} %bitcast.35), channel_id=1, replica_groups=mesh['ep_0'=8,'ep_1'=8,'ep_2'=2,'tp'=4] {'ep_1','ep_2'}, dimensions={0}, use_global_device_ids=true | all-gather | bytes 139264 | tf_op jit(solution)/shard_map/all_gather | solution.py:353
  32.1 0.1 reshape.50.rows_ref
  32.2 0.3 shard_map.177
  32.5 0.0 all-to-all-done
  32.5 0.2 convolution_convert_fusion
  32.7 12.9 %all_to_all.45 = bf16[16,2,1280]{2,1,0:T(2,128)(2,1)S(1)} all-to-all(bf16[16,2,1280]{2,1,0:T(2,128)(2,1)S(1)} %reshape.37), channel_id=1, replica_groups=mesh['ep_0'=8,'ep_1'=8,'ep_2'=2,'tp'=4] {'ep_1','ep_2'}, dimensions={0} | all-to-all | bytes 163840 | tf_op jit(solution)/shard_map/all_to_all | solution.py:26
  45.6 0.0 copy-done
  45.6 0.7 shard_map.178
  46.3 9.9 %all_to_all.46 = bf16[16,2,512]{2,1,0:T(2,128)(2,1)S(1)} all-to-all(bf16[16,2,512]{2,1,0:T(2,128)(2,1)S(1)} %get-tuple-element.62), channel_id=1, replica_groups=mesh['ep_0'=8,'ep_1'=8,'ep_2'=2,'tp'=4] {'ep_1','ep_2'}, dimensions={0} | all-to-all | bytes 65536 | tf_op jit(solution)/shard_map/all_to_all | solution.py:26
  56.2 0.0 copy-start.4
  56.2 0.3 shard_map.179
  56.5 14.5 %all_to_all.47.came_ref = bf16[64,4,128]{2,1,0:T(4,128)(2,1)S(1)} all-to-all(bf16[64,4,128]{2,1,0:T(4,128)(2,1)S(1)} %get-tuple-element.67), channel_id=1, replica_groups=mesh['ep_0'=8,'ep_1'=8,'ep_2'=2,'tp'=4] {'ep_1','ep_2','tp'}, dimensions={0} | all-to-all | bytes 131072 | tf_op jit(solution)/shard_map/all_to_all | solution.py:26
  71.0 0.0 copy-start.2
  71.0 0.0 copy-start.3
  71.0 0.4 shard_map.180
  71.4 0.0 copy-start.1
  71.4 14.3 %all_to_all.48 = bf16[8,32,256]{2,1,0:T(8,128)(2,1)S(1)} all-to-all(bf16[8,32,256]{2,1,0:T(8,128)(2,1)S(1)} %get-tuple-element.70), channel_id=1, replica_groups=mesh['ep_0'=8,'ep_1'=8,'ep_2'=2,'tp'=4] {'ep_0'}, dimensions={0} | all-to-all | bytes 262144 | tf_op jit(solution)/shard_map/all_to_all | solution.py:26
  85.7 9.9 %all_to_all.49.came_ref = bf16[8,16,256]{2,1,0:T(8,128)(2,1)S(1)} all-to-all(bf16[8,16,256]{2,1,0:T(8,128)(2,1)S(1)} %bitcast.39), channel_id=1, replica_groups=mesh['ep_0'=8,'ep_1'=8,'ep_2'=2,'tp'=4] {'tp','ep_2'}, dimensions={0} | all-to-all | bytes 131072 | tf_op jit(solution)/shard_map/all_to_all | solution.py:26
  95.6 0.0 copy-done.4
  95.6 0.0 copy-done.2
  95.6 0.0 copy-done.3
  95.6 0.0 copy-done.1
  95.7 1.4 %shard_map.181 = (bf16[8,16,256]{2,1,0:T(8,128)(2,1)S(1)}, f32[2,256,512]{2,1,0:T(8,128)}) custom-call(bf16[128,2048]{1,0:T(8,128)(2,1)S(1)} %copy-done.1, bf16[8,16,256]{2,1,0:T(8,128)(2,1)S(1)} %all_to_all.49.came_ref, f32[1,2048]{1,0:T(1,128)S(1)} %bitcast.33, bf16[4,2048]{1,0:T(4,128)(2,1)S(1)} %get-tuple-element.72.group_ref, ...), custom_call_target="tpu_custom_call" | custom-call | tf_op jit(solution)/shard_map/pallas_call | solution.py:410
  97.0 8.0 %all_to_all.50 = bf16[8,16,256]{2,1,0:T(8,128)(2,1)S(1)} all-to-all(bf16[8,16,256]{2,1,0:T(8,128)(2,1)S(1)} %get-tuple-element.75), channel_id=1, replica_groups=mesh['ep_0'=8,'ep_1'=8,'ep_2'=2,'tp'=4] {'tp','ep_2'}, dimensions={0} | all-to-all | bytes 131072 | tf_op jit(solution)/shard_map/all_to_all | solution.py:26
  105.0 0.2 convolution_convert_fusion.1
  105.3 15.3 %all_to_all.51 = bf16[64,4,256]{2,1,0:T(4,128)(2,1)S(1)} all-to-all(bf16[64,4,256]{2,1,0:T(4,128)(2,1)S(1)} %reshape.43), channel_id=1, replica_groups=mesh['ep_0'=8,'ep_1'=8,'ep_2'=2,'tp'=4] {'ep_0','ep_1'}, dimensions={0} | all-to-all | bytes 262144 | tf_op jit(solution)/shard_map/all_to_all | solution.py:26
  120.6 0.1 convert_reduce_fusion
  120.8 9.0 %all_to_all.52 = bf16[8,2,256]{2,1,0:T(2,128)(2,1)S(1)} all-to-all(bf16[8,2,256]{2,1,0:T(2,128)(2,1)S(1)} %bitcast.42), channel_id=1, replica_groups=mesh['ep_0'=8,'ep_1'=8,'ep_2'=2,'tp'=4] {'tp','ep_2'}, dimensions={0} | all-to-all | bytes 16384 | tf_op jit(solution)/shard_map/all_to_all | solution.py:26
  129.8 0.6 copy.27
  (13 shorter events, 0.2 us)
Async XLA Ops:
  2.4 30.1 %all-to-all-start = ((bf16[8,16,1792]{2,1,0:T(8,128)(2,1)}), bf16[8,16,1792]{2,1,0:T(8,128)(2,1)S(1)}, u32[]{:S(2)}, u32[]{:S(2)}) async-start(bf16[8,16,1792]{2,1,0:T(8,128)(2,1)} %get-tuple-element.52), calls=%async_computation | async-start | bytes 917504 | tf_op jit(solution)/shard_map/all_to_all | solution.py:26
  13.3 32.3 %copy-start = (f32[2,1,256,512]{3,2,1,0:T(8,128)S(1)}, f32[2,1,256,512]{3,2,1,0:T(8,128)}, u32[]{:S(2)}) copy-start(f32[2,1,256,512]{3,2,1,0:T(8,128)} %param.18) | copy-start | bytes 3145732
  56.2 39.5 %copy-start.4 = (bf16[1,128,2048]{2,1,0:T(8,128)(2,1)S(1)}, bf16[1,128,2048]{2,1,0:T(8,128)(2,1)}, u32[]{:S(2)}) copy-start(bf16[1,128,2048]{2,1,0:T(8,128)(2,1)} %param.33) | copy-start | bytes 1572868
  71.0 24.7 %copy-start.2 = (bf16[1,2048,128]{2,1,0:T(8,128)(2,1)S(1)}, bf16[1,2048,128]{2,1,0:T(8,128)(2,1)}, u32[]{:S(2)}) copy-start(bf16[1,2048,128]{2,1,0:T(8,128)(2,1)} %param.31) | copy-start | bytes 1572868
  71.0 24.7 %copy-start.3 = (bf16[1,2048,128]{2,1,0:T(8,128)(2,1)S(1)}, bf16[1,2048,128]{2,1,0:T(8,128)(2,1)}, u32[]{:S(2)}) copy-start(bf16[1,2048,128]{2,1,0:T(8,128)(2,1)} %param.32) | copy-start | bytes 1572868
  71.4 24.3 %copy-start.1 = (bf16[128,2048]{1,0:T(8,128)(2,1)S(1)}, bf16[128,2048]{1,0:T(8,128)(2,1)}, u32[]{:S(2)}) copy-start(bf16[128,2048]{1,0:T(8,128)(2,1)} %router_ref.1) | copy-start | bytes 1572868

commit v12 on v9

--- a/solution.py
+++ b/solution.py
@@ -153,7 +153,7 @@
 
 def mix(
     which,
-    expert_ref,
+    router_ref,
     came_ref,
     gain_ref,
     group_ref,
@@ -165,12 +165,9 @@
     out_ref,
     new_ref,
     rows_ref,
-    router_ref,
-    sems,
+    sem,
 ):
-    fetch = pltpu.make_async_copy(expert_ref, router_ref, sems.at[0])
-    fetch.start()
-    copy = pltpu.make_async_copy(state_ref, new_ref, sems.at[1])
+    copy = pltpu.make_async_copy(state_ref, new_ref, sem)
     copy.start()
     expert = which()
     size = came_ref.shape[2]
@@ -185,7 +182,6 @@
     groups = lax.dot_general(rows, group_ref[...], over, preferred_element_type=F32)
     units = (gate * jax.nn.sigmoid(gate) * up).astype(BF16)
     output = jnp.dot(units, down_ref[...], preferred_element_type=F32)
-    fetch.wait()
     logits = lax.dot_general(rows, router_ref[...], over, preferred_element_type=F32)
     of_group = lax.broadcasted_iota(jnp.int32, groups.shape, 1)
     own = of_group == expert // (logits.shape[1] // groups.shape[1])
@@ -395,7 +391,7 @@
     slot_part = exchange(outward, "ep_0").astype(F32).sum(axis=0).astype(BF16)
     slot_part = to_all(slot_part.reshape(cores, CAP, piece), heads)
     came = exchange(slot_part.reshape(parts, CAP, piece), CHIPS)
-    operands = (came, ffn_gain, group_rows, rival_lane)
+    operands = (router_expert, came, ffn_gain, group_rows, rival_lane)
     operands += (w_gate[0], w_up[0], w_down[0], new_state)
     back, new_state = kernel_call(
         functools.partial(mix, lambda: lax.axis_index(EP)),
@@ -403,14 +399,13 @@
             pltpu.VMEM((parts, CAP, piece), BF16),
             jax.ShapeDtypeStruct(new_state.shape, F32),
         ],
-        in_specs=[pl.BlockSpec(memory_space=pl.ANY)] + [vmem] * len(operands),
+        in_specs=[vmem] * len(operands),
         out_specs=[vmem, pl.BlockSpec(memory_space=pl.ANY)],
         scratch_shapes=[
             pltpu.VMEM((CAP, width), F32),
-            pltpu.VMEM(router_expert.shape, BF16),
-            pltpu.SemaphoreType.DMA((2,)),
-        ],
-    )(router_expert, *map(on_chip, operands))
+            pltpu.SemaphoreType.DMA,
+        ],
+    )(*map(on_chip, operands))
     summed = exchange(back, CHIPS).reshape(heads, cores, CAP, piece).astype(F32).sum(axis=0)
     dense = lax.dot_general(
         select,

time: 131 us -> 131 us (level)
  no operation moved by 1% of the time
where the time goes in v12:
time: 131 us; the launch traced here: 130 us
  blocking collectives  113 us (86%)
  starting transfers between devices  10.9 us (8%)
  Pallas kernels  4.53 us (3%)
    all_to_all x8, blocking collectives, exchange(): came = lax.all_to_all(blocks, axes, split_axis=0, concat_axis=0, tiled=True)  93.8 us
    all_gather x1, blocking collectives, on_device(): rows_in = lax.all_gather(residual_in, SLAB, axis=0, tiled=True)  18.9 us
    all_to_all x1, starting transfers between devices, exchange(): came = lax.all_to_all(blocks, axes, split_axis=0, concat_axis=0, tiled=True)  10.9 us
  transfers between devices with their start and end apart: 1, of which 0 were waited for; matrix products, arithmetic and copies ran while one was open for 0% of the time, Pallas kernels for 0%

profile of v12, /device:TPU:1, one launch (start us, length us, event | category | flops | bytes accessed | tf_op | source)
XLA Modules:
  0.0 130.2 jit_solution(8724943241645456202)
XLA Ops:
  0.6 1.7 %shard_map.176 = (bf16[8,16,1792]{2,1,0:T(8,128)(2,1)}, bf16[2048,128]{1,0:T(8,128)(2,1)S(1)}, bf16[256,256]{1,0:T(8,128)(2,1)S(1)}, bf16[32,256]{1,0:T(8,128)(2...) custom-call(bf16[16,256]{1,0:T(8,128)(2,1)} %refs_0_.1, ...), custom_call_target="tpu_custom_call" | custom-call | tf_op jit(solution)/shard_map/pallas_call | solution.py:315
  2.4 10.9 %all-to-all-start = ((bf16[8,16,1792]{2,1,0:T(8,128)(2,1)}), bf16[8,16,1792]{2,1,0:T(8,128)(2,1)S(1)}, u32[]{:S(2)}, u32[]{:S(2)}) async-start(bf16[8,16,1792]{2,1,0:T(8,128)(2,1)} %get-tuple-element.52), calls=%async_computation | async-start | bytes 917504 | tf_op jit(solution)/shard_map/all_to_all | solution.py:26
  13.3 0.0 copy-start
  13.3 18.9 %all-gather = bf16[16,2,2048]{2,1,0:T(2,128)(2,1)S(1)} all-gather(bf16[1,2,2048]{2,1,0:T(2,128)(2,1)S(1)} %bitcast.35), channel_id=1, replica_groups=mesh['ep_0'=8,'ep_1'=8,'ep_2'=2,'tp'=4] {'ep_1','ep_2'}, dimensions={0}, use_global_device_ids=true | all-gather | bytes 139264 | tf_op jit(solution)/shard_map/all_gather | solution.py:339
  32.1 0.1 reshape.50.rows_ref
  32.2 0.3 shard_map.177
  32.5 0.0 all-to-all-done
  32.5 0.2 convolution_convert_fusion
  32.7 12.9 %all_to_all.45 = bf16[16,2,1280]{2,1,0:T(2,128)(2,1)S(1)} all-to-all(bf16[16,2,1280]{2,1,0:T(2,128)(2,1)S(1)} %reshape.37), channel_id=1, replica_groups=mesh['ep_0'=8,'ep_1'=8,'ep_2'=2,'tp'=4] {'ep_1','ep_2'}, dimensions={0} | all-to-all | bytes 163840 | tf_op jit(solution)/shard_map/all_to_all | solution.py:26
  45.6 0.0 copy-done
  45.6 0.7 shard_map.178
  46.3 9.9 %all_to_all.46 = bf16[16,2,512]{2,1,0:T(2,128)(2,1)S(1)} all-to-all(bf16[16,2,512]{2,1,0:T(2,128)(2,1)S(1)} %get-tuple-element.62), channel_id=1, replica_groups=mesh['ep_0'=8,'ep_1'=8,'ep_2'=2,'tp'=4] {'ep_1','ep_2'}, dimensions={0} | all-to-all | bytes 65536 | tf_op jit(solution)/shard_map/all_to_all | solution.py:26
  56.2 0.0 copy-start.4
  56.2 0.3 shard_map.179
  56.5 14.5 %all_to_all.47.came_ref = bf16[64,4,128]{2,1,0:T(4,128)(2,1)S(1)} all-to-all(bf16[64,4,128]{2,1,0:T(4,128)(2,1)S(1)} %get-tuple-element.67), channel_id=1, replica_groups=mesh['ep_0'=8,'ep_1'=8,'ep_2'=2,'tp'=4] {'ep_1','ep_2','tp'}, dimensions={0} | all-to-all | bytes 131072 | tf_op jit(solution)/shard_map/all_to_all | solution.py:26
  71.0 0.0 copy-start.2
  71.0 0.0 copy-start.3
  71.0 0.4 shard_map.180
  71.4 0.0 copy-start.1
  71.4 14.3 %all_to_all.48 = bf16[8,32,256]{2,1,0:T(8,128)(2,1)S(1)} all-to-all(bf16[8,32,256]{2,1,0:T(8,128)(2,1)S(1)} %get-tuple-element.70), channel_id=1, replica_groups=mesh['ep_0'=8,'ep_1'=8,'ep_2'=2,'tp'=4] {'ep_0'}, dimensions={0} | all-to-all | bytes 262144 | tf_op jit(solution)/shard_map/all_to_all | solution.py:26
  85.7 9.9 %all_to_all.49.came_ref = bf16[8,16,256]{2,1,0:T(8,128)(2,1)S(1)} all-to-all(bf16[8,16,256]{2,1,0:T(8,128)(2,1)S(1)} %bitcast.39), channel_id=1, replica_groups=mesh['ep_0'=8,'ep_1'=8,'ep_2'=2,'tp'=4] {'tp','ep_2'}, dimensions={0} | all-to-all | bytes 131072 | tf_op jit(solution)/shard_map/all_to_all | solution.py:26
  95.6 0.0 copy-done.4
  95.6 0.0 copy-done.2
  95.6 0.0 copy-done.3
  95.6 0.0 copy-done.1
  95.7 1.2 shard_map.181
  96.9 8.0 %all_to_all.50 = bf16[8,16,256]{2,1,0:T(8,128)(2,1)S(1)} all-to-all(bf16[8,16,256]{2,1,0:T(8,128)(2,1)S(1)} %get-tuple-element.75), channel_id=1, replica_groups=mesh['ep_0'=8,'ep_1'=8,'ep_2'=2,'tp'=4] {'tp','ep_2'}, dimensions={0} | all-to-all | bytes 131072 | tf_op jit(solution)/shard_map/all_to_all | solution.py:26
  104.9 0.2 convolution_convert_fusion.1
  105.2 15.3 %all_to_all.51 = bf16[64,4,256]{2,1,0:T(4,128)(2,1)S(1)} all-to-all(bf16[64,4,256]{2,1,0:T(4,128)(2,1)S(1)} %reshape.43), channel_id=1, replica_groups=mesh['ep_0'=8,'ep_1'=8,'ep_2'=2,'tp'=4] {'ep_0','ep_1'}, dimensions={0} | all-to-all | bytes 262144 | tf_op jit(solution)/shard_map/all_to_all | solution.py:26
  120.5 0.1 convert_reduce_fusion
  120.6 9.0 %all_to_all.52 = bf16[8,2,256]{2,1,0:T(2,128)(2,1)S(1)} all-to-all(bf16[8,2,256]{2,1,0:T(2,128)(2,1)S(1)} %bitcast.42), channel_id=1, replica_groups=mesh['ep_0'=8,'ep_1'=8,'ep_2'=2,'tp'=4] {'tp','ep_2'}, dimensions={0} | all-to-all | bytes 16384 | tf_op jit(solution)/shard_map/all_to_all | solution.py:26
  129.6 0.6 copy.27
  (13 shorter events, 0.2 us)
Async XLA Ops:
  2.4 30.1 %all-to-all-start = ((bf16[8,16,1792]{2,1,0:T(8,128)(2,1)}), bf16[8,16,1792]{2,1,0:T(8,128)(2,1)S(1)}, u32[]{:S(2)}, u32[]{:S(2)}) async-start(bf16[8,16,1792]{2,1,0:T(8,128)(2,1)} %get-tuple-element.52), calls=%async_computation | async-start | bytes 917504 | tf_op jit(solution)/shard_map/all_to_all | solution.py:26
  13.3 32.3 %copy-start = (f32[2,1,256,512]{3,2,1,0:T(8,128)S(1)}, f32[2,1,256,512]{3,2,1,0:T(8,128)}, u32[]{:S(2)}) copy-start(f32[2,1,256,512]{3,2,1,0:T(8,128)} %param.18) | copy-start | bytes 3145732
  56.2 39.5 %copy-start.4 = (bf16[1,128,2048]{2,1,0:T(8,128)(2,1)S(1)}, bf16[1,128,2048]{2,1,0:T(8,128)(2,1)}, u32[]{:S(2)}) copy-start(bf16[1,128,2048]{2,1,0:T(8,128)(2,1)} %param.33) | copy-start | bytes 1572868
  71.0 24.7 %copy-start.2 = (bf16[1,2048,128]{2,1,0:T(8,128)(2,1)S(1)}, bf16[1,2048,128]{2,1,0:T(8,128)(2,1)}, u32[]{:S(2)}) copy-start(bf16[1,2048,128]{2,1,0:T(8,128)(2,1)} %param.31) | copy-start | bytes 1572868
  71.0 24.7 %copy-start.3 = (bf16[1,2048,128]{2,1,0:T(8,128)(2,1)S(1)}, bf16[1,2048,128]{2,1,0:T(8,128)(2,1)}, u32[]{:S(2)}) copy-start(bf16[1,2048,128]{2,1,0:T(8,128)(2,1)} %param.32) | copy-start | bytes 1572868
  71.4 24.3 %copy-start.1 = (bf16[128,2048]{1,0:T(8,128)(2,1)S(1)}, bf16[128,2048]{1,0:T(8,128)(2,1)}, u32[]{:S(2)}) copy-start(bf16[128,2048]{1,0:T(8,128)(2,1)} %router_ref.1) | copy-start | bytes 1572868

commit v13 on v9

--- a/solution.py
+++ b/solution.py
@@ -170,8 +170,11 @@
 ):
     fetch = pltpu.make_async_copy(expert_ref, router_ref, sems.at[0])
     fetch.start()
-    copy = pltpu.make_async_copy(state_ref, new_ref, sems.at[1])
-    copy.start()
+    copies = []
+    for seq in range(state_ref.shape[0]):
+        source, target = state_ref.at[seq], new_ref.at[seq]
+        copies.append(pltpu.make_async_copy(source, target, sems.at[1 + seq]))
+        copies[-1].start()
     expert = which()
     size = came_ref.shape[2]
     for at in range(came_ref.shape[0]):
@@ -198,7 +201,8 @@
     piece = out_ref.shape[2]
     for at in range(out_ref.shape[0]):
         out_ref[at] = output[:, piece * at : piece * (at + 1)]
-    copy.wait()
+    for copy in copies:
+        copy.wait()
 
 
 def pack(heads_ref, held_ref, res_ref, _, out_ref, __):
@@ -408,7 +412,7 @@
         scratch_shapes=[
             pltpu.VMEM((CAP, width), F32),
             pltpu.VMEM(router_expert.shape, BF16),
-            pltpu.SemaphoreType.DMA((2,)),
+            pltpu.SemaphoreType.DMA((1 + seqs,)),
         ],
     )(router_expert, *map(on_chip, operands))
     summed = exchange(back, CHIPS).reshape(heads, cores, CAP, piece).astype(F32).sum(axis=0)

time: 131 us -> 131 us (level)
  no operation moved by 1% of the time
where the time goes in v13:
time: 131 us; the launch traced here: 130 us
  blocking collectives  113 us (86%)
  starting transfers between devices  10.9 us (8%)
  Pallas kernels  4.47 us (3%)
    all_to_all x8, blocking collectives, exchange(): came = lax.all_to_all(blocks, axes, split_axis=0, concat_axis=0, tiled=True)  93.8 us
    all_gather x1, blocking collectives, on_device(): rows_in = lax.all_gather(residual_in, SLAB, axis=0, tiled=True)  18.9 us
    all_to_all x1, starting transfers between devices, exchange(): came = lax.all_to_all(blocks, axes, split_axis=0, concat_axis=0, tiled=True)  10.9 us
  transfers between devices with their start and end apart: 1, of which 0 were waited for; matrix products, arithmetic and copies ran while one was open for 0% of the time, Pallas kernels for 0%

profile of v13, /device:TPU:1, one launch (start us, length us, event | category | flops | bytes accessed | tf_op | source)
XLA Modules:
  0.0 130.2 jit_solution(3526428015716160106)
XLA Ops:
  0.6 1.7 %shard_map.176 = (bf16[8,16,1792]{2,1,0:T(8,128)(2,1)}, bf16[2048,128]{1,0:T(8,128)(2,1)S(1)}, bf16[256,256]{1,0:T(8,128)(2,1)S(1)}, bf16[32,256]{1,0:T(8,128)(2...) custom-call(bf16[16,256]{1,0:T(8,128)(2,1)} %refs_0_.1, ...), custom_call_target="tpu_custom_call" | custom-call | tf_op jit(solution)/shard_map/pallas_call | solution.py:323
  2.4 10.9 %all-to-all-start = ((bf16[8,16,1792]{2,1,0:T(8,128)(2,1)}), bf16[8,16,1792]{2,1,0:T(8,128)(2,1)S(1)}, u32[]{:S(2)}, u32[]{:S(2)}) async-start(bf16[8,16,1792]{2,1,0:T(8,128)(2,1)} %get-tuple-element.52), calls=%async_computation | async-start | bytes 917504 | tf_op jit(solution)/shard_map/all_to_all | solution.py:26
  13.3 0.0 copy-start
  13.3 18.9 %all-gather = bf16[16,2,2048]{2,1,0:T(2,128)(2,1)S(1)} all-gather(bf16[1,2,2048]{2,1,0:T(2,128)(2,1)S(1)} %bitcast.35), channel_id=1, replica_groups=mesh['ep_0'=8,'ep_1'=8,'ep_2'=2,'tp'=4] {'ep_1','ep_2'}, dimensions={0}, use_global_device_ids=true | all-gather | bytes 139264 | tf_op jit(solution)/shard_map/all_gather | solution.py:347
  32.1 0.1 reshape.50.rows_ref
  32.2 0.3 shard_map.177
  32.5 0.0 all-to-all-done
  32.5 0.2 convolution_convert_fusion
  32.7 12.9 %all_to_all.45 = bf16[16,2,1280]{2,1,0:T(2,128)(2,1)S(1)} all-to-all(bf16[16,2,1280]{2,1,0:T(2,128)(2,1)S(1)} %reshape.37), channel_id=1, replica_groups=mesh['ep_0'=8,'ep_1'=8,'ep_2'=2,'tp'=4] {'ep_1','ep_2'}, dimensions={0} | all-to-all | bytes 163840 | tf_op jit(solution)/shard_map/all_to_all | solution.py:26
  45.6 0.0 copy-done
  45.6 0.7 shard_map.178
  46.3 9.9 %all_to_all.46 = bf16[16,2,512]{2,1,0:T(2,128)(2,1)S(1)} all-to-all(bf16[16,2,512]{2,1,0:T(2,128)(2,1)S(1)} %get-tuple-element.62), channel_id=1, replica_groups=mesh['ep_0'=8,'ep_1'=8,'ep_2'=2,'tp'=4] {'ep_1','ep_2'}, dimensions={0} | all-to-all | bytes 65536 | tf_op jit(solution)/shard_map/all_to_all | solution.py:26
  56.2 0.0 copy-start.4
  56.2 0.3 shard_map.179
  56.5 14.5 %all_to_all.47.came_ref = bf16[64,4,128]{2,1,0:T(4,128)(2,1)S(1)} all-to-all(bf16[64,4,128]{2,1,0:T(4,128)(2,1)S(1)} %get-tuple-element.67), channel_id=1, replica_groups=mesh['ep_0'=8,'ep_1'=8,'ep_2'=2,'tp'=4] {'ep_1','ep_2','tp'}, dimensions={0} | all-to-all | bytes 131072 | tf_op jit(solution)/shard_map/all_to_all | solution.py:26
  71.0 0.0 copy-start.2
  71.0 0.0 copy-start.3
  71.0 0.4 shard_map.180
  71.4 0.0 copy-start.1
  71.4 14.3 %all_to_all.48 = bf16[8,32,256]{2,1,0:T(8,128)(2,1)S(1)} all-to-all(bf16[8,32,256]{2,1,0:T(8,128)(2,1)S(1)} %get-tuple-element.70), channel_id=1, replica_groups=mesh['ep_0'=8,'ep_1'=8,'ep_2'=2,'tp'=4] {'ep_0'}, dimensions={0} | all-to-all | bytes 262144 | tf_op jit(solution)/shard_map/all_to_all | solution.py:26
  85.7 9.9 %all_to_all.49.came_ref = bf16[8,16,256]{2,1,0:T(8,128)(2,1)S(1)} all-to-all(bf16[8,16,256]{2,1,0:T(8,128)(2,1)S(1)} %bitcast.39), channel_id=1, replica_groups=mesh['ep_0'=8,'ep_1'=8,'ep_2'=2,'tp'=4] {'tp','ep_2'}, dimensions={0} | all-to-all | bytes 131072 | tf_op jit(solution)/shard_map/all_to_all | solution.py:26
  95.6 0.0 copy-done.4
  95.6 0.0 copy-done.2
  95.6 0.0 copy-done.3
  95.6 0.0 copy-done.1
  95.7 1.2 shard_map.181
  96.8 8.0 %all_to_all.50 = bf16[8,16,256]{2,1,0:T(8,128)(2,1)S(1)} all-to-all(bf16[8,16,256]{2,1,0:T(8,128)(2,1)S(1)} %get-tuple-element.75), channel_id=1, replica_groups=mesh['ep_0'=8,'ep_1'=8,'ep_2'=2,'tp'=4] {'tp','ep_2'}, dimensions={0} | all-to-all | bytes 131072 | tf_op jit(solution)/shard_map/all_to_all | solution.py:26
  104.8 0.2 convolution_convert_fusion.1
  105.1 15.3 %all_to_all.51 = bf16[64,4,256]{2,1,0:T(4,128)(2,1)S(1)} all-to-all(bf16[64,4,256]{2,1,0:T(4,128)(2,1)S(1)} %reshape.43), channel_id=1, replica_groups=mesh['ep_0'=8,'ep_1'=8,'ep_2'=2,'tp'=4] {'ep_0','ep_1'}, dimensions={0} | all-to-all | bytes 262144 | tf_op jit(solution)/shard_map/all_to_all | solution.py:26
  120.4 0.1 convert_reduce_fusion
  120.6 9.0 %all_to_all.52 = bf16[8,2,256]{2,1,0:T(2,128)(2,1)S(1)} all-to-all(bf16[8,2,256]{2,1,0:T(2,128)(2,1)S(1)} %bitcast.42), channel_id=1, replica_groups=mesh['ep_0'=8,'ep_1'=8,'ep_2'=2,'tp'=4] {'tp','ep_2'}, dimensions={0} | all-to-all | bytes 16384 | tf_op jit(solution)/shard_map/all_to_all | solution.py:26
  129.6 0.6 copy.27
  (13 shorter events, 0.2 us)
Async XLA Ops:
  2.4 30.1 %all-to-all-start = ((bf16[8,16,1792]{2,1,0:T(8,128)(2,1)}), bf16[8,16,1792]{2,1,0:T(8,128)(2,1)S(1)}, u32[]{:S(2)}, u32[]{:S(2)}) async-start(bf16[8,16,1792]{2,1,0:T(8,128)(2,1)} %get-tuple-element.52), calls=%async_computation | async-start | bytes 917504 | tf_op jit(solution)/shard_map/all_to_all | solution.py:26
  13.3 32.3 %copy-start = (f32[2,1,256,512]{3,2,1,0:T(8,128)S(1)}, f32[2,1,256,512]{3,2,1,0:T(8,128)}, u32[]{:S(2)}) copy-start(f32[2,1,256,512]{3,2,1,0:T(8,128)} %param.18) | copy-start | bytes 3145732
  56.2 39.5 %copy-start.4 = (bf16[1,128,2048]{2,1,0:T(8,128)(2,1)S(1)}, bf16[1,128,2048]{2,1,0:T(8,128)(2,1)}, u32[]{:S(2)}) copy-start(bf16[1,128,2048]{2,1,0:T(8,128)(2,1)} %param.33) | copy-start | bytes 1572868
  71.0 24.7 %copy-start.2 = (bf16[1,2048,128]{2,1,0:T(8,128)(2,1)S(1)}, bf16[1,2048,128]{2,1,0:T(8,128)(2,1)}, u32[]{:S(2)}) copy-start(bf16[1,2048,128]{2,1,0:T(8,128)(2,1)} %param.31) | copy-start | bytes 1572868
  71.0 24.7 %copy-start.3 = (bf16[1,2048,128]{2,1,0:T(8,128)(2,1)S(1)}, bf16[1,2048,128]{2,1,0:T(8,128)(2,1)}, u32[]{:S(2)}) copy-start(bf16[1,2048,128]{2,1,0:T(8,128)(2,1)} %param.32) | copy-start | bytes 1572868
  71.4 24.3 %copy-start.1 = (bf16[128,2048]{1,0:T(8,128)(2,1)S(1)}, bf16[128,2048]{1,0:T(8,128)(2,1)}, u32[]{:S(2)}) copy-start(bf16[128,2048]{1,0:T(8,128)(2,1)} %expert_ref.1) | copy-start | bytes 1572868
